TPU v7x, 256 devices: a whole 4x4x8 slice. The times are simulated.
256 devices in a mesh: ep: 64 (over z, y, x_hi), tp: 4 (over x_lo, core).
Axes of the slice: x: 4 (x_hi: 2, x_lo: 2; x = x_hi * 2 + x_lo), y: 4, z: 8, core: 2. Of those that a mesh axis runs over, the one named last changes fastest.
Arguments:
- tokens: bfloat16 [6144, 2048], P('ep'), may hold values from -6 to 6
- norm_gain: bfloat16 [2048], replicated, may hold values from 0.099609375 to 1.8984375
- in_weight: bfloat16 [2048, 1024], P(None, 'tp'), may hold values from -0.125 to 0.125
- sequence_state_real: float32 [6144, 4096], P('ep', 'tp'), may hold values from -6 to 6
- sequence_state_imaginary: float32 [6144, 4096], P('ep', 'tp'), may hold values from -6 to 6
- eigen_decay_real: float32 [64, 64], P('tp'), may hold values from -1 to -0.2
- log_step: float32 [64], P('tp'), may hold values from -4.6 to 0
- input_matrix_real: float32 [64, 64, 16], P('tp'), may hold values from -1 to 1
- input_matrix_imaginary: float32 [64, 64, 16], P('tp'), may hold values from -1 to 1
- output_matrix_real: float32 [64, 16, 64], P('tp'), may hold values from -0.75 to 0.75
- output_matrix_imaginary: float32 [64, 16, 64], P('tp'), may hold values from -0.75 to 0.75
- channel_skip_scale: float32 [64, 16], P('tp'), may hold values from -4 to 4
- out_weight: bfloat16 [1024, 2048], P('tp'), may hold values from -0.25 to 0.25
- ffn_gain: bfloat16 [2048], replicated, may hold values from 0.099609375 to 1.8984375
- routes: int32 [6144, 2], P('ep'), may hold values from 0 to 63, all different within a row; in each aligned block of 96 rows (0 to 95, 96 to 191, ...) at most 6 rows name the same one
- group_weight: float32 [6144], P('ep'), may hold values from 0.3 to 1
- expert_logit: float32 [6144, 2], P('ep'), may hold values from -6 to 6
- expert_gate: bfloat16 [64, 2048, 512], P('ep', None, 'tp'), may hold values from -0.125 to 0.125
- expert_up: bfloat16 [64, 2048, 512], P('ep', None, 'tp'), may hold values from -0.125 to 0.125
- expert_down: bfloat16 [64, 512, 2048], P('ep', 'tp'), may hold values from -0.5 to 0.5
- dense_gate: bfloat16 [2048, 2048], P(None, 'tp'), may hold values from -0.125 to 0.125
- dense_up: bfloat16 [2048, 2048], P(None, 'tp'), may hold values from -0.125 to 0.125
- dense_down: bfloat16 [2048, 2048], P('tp'), may hold values from -0.25 to 0.25
- blend_weight: bfloat16 [2048], replicated, may hold values from -0.25 to 0.25
Outputs:
- new_tokens: bfloat16 [6144, 2048], P('ep', 'tp')
- new_state_real: float32 [6144, 4096], P('ep', 'tp')
- new_state_imag: float32 [6144, 4096], P('ep', 'tp')
Inputs may be any that keep to these rules, and one draw needn't show every extreme that they name: `routes`: each row names 2 different experts. Among the rows of one index of ep (aligned blocks of 96 rows) no expert is named by more than 6 rows, and in some block one expert is named by exactly 6 rows.
All inputs are finite; a program needn't handle non-finite values.
Results may differ from a plain program's by a relative error of at most 0.014.
Values may be sent and summed in bfloat16 or wider, within the bound.
No kernel may reach another device: no remote copies, remote signals or barrier semaphores. Data moves between devices by JAX's collectives and lax.ppermute only.
A program may use at most 64 MiB of HBM per device.

v0:
```python
import functools
import math

import jax
import jax.numpy as jnp
from jax import lax
from jax.experimental import pallas as pl
from jax.experimental.pallas import tpu as pltpu
from jax.sharding import PartitionSpec as P


EPS = 1e-06
F32 = jnp.float32
BF16 = jnp.bfloat16
HIGHEST = lax.Precision.HIGHEST
VMEM = pl.BlockSpec(memory_space=pltpu.VMEM)
SMEM = pl.BlockSpec(memory_space=pltpu.SMEM)
ANY = pl.BlockSpec(memory_space=pl.ANY)
HBM = pl.BlockSpec(memory_space=pltpu.HBM)
FREE = pl.BlockSpec(memory_space=pltpu.VMEM)


def iota(shape, dim):
    return lax.broadcasted_iota(jnp.int32, shape, dim)


def nt_dot(a, b, precision=None):
    return lax.dot_general(
        a, b, (((1,), (1,)), ((), ())), precision=precision, preferred_element_type=F32
    )


def dot(a, b, precision=None):
    return jnp.dot(a, b, precision=precision, preferred_element_type=F32)


def cols_of(index, size):
    return pl.ds(pl.multiple_of(index * size, size), size)


def exchanged(value, mask):
    return lax.ppermute(value, "tp", [(i, i ^ mask) for i in range(4)])


def gathered(value):
    across = exchanged(value, 2)
    return [value, exchanged(value, 1), across, exchanged(across, 1)]


def spread_blocks(small, channels):
    rows, entries = small.shape
    groups = rows // channels
    width = groups * entries
    tiler = (iota((entries, width), 1) % entries == iota((entries, width), 0)).astype(BF16)
    tiled = dot(small.astype(BF16), tiler)
    mine = iota((rows, width), 0) // channels == iota((rows, width), 1) // entries
    return jnp.where(mine, tiled, 0.0).astype(BF16)


def row_of(small):
    groups, n = small.shape
    width = groups * n
    tiler = (iota((n, width), 1) % n == iota((n, width), 0)).astype(F32)
    tiled = dot(small, tiler, HIGHEST)
    mine = iota((groups, width), 0) == iota((groups, width), 1) // n
    return jnp.sum(jnp.where(mine, tiled, 0.0), axis=0, keepdims=True)


def state_kernel(*refs):
    inputs, (p0, p1, p2, p3, new_re, new_im), held = refs[0:13], refs[13:19], refs[19:32]
    fresh_re_v, fresh_im_v, sems = refs[32:]
    t = lax.axis_index("tp")
    loads = [
        pltpu.make_async_copy(a, b, sems.at[i]) for i, (a, b) in enumerate(zip(inputs, held))
    ]
    for load in loads:
        load.start()
    decay, skip, tokens_v, gain, in_v, b_re, b_im, re_v, im_v, c_re, c_im, out_v, log_step = held
    groups, entries = decay.shape
    channels = skip.shape[1]
    width = groups * entries
    of_group = iota((1, width), 1) // entries
    loads[12].wait()
    logs = jnp.zeros((1, width), F32)
    for g in range(groups):
        logs = jnp.where(of_group == g, log_step[g], logs)
    step = jnp.exp(logs)
    loads[0].wait()
    eigen = row_of(decay[...])
    freq = math.pi * (iota((1, width), 1) % entries).astype(F32)
    magnitude = jnp.exp(eigen * step)
    turned = freq * step
    lam_re = magnitude * jnp.cos(turned)
    lam_im = magnitude * jnp.sin(turned)
    denom = eigen * eigen + freq * freq
    fac_re = ((lam_re - 1.0) * eigen + lam_im * freq) / denom
    fac_im = (lam_im * eigen - (lam_re - 1.0) * freq) / denom
    loads[2].wait()
    loads[3].wait()
    x = tokens_v[...].astype(F32)
    scale = lax.rsqrt(jnp.mean(x * x, axis=-1, keepdims=True) + EPS)
    normed = (x * scale * gain[...].astype(F32).reshape(1, -1)).astype(BF16)
    loads[4].wait()
    drive = dot(normed, in_v[...]).astype(BF16)
    loads[5].wait()
    loads[6].wait()
    in_re = dot(drive, spread_blocks(b_re[...], channels))
    in_im = dot(drive, spread_blocks(b_im[...], channels))
    loads[7].wait()
    loads[8].wait()
    was_re, was_im = re_v[...], im_v[...]
    fresh_re = lam_re * was_re - lam_im * was_im + (fac_re * in_re - fac_im * in_im)
    fresh_im = lam_re * was_im + lam_im * was_re + (fac_re * in_im + fac_im * in_re)
    fresh_re_v[...] = fresh_re
    fresh_im_v[...] = fresh_im
    stores = [
        pltpu.make_async_copy(fresh_re_v, new_re, sems.at[13]),
        pltpu.make_async_copy(fresh_im_v, new_im, sems.at[14]),
    ]
    for store in stores:
        store.start()
    for i in (1, 9, 10):
        loads[i].wait()
    mixed = (
        nt_dot(fresh_re.astype(BF16), spread_blocks(c_re[...], channels))
        - nt_dot(fresh_im.astype(BF16), spread_blocks(c_im[...], channels))
        + row_of(skip[...]) * drive.astype(F32)
    )
    act = jax.nn.gelu(mixed).astype(BF16)
    loads[11].wait()
    for m, p in enumerate((p0, p1, p2, p3)):
        p[...] = dot(act, out_v[:, cols_of(t ^ m, p.shape[1])]).astype(BF16)
    for store in stores:
        store.wait()


def reshard_kernel(gate, up, down, *pieces):
    t = lax.axis_index("tp")
    hid = gate.shape[1]
    for m, (gu, d) in enumerate(zip(pieces[:4], pieces[4:])):
        part = cols_of(t ^ m, gu.shape[0])
        gu[:, 0:hid] = gate[part, :]
        gu[:, hid:] = up[part, :]
        d[...] = down[:, cols_of(t ^ m, d.shape[1])]


def route_kernel(experts, routes, group_weight, logits, z, w, share0, share1, padded):
    rows = routes.shape[1]
    slots, lanes = z.shape
    padded[...] = jnp.full(padded.shape, -1, jnp.int32)
    padded[0:2, 0:rows] = routes[...]
    named = [padded[k : k + 1, :] for k in range(2)]
    hot = [(iota((experts, lanes), 0) == r).astype(F32) for r in named]
    earlier = (iota((lanes, lanes), 0) < iota((lanes, lanes), 1)).astype(BF16)
    before = dot((hot[0] + hot[1]).astype(BF16), earlier)
    place = [jnp.sum(before * h, axis=0, keepdims=True).astype(jnp.int32) for h in hot]
    slot = [jnp.where(r >= 0, p * experts + r, -1) for r, p in zip(named, place)]
    at = iota((slots, lanes), 0)
    z[...] = jnp.logical_or(at == slot[0], at == slot[1]).astype(F32).astype(BF16)
    eye = iota((lanes, lanes), 0) == iota((lanes, lanes), 1)
    at = iota((rows, slots), 1)
    for k in range(2):
        column = jnp.sum(jnp.where(eye, slot[k], 0), axis=1, keepdims=True)[0:rows]
        w[k * rows : (k + 1) * rows, :] = (at == column).astype(F32).astype(BF16)
    expo = jnp.exp(logits[...])
    share = group_weight[...] * expo / (expo[0:1] + expo[1:2])
    small_eye = iota((rows, rows), 0) == iota((rows, rows), 1)
    for k, out in enumerate((share0, share1)):
        column = jnp.sum(jnp.where(small_eye, share[k : k + 1], 0.0), axis=1, keepdims=True)
        out[...] = jnp.broadcast_to(column, out.shape)


def places(capacity, wide, quarter):
    blocks = quarter // wide.shape[1]
    peers = wide.shape[0] // (capacity * blocks)
    for s in range(capacity):
        for c in range(blocks):
            yield (
                pl.ds(c * capacity + s, peers, stride=capacity * blocks),
                slice(s * peers, (s + 1) * peers),
                slice(c * wide.shape[1], (c + 1) * wide.shape[1]),
            )


def three_terms(row, size):
    if row.shape[1] < size:
        row = jnp.concatenate([row, jnp.zeros((1, size - row.shape[1]), F32)], axis=1)
    high = row.astype(BF16).astype(F32)
    middle = (row - high).astype(BF16).astype(F32)
    low = row - high - middle
    at = iota((8, size), 0)
    block = jnp.where(at == 0, high, jnp.where(at == 1, middle, jnp.where(at == 2, low, 0.0)))
    return block.astype(BF16)


def sum_terms(block):
    return jnp.sum(block.astype(F32), axis=0, keepdims=True)


def pack_kernel(capacity, tokens, p0, p1, p2, p3, z, *refs):
    resid16, packed, wide = refs[-3:]
    t = lax.axis_index("tp")
    quarter = p0.shape[1]
    total = tokens[:, cols_of(t, quarter)].astype(F32) + (
        (p0[...].astype(F32) + p1[...].astype(F32)) + (p2[...].astype(F32) + p3[...].astype(F32))
    )
    short = total.astype(BF16)
    resid16[...] = short
    gap = jnp.zeros((z.shape[1] - short.shape[0], quarter), BF16)
    spread = dot(z[...], jnp.concatenate([short, gap], axis=0))
    for strided, near, cols in places(capacity, wide, quarter):
        wide[strided, :] = spread[near, cols]
    packed[...] = wide[...].astype(BF16)


def dense_kernel(
    gains, a0, a1, a2, a3, blend_weight, gate, up, down, p0, p1, p2, p3, blend,
    full, gate_v, up_v, down_v, sems,
):
    t = lax.axis_index("tp")
    loads = [
        pltpu.make_async_copy(a, b, sems.at[i])
        for i, (a, b) in enumerate(((gate, gate_v), (up, up_v), (down, down_v)))
    ]
    for load in loads:
        load.start()
    quarter = a0.shape[1]
    for m, a in enumerate((a0, a1, a2, a3)):
        full[:, cols_of(t ^ m, quarter)] = a[...]
    x = full[...].astype(F32)
    scale = lax.rsqrt(jnp.mean(x * x, axis=-1, keepdims=True) + EPS)
    normed = (x * scale * gains[...].astype(F32)).astype(BF16)
    score = jnp.sum(
        normed.astype(F32) * blend_weight[...].astype(F32), axis=-1, keepdims=True
    )
    blend[...] = jnp.broadcast_to(jax.nn.sigmoid(score), blend.shape)
    loads[0].wait()
    pre_gate = dot(normed, gate_v[...])
    loads[1].wait()
    pre_up = dot(normed, up_v[...])
    hidden = (jax.nn.silu(pre_gate) * pre_up).astype(BF16)
    loads[2].wait()
    for m, p in enumerate((p0, p1, p2, p3)):
        p[...] = dot(hidden, down_v[:, cols_of(t ^ m, quarter)]).astype(BF16)


def enter_kernel(capacity, arrived, gains, gu0, gu1, gu2, gu3, keep, send, wide, rows, sums):
    t = lax.axis_index("tp")
    lanes = arrived.shape[1]
    quarter = rows.shape[1]
    wide[...] = arrived[...].astype(F32)
    gain = gains[:, cols_of(t, quarter)].astype(F32)
    for strided, near, cols in places(capacity, wide, quarter):
        x = wide[strided, :]
        sums[near, :] = x * x if cols.start == 0 else sums[near, :] + x * x
        rows[near, cols] = (x * gain[:, cols]).astype(BF16)
    squares = nt_dot(jnp.ones((8, lanes), F32), sums[...], HIGHEST)[0:1]
    count = rows.shape[0]
    keep[count:, :] = jnp.broadcast_to(
        jnp.concatenate([squares, jnp.zeros((1, keep.shape[1] - count), F32)], axis=1),
        (8, keep.shape[1]),
    )
    send[count:, :] = three_terms(squares, send.shape[1])
    x = rows[...]
    pair = gu0.shape[1]
    keep[0:count, 0:pair] = dot(x, gu0[...])
    send[0:count, 0:pair] = dot(x, gu1[...]).astype(BF16)
    keep[0:count, pair:] = dot(x, gu2[...])
    send[0:count, pair:] = dot(x, gu3[...]).astype(BF16)


def relay_kernel(keep, came, onward):
    pair = onward.shape[1]
    count = keep.shape[0] - 8
    onward[0:count, :] = (keep[0:count, pair:] + came[0:count, pair:].astype(F32)).astype(BF16)
    squares = keep[count : count + 1, :] + sum_terms(came[count:, :])
    onward[count : count + 8, :] = three_terms(squares[:, 0:pair], pair)
    onward[count + 8 :, :] = three_terms(squares[:, pair:], pair)


def hidden_kernel(width, keep, came, last, hidden):
    count, units = hidden.shape
    pair = 2 * units
    total = (
        keep[0:count, 0:pair] + came[0:count, 0:pair].astype(F32) + last[0:count, :].astype(F32)
    )
    squares = keep[count : count + 1, :] + sum_terms(came[count:, :])
    squares = squares + jnp.concatenate(
        [sum_terms(last[count : count + 8, :]), sum_terms(last[count + 8 :, :])], axis=1
    )
    column = jnp.transpose(jnp.broadcast_to(squares[:, 0:count], (8, count)))[:, 0:1]
    scale = lax.rsqrt(column / width + EPS)
    hidden[...] = (jax.nn.silu(total[:, 0:units] * scale) * (total[:, units:] * scale)).astype(BF16)


def leave_kernel(capacity, h0, h1, h2, h3, d0, d1, d2, d3, out, wide):
    total = dot(h0[...], d0[...])
    for h, d in ((h1, d1), (h2, d2), (h3, d3)):
        total = total + dot(h[...], d[...])
    for strided, near, cols in places(capacity, wide, total.shape[1]):
        wide[strided, :] = total[near, cols]
    out[...] = wide[...].astype(BF16)


def final_kernel(
    capacity, returned, w, share0, share1, resid, blend, p0, p1, p2, p3, out, wide, rows
):
    count, quarter = resid.shape
    wide[...] = returned[...].astype(F32)
    for strided, near, cols in places(capacity, wide, quarter):
        rows[near, cols] = wide[strided, :].astype(BF16)
    picked = dot(w[...], rows[...])
    lanes = wide.shape[1]
    for c in range(quarter // lanes):
        cols = slice(c * lanes, (c + 1) * lanes)
        moe = share0[...] * picked[0:count, cols] + share1[...] * picked[count:, cols]
        dense = (p0[:, cols].astype(F32) + p1[:, cols].astype(F32)) + (
            p2[:, cols].astype(F32) + p3[:, cols].astype(F32)
        )
        out[:, cols] = (resid[:, cols].astype(F32) + moe + blend[...] * dense).astype(BF16)


def call(kernel, outs, scratch=(), limit=4, in_specs=None, out_specs=None):
    out_specs = out_specs or [VMEM] * len(outs)
    out_shape = [
        pltpu.VMEM(s, d) if spec is VMEM else jax.ShapeDtypeStruct(s, d)
        for (s, d), spec in zip(outs, out_specs)
    ]

    def run(*args):
        specs = in_specs or [VMEM] * len(args)
        spaces = {id(VMEM): pltpu.VMEM, id(HBM): pltpu.HBM}
        fixed = [
            pltpu.with_memory_space_constraint(a, spaces.get(id(spec), pl.ANY))
            for a, spec in zip(args, specs)
        ]
        return pl.pallas_call(
            kernel,
            out_shape=tuple(out_shape),
            in_specs=specs,
            out_specs=tuple(out_specs),
            scratch_shapes=list(scratch),
            compiler_params=pltpu.CompilerParams(vmem_limit_bytes=limit << 20),
        )(*fixed)

    return run


def per_device(
    tokens,
    norm_gain,
    in_weight,
    sequence_state_real,
    sequence_state_imaginary,
    eigen_decay_real,
    log_step,
    input_matrix_real,
    input_matrix_imaginary,
    output_matrix_real,
    output_matrix_imaginary,
    channel_skip_scale,
    out_weight,
    ffn_gain,
    routes,
    group_weight,
    expert_logit,
    expert_gate,
    expert_up,
    expert_down,
    dense_gate,
    dense_up,
    dense_down,
    blend_weight,
):
    rows, width = tokens.shape
    tp = lax.axis_size("tp")
    ep = lax.axis_size("ep")
    quarter = width // tp
    lanes = 128
    blocks = quarter // lanes
    capacity = max(2, 2 * rows * routes.shape[1] // (ep * expert_gate.shape[0]))
    slots = ep * capacity
    groups, entries, channels = input_matrix_real.shape
    hid = expert_gate.shape[2]
    gate = expert_gate.reshape(width, hid)
    up = expert_up.reshape(width, hid)
    down = expert_down.reshape(hid, width)
    piece = ((rows, quarter), BF16)

    def by_channel(matrix):
        return jnp.swapaxes(matrix, 1, 2).reshape(groups * channels, entries)

    states = ((rows, groups * entries), F32)
    state_inputs = (
        eigen_decay_real,
        channel_skip_scale,
        tokens,
        norm_gain,
        in_weight,
        by_channel(input_matrix_real),
        by_channel(input_matrix_imaginary),
        sequence_state_real,
        sequence_state_imaginary,
        output_matrix_real.reshape(groups * channels, entries),
        output_matrix_imaginary.reshape(groups * channels, entries),
        out_weight,
        log_step,
    )
    *mix, new_re, new_im = call(
        state_kernel,
        [piece] * 4 + [states] * 2,
        [pltpu.VMEM(x.shape, x.dtype) for x in state_inputs[:-1]]
        + [pltpu.SMEM(log_step.shape, F32)]
        + [pltpu.VMEM(states[0], F32)] * 2
        + [pltpu.SemaphoreType.DMA((15,))],
        20,
        [HBM] * 13,
        [VMEM] * 4 + [HBM] * 2,
    )(*state_inputs)
    mix = [mix[0]] + [exchanged(mix[m], m) for m in (1, 2, 3)]
    pieces = call(
        reshard_kernel, [((quarter, 2 * hid), BF16)] * 4 + [((hid, quarter), BF16)] * 4
    )(gate, up, down)
    moved = [pieces[0]] + [exchanged(pieces[m], m) for m in (1, 2, 3)]
    downs = [pieces[4]] + [exchanged(pieces[4 + m], m) for m in (1, 2, 3)]
    z, w, share0, share1 = call(
        functools.partial(route_kernel, ep),
        [((slots, lanes), BF16), ((2 * rows, slots), BF16)] + [((rows, lanes), F32)] * 2,
        [pltpu.VMEM((8, lanes), jnp.int32)],
    )(routes.T, group_weight.reshape(1, rows), expert_logit.T)
    wide = pltpu.VMEM((slots * blocks, lanes), F32)
    resid16, packed = call(
        functools.partial(pack_kernel, capacity),
        [piece, ((slots * blocks, lanes), BF16)],
        [wide],
        8,
        out_specs=[VMEM, FREE],
    )(tokens, *mix, z)
    arrived = lax.all_to_all(
        packed.reshape(ep, capacity * blocks, lanes), "ep", 0, 0, tiled=True
    ).reshape(slots * blocks, lanes)
    near = gathered(resid16)
    gains = ffn_gain.reshape(1, width)
    *dense, blend = call(
        dense_kernel,
        [piece] * 4 + [((rows, lanes), F32)],
        [pltpu.VMEM((rows, width), BF16)]
        + [pltpu.VMEM(x.shape, BF16) for x in (dense_gate, dense_up, dense_down)]
        + [pltpu.SemaphoreType.DMA((3,))],
        12,
        [VMEM] * 6 + [HBM] * 3,
    )(gains, *near, blend_weight.reshape(1, width), dense_gate, dense_up, dense_down)
    dense = [dense[0]] + [exchanged(dense[m], m) for m in (1, 2, 3)]
    keep, send = call(
        functools.partial(enter_kernel, capacity),
        [((slots + 8, 4 * hid), F32), ((slots + 8, 4 * hid), BF16)],
        [wide, pltpu.VMEM((slots, quarter), BF16), pltpu.VMEM((slots, lanes), F32)],
        8,
    )(arrived, gains, *moved)
    came = exchanged(send, 1)
    (onward,) = call(relay_kernel, [((slots + 16, 2 * hid), BF16)])(keep, came)
    last = exchanged(onward, 2)
    (hidden,) = call(
        functools.partial(hidden_kernel, float(width)), [((slots, hid), BF16)]
    )(keep, came, last)
    (sent,) = call(
        functools.partial(leave_kernel, capacity),
        [((slots * blocks, lanes), BF16)],
        [wide],
        8,
        out_specs=[FREE],
    )(*gathered(hidden), *downs)
    returned = lax.all_to_all(
        sent.reshape(ep, capacity * blocks, lanes), "ep", 0, 0, tiled=True
    ).reshape(slots * blocks, lanes)
    (new_tokens,) = call(
        functools.partial(final_kernel, capacity),
        [piece],
        [wide, pltpu.VMEM((slots, quarter), BF16)],
        8,
        out_specs=[FREE],
    )(returned, w, share0, share1, resid16, blend, *dense)
    return (new_tokens, new_re, new_im)


def solution(mesh):
    in_specs = (
        P("ep", None),
        P(),
        P(None, "tp"),
        P("ep", "tp"),
        P("ep", "tp"),
        P("tp", None),
        P("tp"),
        P("tp", None, None),
        P("tp", None, None),
        P("tp", None, None),
        P("tp", None, None),
        P("tp", None),
        P("tp", None),
        P(),
        P("ep", None),
        P("ep"),
        P("ep", None),
        P("ep", None, "tp"),
        P("ep", None, "tp"),
        P("ep", "tp", None),
        P(None, "tp"),
        P(None, "tp"),
        P("tp", None),
        P(),
    )
    out_specs = (P("ep", "tp"), P("ep", "tp"), P("ep", "tp"))

    return jax.shard_map(
        per_device, mesh=mesh, in_specs=in_specs, out_specs=out_specs, check_vma=False
    )
```

profile of v0, /device:TPU:1, one launch (start us, length us, event | category | flops | bytes accessed | tf_op | source)
XLA Modules:
  0.0 99.1 jit_solution(14983304392800222883)
XLA Ops:
  0.7 4.2 %shard_map.247 = (bf16[96,512]{1,0:T(8,128)(2,1)S(1)}, bf16[96,512]{1,0:T(8,128)(2,1)S(1)}, bf16[96,512]{1,0:T(8,128)(2,1)S(1)}, bf16[96,512]{1,0:T(8,128)(2,1)S...) custom-call(f32[16,64]{1,0:T(8,128)} %refs_0_.1, f32[16,16]{1,0:T(8,128)} %refs_1_.1, bf16[96,2048]{1,0:T(8,128)(2,1)} %tokens.1, ...), custom_call_target="tpu_custom_call" | custom-call | tf_op jit(solution)/shard_map/pallas_call | solution.py:337
  4.9 3.3 %collective-permute-start = (bf16[96,512]{1,0:T(8,128)(2,1)S(1)}, bf16[96,512]{1,0:T(8,128)(2,1)S(1)}, u32[]{:S(2)}, u32[]{:S(2)}) collective-permute-start(bf16[96,512]{1,0:T(8,128)(2,1)S(1)} %get-tuple-element.31), channel_id=1, source_target_pairs={{0,1},{1,0},{2,3},{3,2},{4,5},{5,4},{6,7},{7,6},{8,9},{9,8},{10,11... | collective-permute-start | bytes 294920 | tf_op jit(solution)/shard_map/ppermute | solution.py:42
  8.2 1.7 %collective-permute-start.2 = (bf16[96,512]{1,0:T(8,128)(2,1)S(1)}, bf16[96,512]{1,0:T(8,128)(2,1)S(1)}, u32[]{:S(2)}, u32[]{:S(2)}) collective-permute-start(bf16[96,512]{1,0:T(8,128)(2,1)S(1)} %get-tuple-element.33), channel_id=1, source_target_pairs={{0,3},{1,2},{2,1},{3,0},{4,7},{5,6},{6,5},{7,4},{8,11},{9,10},{10,... | collective-permute-start | bytes 294920 | tf_op jit(solution)/shard_map/ppermute | solution.py:42
  10.3 2.2 %collective-permute-done.1.p2 = bf16[96,512]{1,0:T(8,128)(2,1)S(1)} collective-permute-done((bf16[96,512]{1,0:T(8,128)(2,1)S(1)}, bf16[96,512]{1,0:T(8,128)(2,1)S(1)}, u32[]{:S(2)}, u32[]{:S(2)}) %collective-permute-start.1) | collective-permute-done | bytes 98336 | tf_op jit(solution)/shard_map/ppermute | solution.py:42
  12.5 2.4 %collective-permute-done.2.p3 = bf16[96,512]{1,0:T(8,128)(2,1)S(1)} collective-permute-done((bf16[96,512]{1,0:T(8,128)(2,1)S(1)}, bf16[96,512]{1,0:T(8,128)(2,1)S(1)}, u32[]{:S(2)}, u32[]{:S(2)}) %collective-permute-start.2) | collective-permute-done | bytes 98336 | tf_op jit(solution)/shard_map/ppermute | solution.py:42
  14.8 1.1 %shard_map.249 = (bf16[96,512]{1,0:T(8,128)(2,1)S(1)}, bf16[1536,128]{1,0:T(8,128)(2,1)}) custom-call(bf16[96,2048]{1,0:T(8,128)(2,1)S(1)} %copy-done, bf16[96,512]{1,0:T(8,128)(2,1)S(1)} %get-tuple-element.30.p0, bf16[96,512]{1,0:T(8,128)(2,1)S(1)} %collective-permute-done.p1, bf16[96,512]{1,0:T(8,128)(2,1)S(1)} %collective-permute-done.1.p2, ...), custom_call_target="tpu_custom_call" | custom-call | tf_op jit(solution)/shard_map/pallas_call | solution.py:337
  16.0 12.6 %all-to-all-start = ((bf16[64,24,128]{2,1,0:T(8,128)(2,1)}), bf16[64,24,128]{2,1,0:T(8,128)(2,1)S(1)}, u32[]{:S(2)}, u32[]{:S(2)}) async-start(bf16[64,24,128]{2,1,0:T(8,128)(2,1)} %bitcast.9), calls=%async_computation | async-start | bytes 786432 | tf_op jit(solution)/shard_map/all_to_all | solution.py:439
  29.6 1.4 %collective-permute-start.5 = (bf16[512,256]{1,0:T(8,128)(2,1)S(1)}, bf16[512,256]{1,0:T(8,128)(2,1)S(1)}, u32[]{:S(2)}, u32[]{:S(2)}) collective-permute-start(bf16[512,256]{1,0:T(8,128)(2,1)S(1)} %get-tuple-element.39), channel_id=1, source_target_pairs={{0,3},{1,2},{2,1},{3,0},{4,7},{5,6},{6,5},{7,4},{8,11},{9,10},{10,... | collective-permute-start | bytes 786440 | tf_op jit(solution)/shard_map/ppermute | solution.py:42
  31.1 9.7 %collective-permute-done.4.gu2 = bf16[512,256]{1,0:T(8,128)(2,1)S(1)} collective-permute-done((bf16[512,256]{1,0:T(8,128)(2,1)S(1)}, bf16[512,256]{1,0:T(8,128)(2,1)S(1)}, u32[]{:S(2)}, u32[]{:S(2)}) %collective-permute-start.4) | collective-permute-done | bytes 262176 | tf_op jit(solution)/shard_map/ppermute | solution.py:42
  40.8 5.8 %collective-permute-done.5.gu3 = bf16[512,256]{1,0:T(8,128)(2,1)S(1)} collective-permute-done((bf16[512,256]{1,0:T(8,128)(2,1)S(1)}, bf16[512,256]{1,0:T(8,128)(2,1)S(1)}, u32[]{:S(2)}, u32[]{:S(2)}) %collective-permute-start.5) | collective-permute-done | bytes 262176 | tf_op jit(solution)/shard_map/ppermute | solution.py:42
  47.9 1.4 %collective-permute-done.6.came = bf16[392,512]{1,0:T(8,128)(2,1)S(1)} collective-permute-done((bf16[392,512]{1,0:T(8,128)(2,1)S(1)}, bf16[392,512]{1,0:T(8,128)(2,1)S(1)}, u32[]{:S(2)}, u32[]{:S(2)}) %collective-permute-start.6) | collective-permute-done | bytes 401440 | tf_op jit(solution)/shard_map/ppermute | solution.py:42
  49.9 5.9 %collective-permute-done.7.last = bf16[400,256]{1,0:T(8,128)(2,1)S(1)} collective-permute-done((bf16[400,256]{1,0:T(8,128)(2,1)S(1)}, bf16[400,256]{1,0:T(8,128)(2,1)S(1)}, u32[]{:S(2)}, u32[]{:S(2)}) %collective-permute-start.7) | collective-permute-done | bytes 204832 | tf_op jit(solution)/shard_map/ppermute | solution.py:42
  56.7 1.3 %collective-permute-start.11 = (bf16[128,512]{1,0:T(8,128)(2,1)S(1)}, bf16[128,512]{1,0:T(8,128)(2,1)S(1)}, u32[]{:S(2)}, u32[]{:S(2)}) collective-permute-start(bf16[128,512]{1,0:T(8,128)(2,1)S(1)} %get-tuple-element.43), channel_id=1, source_target_pairs={{0,1},{1,0},{2,3},{3,2},{4,5},{5,4},{6,7},{7,6},{8,9},{9,8},{10,11... | collective-permute-start | bytes 393224 | tf_op jit(solution)/shard_map/ppermute | solution.py:42
  59.9 3.0 %collective-permute-start.10 = (bf16[384,128]{1,0:T(8,128)(2,1)S(1)}, bf16[384,128]{1,0:T(8,128)(2,1)S(1)}, u32[]{:S(2)}, u32[]{:S(2)}) collective-permute-start(bf16[384,128]{1,0:T(8,128)(2,1)S(1)} %collective-permute-done.9.h2), channel_id=1, source_target_pairs={{0,1},{1,0},{2,3},{3,2},{4,5},{5,4},{6,7},{7,6},{8,9},{9,8},{10,11... | collective-permute-start | bytes 294920 | tf_op jit(solution)/shard_map/ppermute | solution.py:42
  63.5 3.4 %collective-permute-done.13.d3 = bf16[128,512]{1,0:T(8,128)(2,1)S(1)} collective-permute-done((bf16[128,512]{1,0:T(8,128)(2,1)S(1)}, bf16[128,512]{1,0:T(8,128)(2,1)S(1)}, u32[]{:S(2)}, u32[]{:S(2)}) %collective-permute-start.13) | collective-permute-done | bytes 131104 | tf_op jit(solution)/shard_map/ppermute | solution.py:42
  66.9 1.4 %shard_map.254 = bf16[1536,128]{1,0:T(8,128)(2,1)} custom-call(bf16[384,128]{1,0:T(8,128)(2,1)S(1)} %shard_map.253.h0, bf16[384,128]{1,0:T(8,128)(2,1)S(1)} %collective-permute-done.8.h1, bf16[384,128]{1,0:T(8,128)(2,1)S(1)} %collective-permute-done.9.h2, bf16[384,128]{1,0:T(8,128)(2,1)S(1)} %collective-permute-done.10.h3, ...), custom_call_target="tpu_custom_call" | custom-call | tf_op jit(solution)/shard_map/pallas_call | solution.py:337
  68.3 11.8 %all-to-all-start.1 = ((bf16[64,24,128]{2,1,0:T(8,128)(2,1)}), bf16[64,24,128]{2,1,0:T(8,128)(2,1)S(1)}, u32[]{:S(2)}, u32[]{:S(2)}) async-start(bf16[64,24,128]{2,1,0:T(8,128)(2,1)} %bitcast.14), calls=%async_computation.1 | async-start | bytes 786432 | tf_op jit(solution)/shard_map/all_to_all | solution.py:473
  81.1 3.8 %collective-permute-done.15.a2 = bf16[96,512]{1,0:T(8,128)(2,1)S(1)} collective-permute-done((bf16[96,512]{1,0:T(8,128)(2,1)S(1)}, bf16[96,512]{1,0:T(8,128)(2,1)S(1)}, u32[]{:S(2)}, u32[]{:S(2)}) %collective-permute-start.15) | collective-permute-done | bytes 98336 | tf_op jit(solution)/shard_map/ppermute | solution.py:42
  84.9 1.6 %collective-permute-start.16 = (bf16[96,512]{1,0:T(8,128)(2,1)S(1)}, bf16[96,512]{1,0:T(8,128)(2,1)S(1)}, u32[]{:S(2)}, u32[]{:S(2)}) collective-permute-start(bf16[96,512]{1,0:T(8,128)(2,1)S(1)} %collective-permute-done.15.a2), channel_id=1, source_target_pairs={{0,1},{1,0},{2,3},{3,2},{4,5},{5,4},{6,7},{7,6},{8,9},{9,8},{10,11... | collective-permute-start | bytes 294920 | tf_op jit(solution)/shard_map/ppermute | solution.py:42
  87.5 3.4 %shard_map.255 = (bf16[96,512]{1,0:T(8,128)(2,1)S(1)}, bf16[96,512]{1,0:T(8,128)(2,1)S(1)}, bf16[96,512]{1,0:T(8,128)(2,1)S(1)}, bf16[96,512]{1,0:T(8,128)(2,1)S(1)}, f32[96,128]{1,0:T(8,128)S(1)}) custom-call(bf16[1,2048]{1,0:T(2,128)(2,1)S(1)} %reshape.55.gains, bf16[96,512]{1,0:T(8,128)(2,1)S(1)} %get-tuple-element.49.a0.resid, ...), custom_call_target="tpu_custom_call" | custom-call | tf_op jit(solution)/shard_map/pallas_call | solution.py:337
  91.7 1.5 %collective-permute-start.19 = (bf16[96,512]{1,0:T(8,128)(2,1)S(1)}, bf16[96,512]{1,0:T(8,128)(2,1)S(1)}, u32[]{:S(2)}, u32[]{:S(2)}) collective-permute-start(bf16[96,512]{1,0:T(8,128)(2,1)S(1)} %get-tuple-element.54), channel_id=1, source_target_pairs={{0,3},{1,2},{2,1},{3,0},{4,7},{5,6},{6,5},{7,4},{8,11},{9,10},{10,... | collective-permute-start | bytes 294920 | tf_op jit(solution)/shard_map/ppermute | solution.py:42
  93.2 2.4 %collective-permute-done.18.p2 = bf16[96,512]{1,0:T(8,128)(2,1)S(1)} collective-permute-done((bf16[96,512]{1,0:T(8,128)(2,1)S(1)}, bf16[96,512]{1,0:T(8,128)(2,1)S(1)}, u32[]{:S(2)}, u32[]{:S(2)}) %collective-permute-start.18) | collective-permute-done | bytes 98336 | tf_op jit(solution)/shard_map/ppermute | solution.py:42
  95.6 2.4 %collective-permute-done.19.p3 = bf16[96,512]{1,0:T(8,128)(2,1)S(1)} collective-permute-done((bf16[96,512]{1,0:T(8,128)(2,1)S(1)}, bf16[96,512]{1,0:T(8,128)(2,1)S(1)}, u32[]{:S(2)}, u32[]{:S(2)}) %collective-permute-start.19) | collective-permute-done | bytes 98336 | tf_op jit(solution)/shard_map/ppermute | solution.py:42
  98.0 1.1 %shard_map.256 = bf16[96,512]{1,0:T(8,128)(2,1)} custom-call(bf16[1536,128]{1,0:T(8,128)(2,1)S(1)} %bitcast.18, bf16[192,384]{1,0:T(8,128)(2,1)S(1)} %get-tuple-element.46.w, f32[96,128]{1,0:T(8,128)S(1)} %get-tuple-element.47.share0, f32[96,128]{1,0:T(8,128)S(1)} %get-tuple-element.48.share1, bf16[96,512]{1,0:T(8,128)(2,1)S(1)} %get-tuple-element.49.a0.resid, ...), custom_call_target="tpu_custom_call" | custom-call | tf_op jit(solution)/shard_map/pallas_call | solution.py:337
  (50 shorter events, 9.5 us)
Async XLA Ops:
  0.7 27.9 %copy-start.1 = (bf16[1,2048,128]{2,1,0:T(8,128)(2,1)S(1)}, bf16[1,2048,128]{2,1,0:T(8,128)(2,1)}, u32[]{:S(2)}) copy-start(bf16[1,2048,128]{2,1,0:T(8,128)(2,1)} %param.41) | copy-start | bytes 1572868
  4.9 5.4 %collective-permute-start = (bf16[96,512]{1,0:T(8,128)(2,1)S(1)}, bf16[96,512]{1,0:T(8,128)(2,1)S(1)}, u32[]{:S(2)}, u32[]{:S(2)}) collective-permute-start(bf16[96,512]{1,0:T(8,128)(2,1)S(1)} %get-tuple-element.31), channel_id=1, source_target_pairs={{0,1},{1,0},{2,3},{3,2},{4,5},{5,4},{6,7},{7,6},{8,9},{9,8},{10,11... | collective-permute-start | bytes 294920 | tf_op jit(solution)/shard_map/ppermute | solution.py:42
  8.2 4.2 %collective-permute-start.1 = (bf16[96,512]{1,0:T(8,128)(2,1)S(1)}, bf16[96,512]{1,0:T(8,128)(2,1)S(1)}, u32[]{:S(2)}, u32[]{:S(2)}) collective-permute-start(bf16[96,512]{1,0:T(8,128)(2,1)S(1)} %get-tuple-element.32), channel_id=1, source_target_pairs={{0,2},{1,3},{2,0},{3,1},{4,6},{5,7},{6,4},{7,5},{8,10},{9,11},{10,... | collective-permute-start | bytes 294920 | tf_op jit(solution)/shard_map/ppermute | solution.py:42
  8.2 6.6 %collective-permute-start.2 = (bf16[96,512]{1,0:T(8,128)(2,1)S(1)}, bf16[96,512]{1,0:T(8,128)(2,1)S(1)}, u32[]{:S(2)}, u32[]{:S(2)}) collective-permute-start(bf16[96,512]{1,0:T(8,128)(2,1)S(1)} %get-tuple-element.33), channel_id=1, source_target_pairs={{0,3},{1,2},{2,1},{3,0},{4,7},{5,6},{6,5},{7,4},{8,11},{9,10},{10,... | collective-permute-start | bytes 294920 | tf_op jit(solution)/shard_map/ppermute | solution.py:42
  16.0 30.6 %all-to-all-start = ((bf16[64,24,128]{2,1,0:T(8,128)(2,1)}), bf16[64,24,128]{2,1,0:T(8,128)(2,1)S(1)}, u32[]{:S(2)}, u32[]{:S(2)}) async-start(bf16[64,24,128]{2,1,0:T(8,128)(2,1)} %bitcast.9), calls=%async_computation | async-start | bytes 786432 | tf_op jit(solution)/shard_map/all_to_all | solution.py:439
  28.8 2.2 %collective-permute-start.3 = (bf16[512,256]{1,0:T(8,128)(2,1)S(1)}, bf16[512,256]{1,0:T(8,128)(2,1)S(1)}, u32[]{:S(2)}, u32[]{:S(2)}) collective-permute-start(bf16[512,256]{1,0:T(8,128)(2,1)S(1)} %get-tuple-element.37), channel_id=1, source_target_pairs={{0,1},{1,0},{2,3},{3,2},{4,5},{5,4},{6,7},{7,6},{8,9},{9,8},{10,11... | collective-permute-start | bytes 786440 | tf_op jit(solution)/shard_map/ppermute | solution.py:42
  29.3 11.4 %collective-permute-start.4 = (bf16[512,256]{1,0:T(8,128)(2,1)S(1)}, bf16[512,256]{1,0:T(8,128)(2,1)S(1)}, u32[]{:S(2)}, u32[]{:S(2)}) collective-permute-start(bf16[512,256]{1,0:T(8,128)(2,1)S(1)} %get-tuple-element.38), channel_id=1, source_target_pairs={{0,2},{1,3},{2,0},{3,1},{4,6},{5,7},{6,4},{7,5},{8,10},{9,11},{10,... | collective-permute-start | bytes 786440 | tf_op jit(solution)/shard_map/ppermute | solution.py:42
  29.6 16.9 %collective-permute-start.5 = (bf16[512,256]{1,0:T(8,128)(2,1)S(1)}, bf16[512,256]{1,0:T(8,128)(2,1)S(1)}, u32[]{:S(2)}, u32[]{:S(2)}) collective-permute-start(bf16[512,256]{1,0:T(8,128)(2,1)S(1)} %get-tuple-element.39), channel_id=1, source_target_pairs={{0,3},{1,2},{2,1},{3,0},{4,7},{5,6},{6,5},{7,4},{8,11},{9,10},{10,... | collective-permute-start | bytes 786440 | tf_op jit(solution)/shard_map/ppermute | solution.py:42
  47.5 1.8 %collective-permute-start.6 = (bf16[392,512]{1,0:T(8,128)(2,1)S(1)}, bf16[392,512]{1,0:T(8,128)(2,1)S(1)}, u32[]{:S(2)}, u32[]{:S(2)}) collective-permute-start(bf16[392,512]{1,0:T(8,128)(2,1)S(1)} %get-tuple-element.41), channel_id=1, source_target_pairs={{0,1},{1,0},{2,3},{3,2},{4,5},{5,4},{6,7},{7,6},{8,9},{9,8},{10,11... | collective-permute-start | bytes 1204232 | tf_op jit(solution)/shard_map/ppermute | solution.py:42
  49.4 37.2 %copy-start.8 = (bf16[2048]{0:T(1024)(128)(2,1)S(1)}, bf16[2048]{0:T(1024)(128)(2,1)}, u32[]{:S(2)}) copy-start(bf16[2048]{0:T(1024)(128)(2,1)} %param.47) | copy-start | bytes 12292
  49.4 6.4 %collective-permute-start.7 = (bf16[400,256]{1,0:T(8,128)(2,1)S(1)}, bf16[400,256]{1,0:T(8,128)(2,1)S(1)}, u32[]{:S(2)}, u32[]{:S(2)}) collective-permute-start(bf16[400,256]{1,0:T(8,128)(2,1)S(1)} %shard_map.252), channel_id=1, source_target_pairs={{0,2},{1,3},{2,0},{3,1},{4,6},{5,7},{6,4},{7,5},{8,10},{9,11},{10,... | collective-permute-start | bytes 614408 | tf_op jit(solution)/shard_map/ppermute | solution.py:42
  56.1 3.8 %collective-permute-start.9 = (bf16[384,128]{1,0:T(8,128)(2,1)S(1)}, bf16[384,128]{1,0:T(8,128)(2,1)S(1)}, u32[]{:S(2)}, u32[]{:S(2)}) collective-permute-start(bf16[384,128]{1,0:T(8,128)(2,1)S(1)} %shard_map.253.h0), channel_id=1, source_target_pairs={{0,2},{1,3},{2,0},{3,1},{4,6},{5,7},{6,4},{7,5},{8,10},{9,11},{10,... | collective-permute-start | bytes 294920 | tf_op jit(solution)/shard_map/ppermute | solution.py:42
  56.7 6.1 %collective-permute-start.11 = (bf16[128,512]{1,0:T(8,128)(2,1)S(1)}, bf16[128,512]{1,0:T(8,128)(2,1)S(1)}, u32[]{:S(2)}, u32[]{:S(2)}) collective-permute-start(bf16[128,512]{1,0:T(8,128)(2,1)S(1)} %get-tuple-element.43), channel_id=1, source_target_pairs={{0,1},{1,0},{2,3},{3,2},{4,5},{5,4},{6,7},{7,6},{8,9},{9,8},{10,11... | collective-permute-start | bytes 393224 | tf_op jit(solution)/shard_map/ppermute | solution.py:42
  58.0 5.5 %collective-permute-start.12 = (bf16[128,512]{1,0:T(8,128)(2,1)S(1)}, bf16[128,512]{1,0:T(8,128)(2,1)S(1)}, u32[]{:S(2)}, u32[]{:S(2)}) collective-permute-start(bf16[128,512]{1,0:T(8,128)(2,1)S(1)} %get-tuple-element.44), channel_id=1, source_target_pairs={{0,2},{1,3},{2,0},{3,1},{4,6},{5,7},{6,4},{7,5},{8,10},{9,11},{10,... | collective-permute-start | bytes 393224 | tf_op jit(solution)/shard_map/ppermute | solution.py:42
  59.1 7.8 %collective-permute-start.13 = (bf16[128,512]{1,0:T(8,128)(2,1)S(1)}, bf16[128,512]{1,0:T(8,128)(2,1)S(1)}, u32[]{:S(2)}, u32[]{:S(2)}) collective-permute-start(bf16[128,512]{1,0:T(8,128)(2,1)S(1)} %get-tuple-element.45), channel_id=1, source_target_pairs={{0,3},{1,2},{2,1},{3,0},{4,7},{5,6},{6,5},{7,4},{8,11},{9,10},{10,... | collective-permute-start | bytes 393224 | tf_op jit(solution)/shard_map/ppermute | solution.py:42
  59.7 7.3 %collective-permute-start.8 = (bf16[384,128]{1,0:T(8,128)(2,1)S(1)}, bf16[384,128]{1,0:T(8,128)(2,1)S(1)}, u32[]{:S(2)}, u32[]{:S(2)}) collective-permute-start(bf16[384,128]{1,0:T(8,128)(2,1)S(1)} %shard_map.253.h0), channel_id=1, source_target_pairs={{0,1},{1,0},{2,3},{3,2},{4,5},{5,4},{6,7},{7,6},{8,9},{9,8},{10,11... | collective-permute-start | bytes 294920 | tf_op jit(solution)/shard_map/ppermute | solution.py:42
  59.9 7.0 %collective-permute-start.10 = (bf16[384,128]{1,0:T(8,128)(2,1)S(1)}, bf16[384,128]{1,0:T(8,128)(2,1)S(1)}, u32[]{:S(2)}, u32[]{:S(2)}) collective-permute-start(bf16[384,128]{1,0:T(8,128)(2,1)S(1)} %collective-permute-done.9.h2), channel_id=1, source_target_pairs={{0,1},{1,0},{2,3},{3,2},{4,5},{5,4},{6,7},{7,6},{8,9},{9,8},{10,11... | collective-permute-start | bytes 294920 | tf_op jit(solution)/shard_map/ppermute | solution.py:42
  68.3 29.7 %all-to-all-start.1 = ((bf16[64,24,128]{2,1,0:T(8,128)(2,1)}), bf16[64,24,128]{2,1,0:T(8,128)(2,1)S(1)}, u32[]{:S(2)}, u32[]{:S(2)}) async-start(bf16[64,24,128]{2,1,0:T(8,128)(2,1)} %bitcast.14), calls=%async_computation.1 | async-start | bytes 786432 | tf_op jit(solution)/shard_map/all_to_all | solution.py:473
  80.2 4.8 %collective-permute-start.15 = (bf16[96,512]{1,0:T(8,128)(2,1)S(1)}, bf16[96,512]{1,0:T(8,128)(2,1)S(1)}, u32[]{:S(2)}, u32[]{:S(2)}) collective-permute-start(bf16[96,512]{1,0:T(8,128)(2,1)S(1)} %get-tuple-element.49.a0.resid), channel_id=1, source_target_pairs={{0,2},{1,3},{2,0},{3,1},{4,6},{5,7},{6,4},{7,5},{8,10},{9,11},{10,... | collective-permute-start | bytes 294920 | tf_op jit(solution)/shard_map/ppermute | solution.py:42
  80.5 6.1 %collective-permute-start.14 = (bf16[96,512]{1,0:T(8,128)(2,1)S(1)}, bf16[96,512]{1,0:T(8,128)(2,1)S(1)}, u32[]{:S(2)}, u32[]{:S(2)}) collective-permute-start(bf16[96,512]{1,0:T(8,128)(2,1)S(1)} %get-tuple-element.49.a0.resid), channel_id=1, source_target_pairs={{0,1},{1,0},{2,3},{3,2},{4,5},{5,4},{6,7},{7,6},{8,9},{9,8},{10,11... | collective-permute-start | bytes 294920 | tf_op jit(solution)/shard_map/ppermute | solution.py:42
  84.9 2.6 %collective-permute-start.16 = (bf16[96,512]{1,0:T(8,128)(2,1)S(1)}, bf16[96,512]{1,0:T(8,128)(2,1)S(1)}, u32[]{:S(2)}, u32[]{:S(2)}) collective-permute-start(bf16[96,512]{1,0:T(8,128)(2,1)S(1)} %collective-permute-done.15.a2), channel_id=1, source_target_pairs={{0,1},{1,0},{2,3},{3,2},{4,5},{5,4},{6,7},{7,6},{8,9},{9,8},{10,11... | collective-permute-start | bytes 294920 | tf_op jit(solution)/shard_map/ppermute | solution.py:42
  90.9 2.2 %collective-permute-start.17 = (bf16[96,512]{1,0:T(8,128)(2,1)S(1)}, bf16[96,512]{1,0:T(8,128)(2,1)S(1)}, u32[]{:S(2)}, u32[]{:S(2)}) collective-permute-start(bf16[96,512]{1,0:T(8,128)(2,1)S(1)} %get-tuple-element.52), channel_id=1, source_target_pairs={{0,1},{1,0},{2,3},{3,2},{4,5},{5,4},{6,7},{7,6},{8,9},{9,8},{10,11... | collective-permute-start | bytes 294920 | tf_op jit(solution)/shard_map/ppermute | solution.py:42
  91.4 4.2 %collective-permute-start.18 = (bf16[96,512]{1,0:T(8,128)(2,1)S(1)}, bf16[96,512]{1,0:T(8,128)(2,1)S(1)}, u32[]{:S(2)}, u32[]{:S(2)}) collective-permute-start(bf16[96,512]{1,0:T(8,128)(2,1)S(1)} %get-tuple-element.53), channel_id=1, source_target_pairs={{0,2},{1,3},{2,0},{3,1},{4,6},{5,7},{6,4},{7,5},{8,10},{9,11},{10,... | collective-permute-start | bytes 294920 | tf_op jit(solution)/shard_map/ppermute | solution.py:42
  91.7 6.3 %collective-permute-start.19 = (bf16[96,512]{1,0:T(8,128)(2,1)S(1)}, bf16[96,512]{1,0:T(8,128)(2,1)S(1)}, u32[]{:S(2)}, u32[]{:S(2)}) collective-permute-start(bf16[96,512]{1,0:T(8,128)(2,1)S(1)} %get-tuple-element.54), channel_id=1, source_target_pairs={{0,3},{1,2},{2,1},{3,0},{4,7},{5,6},{6,5},{7,4},{8,11},{9,10},{10,... | collective-permute-start | bytes 294920 | tf_op jit(solution)/shard_map/ppermute | solution.py:42
  (7 other events, 124.0 us)
where the time goes:
time: 99.4 us; the launch traced here: 99.1 us
  starting transfers between devices  44.2 us (44%)
  waiting for transfers between devices  40.9 us (41%)
  Pallas kernels  13.1 us (13%)
    ppermute x20, waiting for transfers between devices, exchanged(): return lax.ppermute(value, 'tp', [(i, i ^ mask) for i in range(4)])  40.9 us
    ppermute x20, starting transfers between devices, exchanged(): return lax.ppermute(value, 'tp', [(i, i ^ mask) for i in range(4)])  19.7 us
    pallas_call x10, Pallas kernels, run(): pl.pallas_call(kernel, out_shape=tuple(out_shape), in_specs=specs, out_sp...  13.1 us
    all_to_all x1, starting transfers between devices, per_device(): lax.all_to_all(packed.reshape(ep, capacity * blocks, lanes), 'ep', 0, 0,...  12.6 us
    all_to_all x1, starting transfers between devices, per_device(): lax.all_to_all(sent.reshape(ep, capacity * blocks, lanes), 'ep', 0, 0, ti...  11.8 us
  transfers between devices with their start and end apart: 22, of which 12 were waited for; matrix products, arithmetic and copies ran while one was open for 0% of the time, Pallas kernels for 4%

commit v1 on v0

--- a/solution.py
+++ b/solution.py
@@ -137,11 +137,14 @@
 def reshard_kernel(gate, up, down, *pieces):
     t = lax.axis_index("tp")
     hid = gate.shape[1]
-    for m, (gu, d) in enumerate(zip(pieces[:4], pieces[4:])):
-        part = cols_of(t ^ m, gu.shape[0])
-        gu[:, 0:hid] = gate[part, :]
-        gu[:, hid:] = up[part, :]
-        d[...] = down[:, cols_of(t ^ m, d.shape[1])]
+    for m, piece in enumerate(pieces):
+        rows = piece.shape[0] - 2 * hid
+        part = cols_of(t ^ m, rows)
+        piece[0:rows, 0:hid] = gate[part, :]
+        piece[0:rows, hid:] = up[part, :]
+        for half in range(2):
+            low = rows + half * hid
+            piece[low : low + hid, :] = down[:, cols_of(2 * (t ^ m) + half, 2 * hid)]
 
 
 def route_kernel(experts, routes, group_weight, logits, z, w, share0, share1, padded):
@@ -244,7 +247,7 @@
         p[...] = dot(hidden, down_v[:, cols_of(t ^ m, quarter)]).astype(BF16)
 
 
-def enter_kernel(capacity, arrived, gains, gu0, gu1, gu2, gu3, keep, send, wide, rows, sums):
+def enter_kernel(capacity, arrived, gains, w0, w1, w2, w3, keep, send, wide, rows, sums):
     t = lax.axis_index("tp")
     lanes = arrived.shape[1]
     quarter = rows.shape[1]
@@ -262,11 +265,11 @@
     )
     send[count:, :] = three_terms(squares, send.shape[1])
     x = rows[...]
-    pair = gu0.shape[1]
-    keep[0:count, 0:pair] = dot(x, gu0[...])
-    send[0:count, 0:pair] = dot(x, gu1[...]).astype(BF16)
-    keep[0:count, pair:] = dot(x, gu2[...])
-    send[0:count, pair:] = dot(x, gu3[...]).astype(BF16)
+    pair = w0.shape[1]
+    keep[0:count, 0:pair] = dot(x, w0[0:quarter, :])
+    send[0:count, 0:pair] = dot(x, w1[0:quarter, :]).astype(BF16)
+    keep[0:count, pair:] = dot(x, w2[0:quarter, :])
+    send[0:count, pair:] = dot(x, w3[0:quarter, :]).astype(BF16)
 
 
 def relay_kernel(keep, came, onward):
@@ -293,10 +296,15 @@
     hidden[...] = (jax.nn.silu(total[:, 0:units] * scale) * (total[:, units:] * scale)).astype(BF16)
 
 
-def leave_kernel(capacity, h0, h1, h2, h3, d0, d1, d2, d3, out, wide):
-    total = dot(h0[...], d0[...])
-    for h, d in ((h1, d1), (h2, d2), (h3, d3)):
-        total = total + dot(h[...], d[...])
+def leave_kernel(capacity, h0, h1, h2, h3, w0, w1, w2, w3, out, wide, total):
+    units = h0.shape[1]
+    skip = w0.shape[0] - 2 * units
+    size = w0.shape[1]
+    for half in range(2):
+        near = slice(skip + half * units, skip + (half + 1) * units)
+        total[:, half * size : (half + 1) * size] = (
+            dot(h0[...], w0[near, :]) + dot(h1[...], w1[near, :])
+        ) + (dot(h2[...], w2[near, :]) + dot(h3[...], w3[near, :]))
     for strided, near, cols in places(capacity, wide, total.shape[1]):
         wide[strided, :] = total[near, cols]
     out[...] = wide[...].astype(BF16)
@@ -418,11 +426,11 @@
         [VMEM] * 4 + [HBM] * 2,
     )(*state_inputs)
     mix = [mix[0]] + [exchanged(mix[m], m) for m in (1, 2, 3)]
-    pieces = call(
-        reshard_kernel, [((quarter, 2 * hid), BF16)] * 4 + [((hid, quarter), BF16)] * 4
-    )(gate, up, down)
-    moved = [pieces[0]] + [exchanged(pieces[m], m) for m in (1, 2, 3)]
-    downs = [pieces[4]] + [exchanged(pieces[4 + m], m) for m in (1, 2, 3)]
+    pieces = call(reshard_kernel, [((quarter + 2 * hid, 2 * hid), BF16)] * 4)(gate, up, down)
+    piece2 = exchanged(pieces[2], 2)
+    piece3 = exchanged(pieces[3], 3)
+    piece1 = exchanged(pieces[1], 1)
+    moved = [pieces[0], piece1, piece2, piece3]
     z, w, share0, share1 = call(
         functools.partial(route_kernel, ep),
         [((slots, lanes), BF16), ((2 * rows, slots), BF16)] + [((rows, lanes), F32)] * 2,
@@ -436,10 +444,11 @@
         8,
         out_specs=[VMEM, FREE],
     )(tokens, *mix, z)
+    across, beside = exchanged(resid16, 2), exchanged(resid16, 1)
     arrived = lax.all_to_all(
         packed.reshape(ep, capacity * blocks, lanes), "ep", 0, 0, tiled=True
     ).reshape(slots * blocks, lanes)
-    near = gathered(resid16)
+    near = [resid16, beside, across, exchanged(across, 1)]
     gains = ffn_gain.reshape(1, width)
     *dense, blend = call(
         dense_kernel,
@@ -463,13 +472,14 @@
     (hidden,) = call(
         functools.partial(hidden_kernel, float(width)), [((slots, hid), BF16)]
     )(keep, came, last)
+    hidden = gathered(hidden)
     (sent,) = call(
         functools.partial(leave_kernel, capacity),
         [((slots * blocks, lanes), BF16)],
-        [wide],
+        [wide, pltpu.VMEM((slots, quarter), F32)],
         8,
         out_specs=[FREE],
-    )(*gathered(hidden), *downs)
+    )(*hidden, *moved)
     returned = lax.all_to_all(
         sent.reshape(ep, capacity * blocks, lanes), "ep", 0, 0, tiled=True
     ).reshape(slots * blocks, lanes)

time: 99.4 us -> 101 us (1.016)
  waiting for transfers between devices: 40.9 us -> 44.7 us
  starting transfers between devices: 44.2 us -> 42.3 us
    ppermute x20 -> x17, waiting for transfers between devices: 40.9 us -> 44.7 us  [exchanged(): return lax.ppermute(value, 'tp', [(i, i ^ mask) for i in range(4)])]
    ppermute x20 -> x17, starting transfers between devices: 19.7 us -> 17.7 us  [exchanged(): return lax.ppermute(value, 'tp', [(i, i ^ mask) for i in range(4)])]
  transfers between devices with their start and end apart: 22 -> 19, of which waited for: 12 -> 12; matrix products, arithmetic and copies ran while one was open for 0% -> 0% of each run, Pallas kernels for 4% -> 4%
where the time goes in v1:
time: 101 us
  waiting for transfers between devices  44.7 us (44%)
  starting transfers between devices  42.3 us (42%)
  Pallas kernels  13.1 us (13%)
    ppermute x17, waiting for transfers between devices, exchanged(): return lax.ppermute(value, 'tp', [(i, i ^ mask) for i in range(4)])  44.7 us
    ppermute x17, starting transfers between devices, exchanged(): return lax.ppermute(value, 'tp', [(i, i ^ mask) for i in range(4)])  17.7 us
    pallas_call x10, Pallas kernels, run(): pl.pallas_call(kernel, out_shape=tuple(out_shape), in_specs=specs, out_sp...  13.1 us
    all_to_all x1, starting transfers between devices, per_device(): lax.all_to_all(packed.reshape(ep, capacity * blocks, lanes), 'ep', 0, 0,...  12.6 us
    all_to_all x1, starting transfers between devices, per_device(): lax.all_to_all(sent.reshape(ep, capacity * blocks, lanes), 'ep', 0, 0, ti...  12 us
  transfers between devices with their start and end apart: 19, of which 12 were waited for; matrix products, arithmetic and copies ran while one was open for 0% of the time, Pallas kernels for 4%

profile of v1, /device:TPU:1, one launch (start us, length us, event | category | flops | bytes accessed | tf_op | source)
XLA Modules:
  0.0 101.0 jit_solution(17794908517134147179)
XLA Ops:
  0.7 4.2 %shard_map.247 = (bf16[96,512]{1,0:T(8,128)(2,1)S(1)}, bf16[96,512]{1,0:T(8,128)(2,1)S(1)}, bf16[96,512]{1,0:T(8,128)(2,1)S(1)}, bf16[96,512]{1,0:T(8,128)(2,1)S...) custom-call(f32[16,64]{1,0:T(8,128)} %refs_0_.1, f32[16,16]{1,0:T(8,128)} %refs_1_.1, bf16[96,2048]{1,0:T(8,128)(2,1)} %tokens.1, ...), custom_call_target="tpu_custom_call" | custom-call | tf_op jit(solution)/shard_map/pallas_call | solution.py:345
  4.9 3.3 %collective-permute-start = (bf16[96,512]{1,0:T(8,128)(2,1)S(1)}, bf16[96,512]{1,0:T(8,128)(2,1)S(1)}, u32[]{:S(2)}, u32[]{:S(2)}) collective-permute-start(bf16[96,512]{1,0:T(8,128)(2,1)S(1)} %get-tuple-element.27), channel_id=1, source_target_pairs={{0,1},{1,0},{2,3},{3,2},{4,5},{5,4},{6,7},{7,6},{8,9},{9,8},{10,11... | collective-permute-start | bytes 294920 | tf_op jit(solution)/shard_map/ppermute | solution.py:42
  8.2 1.7 %collective-permute-start.2 = (bf16[96,512]{1,0:T(8,128)(2,1)S(1)}, bf16[96,512]{1,0:T(8,128)(2,1)S(1)}, u32[]{:S(2)}, u32[]{:S(2)}) collective-permute-start(bf16[96,512]{1,0:T(8,128)(2,1)S(1)} %get-tuple-element.29), channel_id=1, source_target_pairs={{0,3},{1,2},{2,1},{3,0},{4,7},{5,6},{6,5},{7,4},{8,11},{9,10},{10,... | collective-permute-start | bytes 294920 | tf_op jit(solution)/shard_map/ppermute | solution.py:42
  10.3 2.2 %collective-permute-done.1.p2 = bf16[96,512]{1,0:T(8,128)(2,1)S(1)} collective-permute-done((bf16[96,512]{1,0:T(8,128)(2,1)S(1)}, bf16[96,512]{1,0:T(8,128)(2,1)S(1)}, u32[]{:S(2)}, u32[]{:S(2)}) %collective-permute-start.1) | collective-permute-done | bytes 98336 | tf_op jit(solution)/shard_map/ppermute | solution.py:42
  12.5 2.4 %collective-permute-done.2.p3 = bf16[96,512]{1,0:T(8,128)(2,1)S(1)} collective-permute-done((bf16[96,512]{1,0:T(8,128)(2,1)S(1)}, bf16[96,512]{1,0:T(8,128)(2,1)S(1)}, u32[]{:S(2)}, u32[]{:S(2)}) %collective-permute-start.2) | collective-permute-done | bytes 98336 | tf_op jit(solution)/shard_map/ppermute | solution.py:42
  14.8 1.1 %shard_map.249 = (bf16[96,512]{1,0:T(8,128)(2,1)S(1)}, bf16[1536,128]{1,0:T(8,128)(2,1)}) custom-call(bf16[96,2048]{1,0:T(8,128)(2,1)S(1)} %copy-done, bf16[96,512]{1,0:T(8,128)(2,1)S(1)} %get-tuple-element.26.p0, bf16[96,512]{1,0:T(8,128)(2,1)S(1)} %collective-permute-done.p1, bf16[96,512]{1,0:T(8,128)(2,1)S(1)} %collective-permute-done.1.p2, ...), custom_call_target="tpu_custom_call" | custom-call | tf_op jit(solution)/shard_map/pallas_call | solution.py:345
  15.9 12.6 %all-to-all-start = ((bf16[64,24,128]{2,1,0:T(8,128)(2,1)}), bf16[64,24,128]{2,1,0:T(8,128)(2,1)S(1)}, u32[]{:S(2)}, u32[]{:S(2)}) async-start(bf16[64,24,128]{2,1,0:T(8,128)(2,1)} %bitcast.9), calls=%async_computation | async-start | bytes 786432 | tf_op jit(solution)/shard_map/all_to_all | solution.py:448
  29.6 1.4 %collective-permute-start.5 = (bf16[768,256]{1,0:T(8,128)(2,1)S(1)}, bf16[768,256]{1,0:T(8,128)(2,1)S(1)}, u32[]{:S(2)}, u32[]{:S(2)}) collective-permute-start(bf16[768,256]{1,0:T(8,128)(2,1)S(1)} %get-tuple-element.35), channel_id=1, source_target_pairs={{0,3},{1,2},{2,1},{3,0},{4,7},{5,6},{6,5},{7,4},{8,11},{9,10},{10,... | collective-permute-start | bytes 1179656 | tf_op jit(solution)/shard_map/ppermute | solution.py:42
  31.1 12.6 %collective-permute-done.4.w2 = bf16[768,256]{1,0:T(8,128)(2,1)S(1)} collective-permute-done((bf16[768,256]{1,0:T(8,128)(2,1)S(1)}, bf16[768,256]{1,0:T(8,128)(2,1)S(1)}, u32[]{:S(2)}, u32[]{:S(2)}) %collective-permute-start.4) | collective-permute-done | bytes 393248 | tf_op jit(solution)/shard_map/ppermute | solution.py:42
  43.7 8.5 %collective-permute-done.5.w3 = bf16[768,256]{1,0:T(8,128)(2,1)S(1)} collective-permute-done((bf16[768,256]{1,0:T(8,128)(2,1)S(1)}, bf16[768,256]{1,0:T(8,128)(2,1)S(1)}, u32[]{:S(2)}, u32[]{:S(2)}) %collective-permute-start.5) | collective-permute-done | bytes 393248 | tf_op jit(solution)/shard_map/ppermute | solution.py:42
  53.5 1.4 %collective-permute-done.6.came = bf16[392,512]{1,0:T(8,128)(2,1)S(1)} collective-permute-done((bf16[392,512]{1,0:T(8,128)(2,1)S(1)}, bf16[392,512]{1,0:T(8,128)(2,1)S(1)}, u32[]{:S(2)}, u32[]{:S(2)}) %collective-permute-start.6) | collective-permute-done | bytes 401440 | tf_op jit(solution)/shard_map/ppermute | solution.py:42
  55.5 5.9 %collective-permute-done.7.last = bf16[400,256]{1,0:T(8,128)(2,1)S(1)} collective-permute-done((bf16[400,256]{1,0:T(8,128)(2,1)S(1)}, bf16[400,256]{1,0:T(8,128)(2,1)S(1)}, u32[]{:S(2)}, u32[]{:S(2)}) %collective-permute-start.7) | collective-permute-done | bytes 204832 | tf_op jit(solution)/shard_map/ppermute | solution.py:42
  62.3 1.3 %collective-permute-start.8 = (bf16[384,128]{1,0:T(8,128)(2,1)S(1)}, bf16[384,128]{1,0:T(8,128)(2,1)S(1)}, u32[]{:S(2)}, u32[]{:S(2)}) collective-permute-start(bf16[384,128]{1,0:T(8,128)(2,1)S(1)} %shard_map.253.h0), channel_id=1, source_target_pairs={{0,1},{1,0},{2,3},{3,2},{4,5},{5,4},{6,7},{7,6},{8,9},{9,8},{10,11... | collective-permute-start | bytes 294920 | tf_op jit(solution)/shard_map/ppermute | solution.py:42
  63.6 1.6 %collective-permute-done.9.h2 = bf16[384,128]{1,0:T(8,128)(2,1)S(1)} collective-permute-done((bf16[384,128]{1,0:T(8,128)(2,1)S(1)}, bf16[384,128]{1,0:T(8,128)(2,1)S(1)}, u32[]{:S(2)}, u32[]{:S(2)}) %collective-permute-start.9) | collective-permute-done | bytes 98336 | tf_op jit(solution)/shard_map/ppermute | solution.py:42
  65.2 2.4 %collective-permute-start.10 = (bf16[384,128]{1,0:T(8,128)(2,1)S(1)}, bf16[384,128]{1,0:T(8,128)(2,1)S(1)}, u32[]{:S(2)}, u32[]{:S(2)}) collective-permute-start(bf16[384,128]{1,0:T(8,128)(2,1)S(1)} %collective-permute-done.9.h2), channel_id=1, source_target_pairs={{0,1},{1,0},{2,3},{3,2},{4,5},{5,4},{6,7},{7,6},{8,9},{9,8},{10,11... | collective-permute-start | bytes 294920 | tf_op jit(solution)/shard_map/ppermute | solution.py:42
  68.6 1.4 %shard_map.254 = bf16[1536,128]{1,0:T(8,128)(2,1)} custom-call(bf16[384,128]{1,0:T(8,128)(2,1)S(1)} %shard_map.253.h0, bf16[384,128]{1,0:T(8,128)(2,1)S(1)} %collective-permute-done.8.h1, bf16[384,128]{1,0:T(8,128)(2,1)S(1)} %collective-permute-done.9.h2, bf16[384,128]{1,0:T(8,128)(2,1)S(1)} %collective-permute-done.10.h3, ...), custom_call_target="tpu_custom_call" | custom-call | tf_op jit(solution)/shard_map/pallas_call | solution.py:345
  69.9 12.0 %all-to-all-start.1 = ((bf16[64,24,128]{2,1,0:T(8,128)(2,1)}), bf16[64,24,128]{2,1,0:T(8,128)(2,1)S(1)}, u32[]{:S(2)}, u32[]{:S(2)}) async-start(bf16[64,24,128]{2,1,0:T(8,128)(2,1)} %bitcast.14), calls=%async_computation.1 | async-start | bytes 786432 | tf_op jit(solution)/shard_map/all_to_all | solution.py:483
  83.1 3.5 %collective-permute-done.12.a2 = bf16[96,512]{1,0:T(8,128)(2,1)S(1)} collective-permute-done((bf16[96,512]{1,0:T(8,128)(2,1)S(1)}, bf16[96,512]{1,0:T(8,128)(2,1)S(1)}, u32[]{:S(2)}, u32[]{:S(2)}) %collective-permute-start.12) | collective-permute-done | bytes 98336 | tf_op jit(solution)/shard_map/ppermute | solution.py:42
  86.7 1.8 %collective-permute-start.13 = (bf16[96,512]{1,0:T(8,128)(2,1)S(1)}, bf16[96,512]{1,0:T(8,128)(2,1)S(1)}, u32[]{:S(2)}, u32[]{:S(2)}) collective-permute-start(bf16[96,512]{1,0:T(8,128)(2,1)S(1)} %collective-permute-done.12.a2), channel_id=1, source_target_pairs={{0,1},{1,0},{2,3},{3,2},{4,5},{5,4},{6,7},{7,6},{8,9},{9,8},{10,11... | collective-permute-start | bytes 294920 | tf_op jit(solution)/shard_map/ppermute | solution.py:42
  89.4 3.4 %shard_map.255 = (bf16[96,512]{1,0:T(8,128)(2,1)S(1)}, bf16[96,512]{1,0:T(8,128)(2,1)S(1)}, bf16[96,512]{1,0:T(8,128)(2,1)S(1)}, bf16[96,512]{1,0:T(8,128)(2,1)S(1)}, f32[96,128]{1,0:T(8,128)S(1)}) custom-call(bf16[1,2048]{1,0:T(2,128)(2,1)S(1)} %reshape.55.gains, bf16[96,512]{1,0:T(8,128)(2,1)S(1)} %get-tuple-element.41.a0.resid, ...), custom_call_target="tpu_custom_call" | custom-call | tf_op jit(solution)/shard_map/pallas_call | solution.py:345
  93.3 1.7 %collective-permute-start.16 = (bf16[96,512]{1,0:T(8,128)(2,1)S(1)}, bf16[96,512]{1,0:T(8,128)(2,1)S(1)}, u32[]{:S(2)}, u32[]{:S(2)}) collective-permute-start(bf16[96,512]{1,0:T(8,128)(2,1)S(1)} %get-tuple-element.46), channel_id=1, source_target_pairs={{0,3},{1,2},{2,1},{3,0},{4,7},{5,6},{6,5},{7,4},{8,11},{9,10},{10,... | collective-permute-start | bytes 294920 | tf_op jit(solution)/shard_map/ppermute | solution.py:42
  95.0 2.4 %collective-permute-done.15.p2 = bf16[96,512]{1,0:T(8,128)(2,1)S(1)} collective-permute-done((bf16[96,512]{1,0:T(8,128)(2,1)S(1)}, bf16[96,512]{1,0:T(8,128)(2,1)S(1)}, u32[]{:S(2)}, u32[]{:S(2)}) %collective-permute-start.15) | collective-permute-done | bytes 98336 | tf_op jit(solution)/shard_map/ppermute | solution.py:42
  97.5 2.4 %collective-permute-done.16.p3 = bf16[96,512]{1,0:T(8,128)(2,1)S(1)} collective-permute-done((bf16[96,512]{1,0:T(8,128)(2,1)S(1)}, bf16[96,512]{1,0:T(8,128)(2,1)S(1)}, u32[]{:S(2)}, u32[]{:S(2)}) %collective-permute-start.16) | collective-permute-done | bytes 98336 | tf_op jit(solution)/shard_map/ppermute | solution.py:42
  99.9 1.1 %shard_map.256 = bf16[96,512]{1,0:T(8,128)(2,1)} custom-call(bf16[1536,128]{1,0:T(8,128)(2,1)S(1)} %bitcast.18, bf16[192,384]{1,0:T(8,128)(2,1)S(1)} %get-tuple-element.38.w, f32[96,128]{1,0:T(8,128)S(1)} %get-tuple-element.39.share0, f32[96,128]{1,0:T(8,128)S(1)} %get-tuple-element.40.share1, bf16[96,512]{1,0:T(8,128)(2,1)S(1)} %get-tuple-element.41.a0.resid, ...), custom_call_target="tpu_custom_call" | custom-call | tf_op jit(solution)/shard_map/pallas_call | solution.py:345
  (44 shorter events, 7.9 us)
Async XLA Ops:
  0.7 27.9 %copy-start.1 = (bf16[1,2048,128]{2,1,0:T(8,128)(2,1)S(1)}, bf16[1,2048,128]{2,1,0:T(8,128)(2,1)}, u32[]{:S(2)}) copy-start(bf16[1,2048,128]{2,1,0:T(8,128)(2,1)} %param.41) | copy-start | bytes 1572868
  0.7 27.9 %copy-start.2 = (bf16[1,2048,128]{2,1,0:T(8,128)(2,1)S(1)}, bf16[1,2048,128]{2,1,0:T(8,128)(2,1)}, u32[]{:S(2)}) copy-start(bf16[1,2048,128]{2,1,0:T(8,128)(2,1)} %param.42) | copy-start | bytes 1572868
  0.7 27.9 %copy-start.3 = (bf16[1,128,2048]{2,1,0:T(8,128)(2,1)S(1)}, bf16[1,128,2048]{2,1,0:T(8,128)(2,1)}, u32[]{:S(2)}) copy-start(bf16[1,128,2048]{2,1,0:T(8,128)(2,1)} %param.43) | copy-start | bytes 1572868
  4.9 26.1 %copy-start.7 = (bf16[2048]{0:T(1024)(128)(2,1)S(1)}, bf16[2048]{0:T(1024)(128)(2,1)}, u32[]{:S(2)}) copy-start(bf16[2048]{0:T(1024)(128)(2,1)} %param.37) | copy-start | bytes 12292
  4.9 5.4 %collective-permute-start = (bf16[96,512]{1,0:T(8,128)(2,1)S(1)}, bf16[96,512]{1,0:T(8,128)(2,1)S(1)}, u32[]{:S(2)}, u32[]{:S(2)}) collective-permute-start(bf16[96,512]{1,0:T(8,128)(2,1)S(1)} %get-tuple-element.27), channel_id=1, source_target_pairs={{0,1},{1,0},{2,3},{3,2},{4,5},{5,4},{6,7},{7,6},{8,9},{9,8},{10,11... | collective-permute-start | bytes 294920 | tf_op jit(solution)/shard_map/ppermute | solution.py:42
  8.2 4.2 %collective-permute-start.1 = (bf16[96,512]{1,0:T(8,128)(2,1)S(1)}, bf16[96,512]{1,0:T(8,128)(2,1)S(1)}, u32[]{:S(2)}, u32[]{:S(2)}) collective-permute-start(bf16[96,512]{1,0:T(8,128)(2,1)S(1)} %get-tuple-element.28), channel_id=1, source_target_pairs={{0,2},{1,3},{2,0},{3,1},{4,6},{5,7},{6,4},{7,5},{8,10},{9,11},{10,... | collective-permute-start | bytes 294920 | tf_op jit(solution)/shard_map/ppermute | solution.py:42
  8.2 6.6 %collective-permute-start.2 = (bf16[96,512]{1,0:T(8,128)(2,1)S(1)}, bf16[96,512]{1,0:T(8,128)(2,1)S(1)}, u32[]{:S(2)}, u32[]{:S(2)}) collective-permute-start(bf16[96,512]{1,0:T(8,128)(2,1)S(1)} %get-tuple-element.29), channel_id=1, source_target_pairs={{0,3},{1,2},{2,1},{3,0},{4,7},{5,6},{6,5},{7,4},{8,11},{9,10},{10,... | collective-permute-start | bytes 294920 | tf_op jit(solution)/shard_map/ppermute | solution.py:42
  15.9 36.2 %all-to-all-start = ((bf16[64,24,128]{2,1,0:T(8,128)(2,1)}), bf16[64,24,128]{2,1,0:T(8,128)(2,1)S(1)}, u32[]{:S(2)}, u32[]{:S(2)}) async-start(bf16[64,24,128]{2,1,0:T(8,128)(2,1)} %bitcast.9), calls=%async_computation | async-start | bytes 786432 | tf_op jit(solution)/shard_map/all_to_all | solution.py:448
  28.8 2.2 %collective-permute-start.3 = (bf16[768,256]{1,0:T(8,128)(2,1)S(1)}, bf16[768,256]{1,0:T(8,128)(2,1)S(1)}, u32[]{:S(2)}, u32[]{:S(2)}) collective-permute-start(bf16[768,256]{1,0:T(8,128)(2,1)S(1)} %get-tuple-element.33), channel_id=1, source_target_pairs={{0,1},{1,0},{2,3},{3,2},{4,5},{5,4},{6,7},{7,6},{8,9},{9,8},{10,11... | collective-permute-start | bytes 1179656 | tf_op jit(solution)/shard_map/ppermute | solution.py:42
  29.3 14.4 %collective-permute-start.4 = (bf16[768,256]{1,0:T(8,128)(2,1)S(1)}, bf16[768,256]{1,0:T(8,128)(2,1)S(1)}, u32[]{:S(2)}, u32[]{:S(2)}) collective-permute-start(bf16[768,256]{1,0:T(8,128)(2,1)S(1)} %get-tuple-element.34), channel_id=1, source_target_pairs={{0,2},{1,3},{2,0},{3,1},{4,6},{5,7},{6,4},{7,5},{8,10},{9,11},{10,... | collective-permute-start | bytes 1179656 | tf_op jit(solution)/shard_map/ppermute | solution.py:42
  29.6 22.5 %collective-permute-start.5 = (bf16[768,256]{1,0:T(8,128)(2,1)S(1)}, bf16[768,256]{1,0:T(8,128)(2,1)S(1)}, u32[]{:S(2)}, u32[]{:S(2)}) collective-permute-start(bf16[768,256]{1,0:T(8,128)(2,1)S(1)} %get-tuple-element.35), channel_id=1, source_target_pairs={{0,3},{1,2},{2,1},{3,0},{4,7},{5,6},{6,5},{7,4},{8,11},{9,10},{10,... | collective-permute-start | bytes 1179656 | tf_op jit(solution)/shard_map/ppermute | solution.py:42
  53.1 1.8 %collective-permute-start.6 = (bf16[392,512]{1,0:T(8,128)(2,1)S(1)}, bf16[392,512]{1,0:T(8,128)(2,1)S(1)}, u32[]{:S(2)}, u32[]{:S(2)}) collective-permute-start(bf16[392,512]{1,0:T(8,128)(2,1)S(1)} %get-tuple-element.37), channel_id=1, source_target_pairs={{0,1},{1,0},{2,3},{3,2},{4,5},{5,4},{6,7},{7,6},{8,9},{9,8},{10,11... | collective-permute-start | bytes 1204232 | tf_op jit(solution)/shard_map/ppermute | solution.py:42
  55.0 33.4 %copy-start.8 = (bf16[2048]{0:T(1024)(128)(2,1)S(1)}, bf16[2048]{0:T(1024)(128)(2,1)}, u32[]{:S(2)}) copy-start(bf16[2048]{0:T(1024)(128)(2,1)} %param.47) | copy-start | bytes 12292
  55.0 6.4 %collective-permute-start.7 = (bf16[400,256]{1,0:T(8,128)(2,1)S(1)}, bf16[400,256]{1,0:T(8,128)(2,1)S(1)}, u32[]{:S(2)}, u32[]{:S(2)}) collective-permute-start(bf16[400,256]{1,0:T(8,128)(2,1)S(1)} %shard_map.252), channel_id=1, source_target_pairs={{0,2},{1,3},{2,0},{3,1},{4,6},{5,7},{6,4},{7,5},{8,10},{9,11},{10,... | collective-permute-start | bytes 614408 | tf_op jit(solution)/shard_map/ppermute | solution.py:42
  61.7 3.6 %collective-permute-start.9 = (bf16[384,128]{1,0:T(8,128)(2,1)S(1)}, bf16[384,128]{1,0:T(8,128)(2,1)S(1)}, u32[]{:S(2)}, u32[]{:S(2)}) collective-permute-start(bf16[384,128]{1,0:T(8,128)(2,1)S(1)} %shard_map.253.h0), channel_id=1, source_target_pairs={{0,2},{1,3},{2,0},{3,1},{4,6},{5,7},{6,4},{7,5},{8,10},{9,11},{10,... | collective-permute-start | bytes 294920 | tf_op jit(solution)/shard_map/ppermute | solution.py:42
  62.3 5.3 %collective-permute-start.8 = (bf16[384,128]{1,0:T(8,128)(2,1)S(1)}, bf16[384,128]{1,0:T(8,128)(2,1)S(1)}, u32[]{:S(2)}, u32[]{:S(2)}) collective-permute-start(bf16[384,128]{1,0:T(8,128)(2,1)S(1)} %shard_map.253.h0), channel_id=1, source_target_pairs={{0,1},{1,0},{2,3},{3,2},{4,5},{5,4},{6,7},{7,6},{8,9},{9,8},{10,11... | collective-permute-start | bytes 294920 | tf_op jit(solution)/shard_map/ppermute | solution.py:42
  65.2 3.3 %collective-permute-start.10 = (bf16[384,128]{1,0:T(8,128)(2,1)S(1)}, bf16[384,128]{1,0:T(8,128)(2,1)S(1)}, u32[]{:S(2)}, u32[]{:S(2)}) collective-permute-start(bf16[384,128]{1,0:T(8,128)(2,1)S(1)} %collective-permute-done.9.h2), channel_id=1, source_target_pairs={{0,1},{1,0},{2,3},{3,2},{4,5},{5,4},{6,7},{7,6},{8,9},{9,8},{10,11... | collective-permute-start | bytes 294920 | tf_op jit(solution)/shard_map/ppermute | solution.py:42
  69.9 30.0 %all-to-all-start.1 = ((bf16[64,24,128]{2,1,0:T(8,128)(2,1)}), bf16[64,24,128]{2,1,0:T(8,128)(2,1)S(1)}, u32[]{:S(2)}, u32[]{:S(2)}) async-start(bf16[64,24,128]{2,1,0:T(8,128)(2,1)} %bitcast.14), calls=%async_computation.1 | async-start | bytes 786432 | tf_op jit(solution)/shard_map/all_to_all | solution.py:483
  81.9 4.7 %collective-permute-start.12 = (bf16[96,512]{1,0:T(8,128)(2,1)S(1)}, bf16[96,512]{1,0:T(8,128)(2,1)S(1)}, u32[]{:S(2)}, u32[]{:S(2)}) collective-permute-start(bf16[96,512]{1,0:T(8,128)(2,1)S(1)} %get-tuple-element.41.a0.resid), channel_id=1, source_target_pairs={{0,2},{1,3},{2,0},{3,1},{4,6},{5,7},{6,4},{7,5},{8,10},{9,11},{10,... | collective-permute-start | bytes 294920 | tf_op jit(solution)/shard_map/ppermute | solution.py:42
  82.2 6.2 %collective-permute-start.11 = (bf16[96,512]{1,0:T(8,128)(2,1)S(1)}, bf16[96,512]{1,0:T(8,128)(2,1)S(1)}, u32[]{:S(2)}, u32[]{:S(2)}) collective-permute-start(bf16[96,512]{1,0:T(8,128)(2,1)S(1)} %get-tuple-element.41.a0.resid), channel_id=1, source_target_pairs={{0,1},{1,0},{2,3},{3,2},{4,5},{5,4},{6,7},{7,6},{8,9},{9,8},{10,11... | collective-permute-start | bytes 294920 | tf_op jit(solution)/shard_map/ppermute | solution.py:42
  86.7 2.7 %collective-permute-start.13 = (bf16[96,512]{1,0:T(8,128)(2,1)S(1)}, bf16[96,512]{1,0:T(8,128)(2,1)S(1)}, u32[]{:S(2)}, u32[]{:S(2)}) collective-permute-start(bf16[96,512]{1,0:T(8,128)(2,1)S(1)} %collective-permute-done.12.a2), channel_id=1, source_target_pairs={{0,1},{1,0},{2,3},{3,2},{4,5},{5,4},{6,7},{7,6},{8,9},{9,8},{10,11... | collective-permute-start | bytes 294920 | tf_op jit(solution)/shard_map/ppermute | solution.py:42
  92.8 2.2 %collective-permute-start.14 = (bf16[96,512]{1,0:T(8,128)(2,1)S(1)}, bf16[96,512]{1,0:T(8,128)(2,1)S(1)}, u32[]{:S(2)}, u32[]{:S(2)}) collective-permute-start(bf16[96,512]{1,0:T(8,128)(2,1)S(1)} %get-tuple-element.44), channel_id=1, source_target_pairs={{0,1},{1,0},{2,3},{3,2},{4,5},{5,4},{6,7},{7,6},{8,9},{9,8},{10,11... | collective-permute-start | bytes 294920 | tf_op jit(solution)/shard_map/ppermute | solution.py:42
  93.3 4.2 %collective-permute-start.15 = (bf16[96,512]{1,0:T(8,128)(2,1)S(1)}, bf16[96,512]{1,0:T(8,128)(2,1)S(1)}, u32[]{:S(2)}, u32[]{:S(2)}) collective-permute-start(bf16[96,512]{1,0:T(8,128)(2,1)S(1)} %get-tuple-element.45), channel_id=1, source_target_pairs={{0,2},{1,3},{2,0},{3,1},{4,6},{5,7},{6,4},{7,5},{8,10},{9,11},{10,... | collective-permute-start | bytes 294920 | tf_op jit(solution)/shard_map/ppermute | solution.py:42
  93.3 6.6 %collective-permute-start.16 = (bf16[96,512]{1,0:T(8,128)(2,1)S(1)}, bf16[96,512]{1,0:T(8,128)(2,1)S(1)}, u32[]{:S(2)}, u32[]{:S(2)}) collective-permute-start(bf16[96,512]{1,0:T(8,128)(2,1)S(1)} %get-tuple-element.46), channel_id=1, source_target_pairs={{0,3},{1,2},{2,1},{3,0},{4,7},{5,6},{6,5},{7,4},{8,11},{9,10},{10,... | collective-permute-start | bytes 294920 | tf_op jit(solution)/shard_map/ppermute | solution.py:42
  (4 other events, 42.1 us)

commit v2 on v0

--- a/solution.py
+++ b/solution.py
@@ -68,25 +68,26 @@
 
 def state_kernel(*refs):
     inputs, (p0, p1, p2, p3, new_re, new_im), held = refs[0:13], refs[13:19], refs[19:32]
-    fresh_re_v, fresh_im_v, sems = refs[32:]
+    fresh_re_v, fresh_im_v, blocks_v, sems = refs[32:]
     t = lax.axis_index("tp")
     loads = [
         pltpu.make_async_copy(a, b, sems.at[i]) for i, (a, b) in enumerate(zip(inputs, held))
     ]
     for load in loads:
         load.start()
-    decay, skip, tokens_v, gain, in_v, b_re, b_im, re_v, im_v, c_re, c_im, out_v, log_step = held
+    log_step, decay, skip, b_re, b_im, c_re, c_im, tokens_v, gain, in_v, re_v, im_v, out_v = held
     groups, entries = decay.shape
     channels = skip.shape[1]
     width = groups * entries
     of_group = iota((1, width), 1) // entries
-    loads[12].wait()
+    for load in loads[0:3]:
+        load.wait()
     logs = jnp.zeros((1, width), F32)
     for g in range(groups):
         logs = jnp.where(of_group == g, log_step[g], logs)
     step = jnp.exp(logs)
-    loads[0].wait()
     eigen = row_of(decay[...])
+    direct = row_of(skip[...])
     freq = math.pi * (iota((1, width), 1) % entries).astype(F32)
     magnitude = jnp.exp(eigen * step)
     turned = freq * step
@@ -95,19 +96,21 @@
     denom = eigen * eigen + freq * freq
     fac_re = ((lam_re - 1.0) * eigen + lam_im * freq) / denom
     fac_im = (lam_im * eigen - (lam_re - 1.0) * freq) / denom
-    loads[2].wait()
-    loads[3].wait()
+    for load in loads[3:7]:
+        load.wait()
+    for k, small in enumerate((b_re, b_im, c_re, c_im)):
+        blocks_v[k] = spread_blocks(small[...], channels)
+    loads[7].wait()
+    loads[8].wait()
     x = tokens_v[...].astype(F32)
     scale = lax.rsqrt(jnp.mean(x * x, axis=-1, keepdims=True) + EPS)
     normed = (x * scale * gain[...].astype(F32).reshape(1, -1)).astype(BF16)
-    loads[4].wait()
+    loads[9].wait()
     drive = dot(normed, in_v[...]).astype(BF16)
-    loads[5].wait()
-    loads[6].wait()
-    in_re = dot(drive, spread_blocks(b_re[...], channels))
-    in_im = dot(drive, spread_blocks(b_im[...], channels))
-    loads[7].wait()
-    loads[8].wait()
+    in_re = dot(drive, blocks_v[0])
+    in_im = dot(drive, blocks_v[1])
+    loads[10].wait()
+    loads[11].wait()
     was_re, was_im = re_v[...], im_v[...]
     fresh_re = lam_re * was_re - lam_im * was_im + (fac_re * in_re - fac_im * in_im)
     fresh_im = lam_re * was_im + lam_im * was_re + (fac_re * in_im + fac_im * in_re)
@@ -119,15 +122,13 @@
     ]
     for store in stores:
         store.start()
-    for i in (1, 9, 10):
-        loads[i].wait()
     mixed = (
-        nt_dot(fresh_re.astype(BF16), spread_blocks(c_re[...], channels))
-        - nt_dot(fresh_im.astype(BF16), spread_blocks(c_im[...], channels))
-        + row_of(skip[...]) * drive.astype(F32)
+        nt_dot(fresh_re.astype(BF16), blocks_v[2])
+        - nt_dot(fresh_im.astype(BF16), blocks_v[3])
+        + direct * drive.astype(F32)
     )
     act = jax.nn.gelu(mixed).astype(BF16)
-    loads[11].wait()
+    loads[12].wait()
     for m, p in enumerate((p0, p1, p2, p3)):
         p[...] = dot(act, out_v[:, cols_of(t ^ m, p.shape[1])]).astype(BF16)
     for store in stores:
@@ -137,11 +138,11 @@
 def reshard_kernel(gate, up, down, *pieces):
     t = lax.axis_index("tp")
     hid = gate.shape[1]
-    for m, (gu, d) in enumerate(zip(pieces[:4], pieces[4:])):
-        part = cols_of(t ^ m, gu.shape[0])
-        gu[:, 0:hid] = gate[part, :]
-        gu[:, hid:] = up[part, :]
-        d[...] = down[:, cols_of(t ^ m, d.shape[1])]
+    for m, (wide, deep) in enumerate(zip(pieces[:4], pieces[4:])):
+        part = cols_of(t ^ m, wide.shape[0])
+        wide[:, 0:hid] = gate[part, :]
+        wide[:, hid:] = up[part, :]
+        deep[...] = down[:, cols_of(t ^ m, deep.shape[1])]
 
 
 def route_kernel(experts, routes, group_weight, logits, z, w, share0, share1, padded):
@@ -244,7 +245,7 @@
         p[...] = dot(hidden, down_v[:, cols_of(t ^ m, quarter)]).astype(BF16)
 
 
-def enter_kernel(capacity, arrived, gains, gu0, gu1, gu2, gu3, keep, send, wide, rows, sums):
+def enter_kernel(capacity, arrived, gains, w0, w1, w2, w3, keep, send, wide, rows, sums):
     t = lax.axis_index("tp")
     lanes = arrived.shape[1]
     quarter = rows.shape[1]
@@ -262,11 +263,11 @@
     )
     send[count:, :] = three_terms(squares, send.shape[1])
     x = rows[...]
-    pair = gu0.shape[1]
-    keep[0:count, 0:pair] = dot(x, gu0[...])
-    send[0:count, 0:pair] = dot(x, gu1[...]).astype(BF16)
-    keep[0:count, pair:] = dot(x, gu2[...])
-    send[0:count, pair:] = dot(x, gu3[...]).astype(BF16)
+    pair = w0.shape[1]
+    keep[0:count, 0:pair] = dot(x, w0[...])
+    send[0:count, 0:pair] = dot(x, w1[...]).astype(BF16)
+    keep[0:count, pair:] = dot(x, w2[...])
+    send[0:count, pair:] = dot(x, w3[...]).astype(BF16)
 
 
 def relay_kernel(keep, came, onward):
@@ -293,10 +294,10 @@
     hidden[...] = (jax.nn.silu(total[:, 0:units] * scale) * (total[:, units:] * scale)).astype(BF16)
 
 
-def leave_kernel(capacity, h0, h1, h2, h3, d0, d1, d2, d3, out, wide):
-    total = dot(h0[...], d0[...])
-    for h, d in ((h1, d1), (h2, d2), (h3, d3)):
-        total = total + dot(h[...], d[...])
+def leave_kernel(capacity, h0, h1, h2, h3, w0, w1, w2, w3, out, wide):
+    total = (dot(h0[...], w0[...]) + dot(h1[...], w1[...])) + (
+        dot(h2[...], w2[...]) + dot(h3[...], w3[...])
+    )
     for strided, near, cols in places(capacity, wide, total.shape[1]):
         wide[strided, :] = total[near, cols]
     out[...] = wide[...].astype(BF16)
@@ -392,26 +393,27 @@
 
     states = ((rows, groups * entries), F32)
     state_inputs = (
+        log_step,
         eigen_decay_real,
         channel_skip_scale,
+        by_channel(input_matrix_real),
+        by_channel(input_matrix_imaginary),
+        output_matrix_real.reshape(groups * channels, entries),
+        output_matrix_imaginary.reshape(groups * channels, entries),
         tokens,
         norm_gain,
         in_weight,
-        by_channel(input_matrix_real),
-        by_channel(input_matrix_imaginary),
         sequence_state_real,
         sequence_state_imaginary,
-        output_matrix_real.reshape(groups * channels, entries),
-        output_matrix_imaginary.reshape(groups * channels, entries),
         out_weight,
-        log_step,
     )
     *mix, new_re, new_im = call(
         state_kernel,
         [piece] * 4 + [states] * 2,
-        [pltpu.VMEM(x.shape, x.dtype) for x in state_inputs[:-1]]
-        + [pltpu.SMEM(log_step.shape, F32)]
+        [pltpu.SMEM(log_step.shape, F32)]
+        + [pltpu.VMEM(x.shape, x.dtype) for x in state_inputs[1:]]
         + [pltpu.VMEM(states[0], F32)] * 2
+        + [pltpu.VMEM((4, groups * channels, groups * entries), BF16)]
         + [pltpu.SemaphoreType.DMA((15,))],
         20,
         [HBM] * 13,
@@ -421,7 +423,9 @@
     pieces = call(
         reshard_kernel, [((quarter, 2 * hid), BF16)] * 4 + [((hid, quarter), BF16)] * 4
     )(gate, up, down)
-    moved = [pieces[0]] + [exchanged(pieces[m], m) for m in (1, 2, 3)]
+    wide2 = exchanged(pieces[2], 2)
+    wide3 = exchanged(pieces[3], 3)
+    moved = [pieces[0], exchanged(pieces[1], 1), wide2, wide3]
     downs = [pieces[4]] + [exchanged(pieces[4 + m], m) for m in (1, 2, 3)]
     z, w, share0, share1 = call(
         functools.partial(route_kernel, ep),
@@ -436,10 +440,11 @@
         8,
         out_specs=[VMEM, FREE],
     )(tokens, *mix, z)
+    across = exchanged(resid16, 2)
     arrived = lax.all_to_all(
         packed.reshape(ep, capacity * blocks, lanes), "ep", 0, 0, tiled=True
     ).reshape(slots * blocks, lanes)
-    near = gathered(resid16)
+    near = [resid16, exchanged(resid16, 1), across, exchanged(across, 1)]
     gains = ffn_gain.reshape(1, width)
     *dense, blend = call(
         dense_kernel,
@@ -449,6 +454,7 @@
         + [pltpu.SemaphoreType.DMA((3,))],
         12,
         [VMEM] * 6 + [HBM] * 3,
+        [FREE] * 5,
     )(gains, *near, blend_weight.reshape(1, width), dense_gate, dense_up, dense_down)
     dense = [dense[0]] + [exchanged(dense[m], m) for m in (1, 2, 3)]
     keep, send = call(
@@ -463,13 +469,14 @@
     (hidden,) = call(
         functools.partial(hidden_kernel, float(width)), [((slots, hid), BF16)]
     )(keep, came, last)
+    hidden = gathered(hidden)
     (sent,) = call(
         functools.partial(leave_kernel, capacity),
         [((slots * blocks, lanes), BF16)],
         [wide],
         8,
         out_specs=[FREE],
-    )(*gathered(hidden), *downs)
+    )(*hidden, *downs)
     returned = lax.all_to_all(
         sent.reshape(ep, capacity * blocks, lanes), "ep", 0, 0, tiled=True
     ).reshape(slots * blocks, lanes)

time: 99.4 us -> 99.3 us (level)
  no operation moved by 1% of the time
where the time goes in v2:
time: 99.3 us; the launch traced here: 99 us
  starting transfers between devices  44.2 us (45%)
  waiting for transfers between devices  40.9 us (41%)
  Pallas kernels  13.1 us (13%)
    ppermute x20, waiting for transfers between devices, exchanged(): return lax.ppermute(value, 'tp', [(i, i ^ mask) for i in range(4)])  40.9 us
    ppermute x20, starting transfers between devices, exchanged(): return lax.ppermute(value, 'tp', [(i, i ^ mask) for i in range(4)])  19.8 us
    pallas_call x10, Pallas kernels, run(): pl.pallas_call(kernel, out_shape=tuple(out_shape), in_specs=specs, out_sp...  13.1 us
    all_to_all x1, starting transfers between devices, per_device(): lax.all_to_all(packed.reshape(ep, capacity * blocks, lanes), 'ep', 0, 0,...  12.6 us
    all_to_all x1, starting transfers between devices, per_device(): lax.all_to_all(sent.reshape(ep, capacity * blocks, lanes), 'ep', 0, 0, ti...  11.8 us
  transfers between devices with their start and end apart: 22, of which 12 were waited for; matrix products, arithmetic and copies ran while one was open for 0% of the time, Pallas kernels for 4%

profile of v2, /device:TPU:1, one launch (start us, length us, event | category | flops | bytes accessed | tf_op | source)
XLA Modules:
  0.0 99.0 jit_solution(16966902371020710470)
XLA Ops:
  0.7 4.1 %shard_map.247 = (bf16[96,512]{1,0:T(8,128)(2,1)S(1)}, bf16[96,512]{1,0:T(8,128)(2,1)S(1)}, bf16[96,512]{1,0:T(8,128)(2,1)S(1)}, bf16[96,512]{1,0:T(8,128)(2,1)S...) custom-call(f32[16]{0:T(128)} %refs_0_.1, f32[16,64]{1,0:T(8,128)} %refs_1_.1, f32[16,16]{1,0:T(8,128)} %refs_2_.1, ...), custom_call_target="tpu_custom_call" | custom-call | tf_op jit(solution)/shard_map/pallas_call | solution.py:338
  4.9 3.3 %collective-permute-start = (bf16[96,512]{1,0:T(8,128)(2,1)S(1)}, bf16[96,512]{1,0:T(8,128)(2,1)S(1)}, u32[]{:S(2)}, u32[]{:S(2)}) collective-permute-start(bf16[96,512]{1,0:T(8,128)(2,1)S(1)} %get-tuple-element.31), channel_id=1, source_target_pairs={{0,1},{1,0},{2,3},{3,2},{4,5},{5,4},{6,7},{7,6},{8,9},{9,8},{10,11... | collective-permute-start | bytes 294920 | tf_op jit(solution)/shard_map/ppermute | solution.py:42
  8.2 1.7 %collective-permute-start.2 = (bf16[96,512]{1,0:T(8,128)(2,1)S(1)}, bf16[96,512]{1,0:T(8,128)(2,1)S(1)}, u32[]{:S(2)}, u32[]{:S(2)}) collective-permute-start(bf16[96,512]{1,0:T(8,128)(2,1)S(1)} %get-tuple-element.33), channel_id=1, source_target_pairs={{0,3},{1,2},{2,1},{3,0},{4,7},{5,6},{6,5},{7,4},{8,11},{9,10},{10,... | collective-permute-start | bytes 294920 | tf_op jit(solution)/shard_map/ppermute | solution.py:42
  10.2 2.2 %collective-permute-done.1.p2 = bf16[96,512]{1,0:T(8,128)(2,1)S(1)} collective-permute-done((bf16[96,512]{1,0:T(8,128)(2,1)S(1)}, bf16[96,512]{1,0:T(8,128)(2,1)S(1)}, u32[]{:S(2)}, u32[]{:S(2)}) %collective-permute-start.1) | collective-permute-done | bytes 98336 | tf_op jit(solution)/shard_map/ppermute | solution.py:42
  12.4 2.4 %collective-permute-done.2.p3 = bf16[96,512]{1,0:T(8,128)(2,1)S(1)} collective-permute-done((bf16[96,512]{1,0:T(8,128)(2,1)S(1)}, bf16[96,512]{1,0:T(8,128)(2,1)S(1)}, u32[]{:S(2)}, u32[]{:S(2)}) %collective-permute-start.2) | collective-permute-done | bytes 98336 | tf_op jit(solution)/shard_map/ppermute | solution.py:42
  14.8 1.1 %shard_map.249 = (bf16[96,512]{1,0:T(8,128)(2,1)S(1)}, bf16[1536,128]{1,0:T(8,128)(2,1)}) custom-call(bf16[96,2048]{1,0:T(8,128)(2,1)S(1)} %copy-done, bf16[96,512]{1,0:T(8,128)(2,1)S(1)} %get-tuple-element.30.p0, bf16[96,512]{1,0:T(8,128)(2,1)S(1)} %collective-permute-done.p1, bf16[96,512]{1,0:T(8,128)(2,1)S(1)} %collective-permute-done.1.p2, ...), custom_call_target="tpu_custom_call" | custom-call | tf_op jit(solution)/shard_map/pallas_call | solution.py:338
  15.9 12.6 %all-to-all-start = ((bf16[64,24,128]{2,1,0:T(8,128)(2,1)}), bf16[64,24,128]{2,1,0:T(8,128)(2,1)S(1)}, u32[]{:S(2)}, u32[]{:S(2)}) async-start(bf16[64,24,128]{2,1,0:T(8,128)(2,1)} %bitcast.9), calls=%async_computation | async-start | bytes 786432 | tf_op jit(solution)/shard_map/all_to_all | solution.py:444
  29.6 1.4 %collective-permute-start.5 = (bf16[512,256]{1,0:T(8,128)(2,1)S(1)}, bf16[512,256]{1,0:T(8,128)(2,1)S(1)}, u32[]{:S(2)}, u32[]{:S(2)}) collective-permute-start(bf16[512,256]{1,0:T(8,128)(2,1)S(1)} %get-tuple-element.39), channel_id=1, source_target_pairs={{0,3},{1,2},{2,1},{3,0},{4,7},{5,6},{6,5},{7,4},{8,11},{9,10},{10,... | collective-permute-start | bytes 786440 | tf_op jit(solution)/shard_map/ppermute | solution.py:42
  31.0 9.7 %collective-permute-done.4.w2 = bf16[512,256]{1,0:T(8,128)(2,1)S(1)} collective-permute-done((bf16[512,256]{1,0:T(8,128)(2,1)S(1)}, bf16[512,256]{1,0:T(8,128)(2,1)S(1)}, u32[]{:S(2)}, u32[]{:S(2)}) %collective-permute-start.4) | collective-permute-done | bytes 262176 | tf_op jit(solution)/shard_map/ppermute | solution.py:42
  40.7 5.8 %collective-permute-done.5.w3 = bf16[512,256]{1,0:T(8,128)(2,1)S(1)} collective-permute-done((bf16[512,256]{1,0:T(8,128)(2,1)S(1)}, bf16[512,256]{1,0:T(8,128)(2,1)S(1)}, u32[]{:S(2)}, u32[]{:S(2)}) %collective-permute-start.5) | collective-permute-done | bytes 262176 | tf_op jit(solution)/shard_map/ppermute | solution.py:42
  47.9 1.4 %collective-permute-done.6.came = bf16[392,512]{1,0:T(8,128)(2,1)S(1)} collective-permute-done((bf16[392,512]{1,0:T(8,128)(2,1)S(1)}, bf16[392,512]{1,0:T(8,128)(2,1)S(1)}, u32[]{:S(2)}, u32[]{:S(2)}) %collective-permute-start.6) | collective-permute-done | bytes 401440 | tf_op jit(solution)/shard_map/ppermute | solution.py:42
  49.8 5.9 %collective-permute-done.7.last = bf16[400,256]{1,0:T(8,128)(2,1)S(1)} collective-permute-done((bf16[400,256]{1,0:T(8,128)(2,1)S(1)}, bf16[400,256]{1,0:T(8,128)(2,1)S(1)}, u32[]{:S(2)}, u32[]{:S(2)}) %collective-permute-start.7) | collective-permute-done | bytes 204832 | tf_op jit(solution)/shard_map/ppermute | solution.py:42
  56.6 1.3 %collective-permute-start.11 = (bf16[128,512]{1,0:T(8,128)(2,1)S(1)}, bf16[128,512]{1,0:T(8,128)(2,1)S(1)}, u32[]{:S(2)}, u32[]{:S(2)}) collective-permute-start(bf16[128,512]{1,0:T(8,128)(2,1)S(1)} %get-tuple-element.43), channel_id=1, source_target_pairs={{0,1},{1,0},{2,3},{3,2},{4,5},{5,4},{6,7},{7,6},{8,9},{9,8},{10,11... | collective-permute-start | bytes 393224 | tf_op jit(solution)/shard_map/ppermute | solution.py:42
  59.8 3.0 %collective-permute-start.10 = (bf16[384,128]{1,0:T(8,128)(2,1)S(1)}, bf16[384,128]{1,0:T(8,128)(2,1)S(1)}, u32[]{:S(2)}, u32[]{:S(2)}) collective-permute-start(bf16[384,128]{1,0:T(8,128)(2,1)S(1)} %collective-permute-done.9.h2), channel_id=1, source_target_pairs={{0,1},{1,0},{2,3},{3,2},{4,5},{5,4},{6,7},{7,6},{8,9},{9,8},{10,11... | collective-permute-start | bytes 294920 | tf_op jit(solution)/shard_map/ppermute | solution.py:42
  63.5 3.4 %collective-permute-done.13.w3 = bf16[128,512]{1,0:T(8,128)(2,1)S(1)} collective-permute-done((bf16[128,512]{1,0:T(8,128)(2,1)S(1)}, bf16[128,512]{1,0:T(8,128)(2,1)S(1)}, u32[]{:S(2)}, u32[]{:S(2)}) %collective-permute-start.13) | collective-permute-done | bytes 131104 | tf_op jit(solution)/shard_map/ppermute | solution.py:42
  66.9 1.4 %shard_map.254 = bf16[1536,128]{1,0:T(8,128)(2,1)} custom-call(bf16[384,128]{1,0:T(8,128)(2,1)S(1)} %shard_map.253.h0, bf16[384,128]{1,0:T(8,128)(2,1)S(1)} %collective-permute-done.8.h1, bf16[384,128]{1,0:T(8,128)(2,1)S(1)} %collective-permute-done.9.h2, bf16[384,128]{1,0:T(8,128)(2,1)S(1)} %collective-permute-done.10.h3, ...), custom_call_target="tpu_custom_call" | custom-call | tf_op jit(solution)/shard_map/pallas_call | solution.py:338
  68.3 11.8 %all-to-all-start.1 = ((bf16[64,24,128]{2,1,0:T(8,128)(2,1)}), bf16[64,24,128]{2,1,0:T(8,128)(2,1)S(1)}, u32[]{:S(2)}, u32[]{:S(2)}) async-start(bf16[64,24,128]{2,1,0:T(8,128)(2,1)} %bitcast.14), calls=%async_computation.1 | async-start | bytes 786432 | tf_op jit(solution)/shard_map/all_to_all | solution.py:480
  81.1 3.8 %collective-permute-done.15.a2 = bf16[96,512]{1,0:T(8,128)(2,1)S(1)} collective-permute-done((bf16[96,512]{1,0:T(8,128)(2,1)S(1)}, bf16[96,512]{1,0:T(8,128)(2,1)S(1)}, u32[]{:S(2)}, u32[]{:S(2)}) %collective-permute-start.15) | collective-permute-done | bytes 98336 | tf_op jit(solution)/shard_map/ppermute | solution.py:42
  84.9 1.7 %collective-permute-start.16 = (bf16[96,512]{1,0:T(8,128)(2,1)S(1)}, bf16[96,512]{1,0:T(8,128)(2,1)S(1)}, u32[]{:S(2)}, u32[]{:S(2)}) collective-permute-start(bf16[96,512]{1,0:T(8,128)(2,1)S(1)} %collective-permute-done.15.a2), channel_id=1, source_target_pairs={{0,1},{1,0},{2,3},{3,2},{4,5},{5,4},{6,7},{7,6},{8,9},{9,8},{10,11... | collective-permute-start | bytes 294920 | tf_op jit(solution)/shard_map/ppermute | solution.py:42
  87.5 3.4 %shard_map.255 = (bf16[96,512]{1,0:T(8,128)(2,1)S(1)}, bf16[96,512]{1,0:T(8,128)(2,1)S(1)}, bf16[96,512]{1,0:T(8,128)(2,1)S(1)}, bf16[96,512]{1,0:T(8,128)(2,1)S(1)}, f32[96,128]{1,0:T(8,128)S(1)}) custom-call(bf16[1,2048]{1,0:T(2,128)(2,1)S(1)} %reshape.55.gains, bf16[96,512]{1,0:T(8,128)(2,1)S(1)} %get-tuple-element.49.a0.resid, ...), custom_call_target="tpu_custom_call" | custom-call | tf_op jit(solution)/shard_map/pallas_call | solution.py:338
  91.6 1.5 %collective-permute-start.19 = (bf16[96,512]{1,0:T(8,128)(2,1)S(1)}, bf16[96,512]{1,0:T(8,128)(2,1)S(1)}, u32[]{:S(2)}, u32[]{:S(2)}) collective-permute-start(bf16[96,512]{1,0:T(8,128)(2,1)S(1)} %get-tuple-element.54), channel_id=1, source_target_pairs={{0,3},{1,2},{2,1},{3,0},{4,7},{5,6},{6,5},{7,4},{8,11},{9,10},{10,... | collective-permute-start | bytes 294920 | tf_op jit(solution)/shard_map/ppermute | solution.py:42
  93.1 2.4 %collective-permute-done.18.p2 = bf16[96,512]{1,0:T(8,128)(2,1)S(1)} collective-permute-done((bf16[96,512]{1,0:T(8,128)(2,1)S(1)}, bf16[96,512]{1,0:T(8,128)(2,1)S(1)}, u32[]{:S(2)}, u32[]{:S(2)}) %collective-permute-start.18) | collective-permute-done | bytes 98336 | tf_op jit(solution)/shard_map/ppermute | solution.py:42
  95.5 2.4 %collective-permute-done.19.p3 = bf16[96,512]{1,0:T(8,128)(2,1)S(1)} collective-permute-done((bf16[96,512]{1,0:T(8,128)(2,1)S(1)}, bf16[96,512]{1,0:T(8,128)(2,1)S(1)}, u32[]{:S(2)}, u32[]{:S(2)}) %collective-permute-start.19) | collective-permute-done | bytes 98336 | tf_op jit(solution)/shard_map/ppermute | solution.py:42
  97.9 1.1 %shard_map.256 = bf16[96,512]{1,0:T(8,128)(2,1)} custom-call(bf16[1536,128]{1,0:T(8,128)(2,1)S(1)} %bitcast.18, bf16[192,384]{1,0:T(8,128)(2,1)S(1)} %get-tuple-element.46.w, f32[96,128]{1,0:T(8,128)S(1)} %get-tuple-element.47.share0, f32[96,128]{1,0:T(8,128)S(1)} %get-tuple-element.48.share1, bf16[96,512]{1,0:T(8,128)(2,1)S(1)} %get-tuple-element.49.a0.resid, ...), custom_call_target="tpu_custom_call" | custom-call | tf_op jit(solution)/shard_map/pallas_call | solution.py:338
  (50 shorter events, 9.5 us)
Async XLA Ops:
  0.7 27.8 %copy-start.1 = (bf16[1,2048,128]{2,1,0:T(8,128)(2,1)S(1)}, bf16[1,2048,128]{2,1,0:T(8,128)(2,1)}, u32[]{:S(2)}) copy-start(bf16[1,2048,128]{2,1,0:T(8,128)(2,1)} %param.41) | copy-start | bytes 1572868
  4.9 5.4 %collective-permute-start = (bf16[96,512]{1,0:T(8,128)(2,1)S(1)}, bf16[96,512]{1,0:T(8,128)(2,1)S(1)}, u32[]{:S(2)}, u32[]{:S(2)}) collective-permute-start(bf16[96,512]{1,0:T(8,128)(2,1)S(1)} %get-tuple-element.31), channel_id=1, source_target_pairs={{0,1},{1,0},{2,3},{3,2},{4,5},{5,4},{6,7},{7,6},{8,9},{9,8},{10,11... | collective-permute-start | bytes 294920 | tf_op jit(solution)/shard_map/ppermute | solution.py:42
  8.2 4.2 %collective-permute-start.1 = (bf16[96,512]{1,0:T(8,128)(2,1)S(1)}, bf16[96,512]{1,0:T(8,128)(2,1)S(1)}, u32[]{:S(2)}, u32[]{:S(2)}) collective-permute-start(bf16[96,512]{1,0:T(8,128)(2,1)S(1)} %get-tuple-element.32), channel_id=1, source_target_pairs={{0,2},{1,3},{2,0},{3,1},{4,6},{5,7},{6,4},{7,5},{8,10},{9,11},{10,... | collective-permute-start | bytes 294920 | tf_op jit(solution)/shard_map/ppermute | solution.py:42
  8.2 6.6 %collective-permute-start.2 = (bf16[96,512]{1,0:T(8,128)(2,1)S(1)}, bf16[96,512]{1,0:T(8,128)(2,1)S(1)}, u32[]{:S(2)}, u32[]{:S(2)}) collective-permute-start(bf16[96,512]{1,0:T(8,128)(2,1)S(1)} %get-tuple-element.33), channel_id=1, source_target_pairs={{0,3},{1,2},{2,1},{3,0},{4,7},{5,6},{6,5},{7,4},{8,11},{9,10},{10,... | collective-permute-start | bytes 294920 | tf_op jit(solution)/shard_map/ppermute | solution.py:42
  15.9 30.5 %all-to-all-start = ((bf16[64,24,128]{2,1,0:T(8,128)(2,1)}), bf16[64,24,128]{2,1,0:T(8,128)(2,1)S(1)}, u32[]{:S(2)}, u32[]{:S(2)}) async-start(bf16[64,24,128]{2,1,0:T(8,128)(2,1)} %bitcast.9), calls=%async_computation | async-start | bytes 786432 | tf_op jit(solution)/shard_map/all_to_all | solution.py:444
  28.8 2.2 %collective-permute-start.3 = (bf16[512,256]{1,0:T(8,128)(2,1)S(1)}, bf16[512,256]{1,0:T(8,128)(2,1)S(1)}, u32[]{:S(2)}, u32[]{:S(2)}) collective-permute-start(bf16[512,256]{1,0:T(8,128)(2,1)S(1)} %get-tuple-element.37), channel_id=1, source_target_pairs={{0,1},{1,0},{2,3},{3,2},{4,5},{5,4},{6,7},{7,6},{8,9},{9,8},{10,11... | collective-permute-start | bytes 786440 | tf_op jit(solution)/shard_map/ppermute | solution.py:42
  29.2 11.5 %collective-permute-start.4 = (bf16[512,256]{1,0:T(8,128)(2,1)S(1)}, bf16[512,256]{1,0:T(8,128)(2,1)S(1)}, u32[]{:S(2)}, u32[]{:S(2)}) collective-permute-start(bf16[512,256]{1,0:T(8,128)(2,1)S(1)} %get-tuple-element.38), channel_id=1, source_target_pairs={{0,2},{1,3},{2,0},{3,1},{4,6},{5,7},{6,4},{7,5},{8,10},{9,11},{10,... | collective-permute-start | bytes 786440 | tf_op jit(solution)/shard_map/ppermute | solution.py:42
  29.6 16.9 %collective-permute-start.5 = (bf16[512,256]{1,0:T(8,128)(2,1)S(1)}, bf16[512,256]{1,0:T(8,128)(2,1)S(1)}, u32[]{:S(2)}, u32[]{:S(2)}) collective-permute-start(bf16[512,256]{1,0:T(8,128)(2,1)S(1)} %get-tuple-element.39), channel_id=1, source_target_pairs={{0,3},{1,2},{2,1},{3,0},{4,7},{5,6},{6,5},{7,4},{8,11},{9,10},{10,... | collective-permute-start | bytes 786440 | tf_op jit(solution)/shard_map/ppermute | solution.py:42
  47.4 1.8 %collective-permute-start.6 = (bf16[392,512]{1,0:T(8,128)(2,1)S(1)}, bf16[392,512]{1,0:T(8,128)(2,1)S(1)}, u32[]{:S(2)}, u32[]{:S(2)}) collective-permute-start(bf16[392,512]{1,0:T(8,128)(2,1)S(1)} %get-tuple-element.41), channel_id=1, source_target_pairs={{0,1},{1,0},{2,3},{3,2},{4,5},{5,4},{6,7},{7,6},{8,9},{9,8},{10,11... | collective-permute-start | bytes 1204232 | tf_op jit(solution)/shard_map/ppermute | solution.py:42
  49.3 37.2 %copy-start.8 = (bf16[2048]{0:T(1024)(128)(2,1)S(1)}, bf16[2048]{0:T(1024)(128)(2,1)}, u32[]{:S(2)}) copy-start(bf16[2048]{0:T(1024)(128)(2,1)} %param.47) | copy-start | bytes 12292
  49.3 6.4 %collective-permute-start.7 = (bf16[400,256]{1,0:T(8,128)(2,1)S(1)}, bf16[400,256]{1,0:T(8,128)(2,1)S(1)}, u32[]{:S(2)}, u32[]{:S(2)}) collective-permute-start(bf16[400,256]{1,0:T(8,128)(2,1)S(1)} %shard_map.252), channel_id=1, source_target_pairs={{0,2},{1,3},{2,0},{3,1},{4,6},{5,7},{6,4},{7,5},{8,10},{9,11},{10,... | collective-permute-start | bytes 614408 | tf_op jit(solution)/shard_map/ppermute | solution.py:42
  56.0 3.8 %collective-permute-start.9 = (bf16[384,128]{1,0:T(8,128)(2,1)S(1)}, bf16[384,128]{1,0:T(8,128)(2,1)S(1)}, u32[]{:S(2)}, u32[]{:S(2)}) collective-permute-start(bf16[384,128]{1,0:T(8,128)(2,1)S(1)} %shard_map.253.h0), channel_id=1, source_target_pairs={{0,2},{1,3},{2,0},{3,1},{4,6},{5,7},{6,4},{7,5},{8,10},{9,11},{10,... | collective-permute-start | bytes 294920 | tf_op jit(solution)/shard_map/ppermute | solution.py:42
  56.6 6.2 %collective-permute-start.11 = (bf16[128,512]{1,0:T(8,128)(2,1)S(1)}, bf16[128,512]{1,0:T(8,128)(2,1)S(1)}, u32[]{:S(2)}, u32[]{:S(2)}) collective-permute-start(bf16[128,512]{1,0:T(8,128)(2,1)S(1)} %get-tuple-element.43), channel_id=1, source_target_pairs={{0,1},{1,0},{2,3},{3,2},{4,5},{5,4},{6,7},{7,6},{8,9},{9,8},{10,11... | collective-permute-start | bytes 393224 | tf_op jit(solution)/shard_map/ppermute | solution.py:42
  58.0 5.5 %collective-permute-start.12 = (bf16[128,512]{1,0:T(8,128)(2,1)S(1)}, bf16[128,512]{1,0:T(8,128)(2,1)S(1)}, u32[]{:S(2)}, u32[]{:S(2)}) collective-permute-start(bf16[128,512]{1,0:T(8,128)(2,1)S(1)} %get-tuple-element.44), channel_id=1, source_target_pairs={{0,2},{1,3},{2,0},{3,1},{4,6},{5,7},{6,4},{7,5},{8,10},{9,11},{10,... | collective-permute-start | bytes 393224 | tf_op jit(solution)/shard_map/ppermute | solution.py:42
  59.1 7.8 %collective-permute-start.13 = (bf16[128,512]{1,0:T(8,128)(2,1)S(1)}, bf16[128,512]{1,0:T(8,128)(2,1)S(1)}, u32[]{:S(2)}, u32[]{:S(2)}) collective-permute-start(bf16[128,512]{1,0:T(8,128)(2,1)S(1)} %get-tuple-element.45), channel_id=1, source_target_pairs={{0,3},{1,2},{2,1},{3,0},{4,7},{5,6},{6,5},{7,4},{8,11},{9,10},{10,... | collective-permute-start | bytes 393224 | tf_op jit(solution)/shard_map/ppermute | solution.py:42
  59.6 7.3 %collective-permute-start.8 = (bf16[384,128]{1,0:T(8,128)(2,1)S(1)}, bf16[384,128]{1,0:T(8,128)(2,1)S(1)}, u32[]{:S(2)}, u32[]{:S(2)}) collective-permute-start(bf16[384,128]{1,0:T(8,128)(2,1)S(1)} %shard_map.253.h0), channel_id=1, source_target_pairs={{0,1},{1,0},{2,3},{3,2},{4,5},{5,4},{6,7},{7,6},{8,9},{9,8},{10,11... | collective-permute-start | bytes 294920 | tf_op jit(solution)/shard_map/ppermute | solution.py:42
  59.8 7.0 %collective-permute-start.10 = (bf16[384,128]{1,0:T(8,128)(2,1)S(1)}, bf16[384,128]{1,0:T(8,128)(2,1)S(1)}, u32[]{:S(2)}, u32[]{:S(2)}) collective-permute-start(bf16[384,128]{1,0:T(8,128)(2,1)S(1)} %collective-permute-done.9.h2), channel_id=1, source_target_pairs={{0,1},{1,0},{2,3},{3,2},{4,5},{5,4},{6,7},{7,6},{8,9},{9,8},{10,11... | collective-permute-start | bytes 294920 | tf_op jit(solution)/shard_map/ppermute | solution.py:42
  68.3 29.7 %all-to-all-start.1 = ((bf16[64,24,128]{2,1,0:T(8,128)(2,1)}), bf16[64,24,128]{2,1,0:T(8,128)(2,1)S(1)}, u32[]{:S(2)}, u32[]{:S(2)}) async-start(bf16[64,24,128]{2,1,0:T(8,128)(2,1)} %bitcast.14), calls=%async_computation.1 | async-start | bytes 786432 | tf_op jit(solution)/shard_map/all_to_all | solution.py:480
  80.1 4.8 %collective-permute-start.15 = (bf16[96,512]{1,0:T(8,128)(2,1)S(1)}, bf16[96,512]{1,0:T(8,128)(2,1)S(1)}, u32[]{:S(2)}, u32[]{:S(2)}) collective-permute-start(bf16[96,512]{1,0:T(8,128)(2,1)S(1)} %get-tuple-element.49.a0.resid), channel_id=1, source_target_pairs={{0,2},{1,3},{2,0},{3,1},{4,6},{5,7},{6,4},{7,5},{8,10},{9,11},{10,... | collective-permute-start | bytes 294920 | tf_op jit(solution)/shard_map/ppermute | solution.py:42
  80.4 6.1 %collective-permute-start.14 = (bf16[96,512]{1,0:T(8,128)(2,1)S(1)}, bf16[96,512]{1,0:T(8,128)(2,1)S(1)}, u32[]{:S(2)}, u32[]{:S(2)}) collective-permute-start(bf16[96,512]{1,0:T(8,128)(2,1)S(1)} %get-tuple-element.49.a0.resid), channel_id=1, source_target_pairs={{0,1},{1,0},{2,3},{3,2},{4,5},{5,4},{6,7},{7,6},{8,9},{9,8},{10,11... | collective-permute-start | bytes 294920 | tf_op jit(solution)/shard_map/ppermute | solution.py:42
  84.9 2.6 %collective-permute-start.16 = (bf16[96,512]{1,0:T(8,128)(2,1)S(1)}, bf16[96,512]{1,0:T(8,128)(2,1)S(1)}, u32[]{:S(2)}, u32[]{:S(2)}) collective-permute-start(bf16[96,512]{1,0:T(8,128)(2,1)S(1)} %collective-permute-done.15.a2), channel_id=1, source_target_pairs={{0,1},{1,0},{2,3},{3,2},{4,5},{5,4},{6,7},{7,6},{8,9},{9,8},{10,11... | collective-permute-start | bytes 294920 | tf_op jit(solution)/shard_map/ppermute | solution.py:42
  90.9 2.2 %collective-permute-start.17 = (bf16[96,512]{1,0:T(8,128)(2,1)S(1)}, bf16[96,512]{1,0:T(8,128)(2,1)S(1)}, u32[]{:S(2)}, u32[]{:S(2)}) collective-permute-start(bf16[96,512]{1,0:T(8,128)(2,1)S(1)} %get-tuple-element.52), channel_id=1, source_target_pairs={{0,1},{1,0},{2,3},{3,2},{4,5},{5,4},{6,7},{7,6},{8,9},{9,8},{10,11... | collective-permute-start | bytes 294920 | tf_op jit(solution)/shard_map/ppermute | solution.py:42
  91.3 4.2 %collective-permute-start.18 = (bf16[96,512]{1,0:T(8,128)(2,1)S(1)}, bf16[96,512]{1,0:T(8,128)(2,1)S(1)}, u32[]{:S(2)}, u32[]{:S(2)}) collective-permute-start(bf16[96,512]{1,0:T(8,128)(2,1)S(1)} %get-tuple-element.53), channel_id=1, source_target_pairs={{0,2},{1,3},{2,0},{3,1},{4,6},{5,7},{6,4},{7,5},{8,10},{9,11},{10,... | collective-permute-start | bytes 294920 | tf_op jit(solution)/shard_map/ppermute | solution.py:42
  91.6 6.3 %collective-permute-start.19 = (bf16[96,512]{1,0:T(8,128)(2,1)S(1)}, bf16[96,512]{1,0:T(8,128)(2,1)S(1)}, u32[]{:S(2)}, u32[]{:S(2)}) collective-permute-start(bf16[96,512]{1,0:T(8,128)(2,1)S(1)} %get-tuple-element.54), channel_id=1, source_target_pairs={{0,3},{1,2},{2,1},{3,0},{4,7},{5,6},{6,5},{7,4},{8,11},{9,10},{10,... | collective-permute-start | bytes 294920 | tf_op jit(solution)/shard_map/ppermute | solution.py:42
  (7 other events, 123.6 us)

commit v3 on v2

--- a/solution.py
+++ b/solution.py
@@ -67,8 +67,8 @@
 
 
 def state_kernel(*refs):
-    inputs, (p0, p1, p2, p3, new_re, new_im), held = refs[0:13], refs[13:19], refs[19:32]
-    fresh_re_v, fresh_im_v, blocks_v, sems = refs[32:]
+    inputs, (own, beside, new_re, new_im), held = refs[0:13], refs[13:17], refs[17:30]
+    fresh_re_v, fresh_im_v, blocks_v, sems = refs[30:]
     t = lax.axis_index("tp")
     loads = [
         pltpu.make_async_copy(a, b, sems.at[i]) for i, (a, b) in enumerate(zip(inputs, held))
@@ -129,20 +129,37 @@
     )
     act = jax.nn.gelu(mixed).astype(BF16)
     loads[12].wait()
-    for m, p in enumerate((p0, p1, p2, p3)):
-        p[...] = dot(act, out_v[:, cols_of(t ^ m, p.shape[1])]).astype(BF16)
+    quarter = own.shape[1] // 2
+    for m, pair in ((1, beside), (3, beside), (0, own), (2, own)):
+        near = pl.ds((m // 2) * quarter, quarter)
+        pair[:, near] = dot(act, out_v[:, cols_of(t ^ m, quarter)]).astype(BF16)
     for store in stores:
         store.wait()
 
 
-def reshard_kernel(gate, up, down, *pieces):
+def half_kernel(own, came, onward):
+    quarter = onward.shape[1]
+    onward[...] = (own[:, quarter:].astype(F32) + came[:, quarter:].astype(F32)).astype(BF16)
+
+
+def reshard_kernel(gate, up, down, *refs):
+    pieces, sems = refs[:8], refs[8]
     t = lax.axis_index("tp")
     hid = gate.shape[1]
-    for m, (wide, deep) in enumerate(zip(pieces[:4], pieces[4:])):
+    copies = []
+    for m in (3, 2, 1, 0):
+        wide, deep = pieces[m], pieces[4 + m]
         part = cols_of(t ^ m, wide.shape[0])
-        wide[:, 0:hid] = gate[part, :]
-        wide[:, hid:] = up[part, :]
-        deep[...] = down[:, cols_of(t ^ m, deep.shape[1])]
+        for source, target in (
+            (gate.at[part, :], wide.at[:, pl.ds(0, hid)]),
+            (up.at[part, :], wide.at[:, pl.ds(hid, hid)]),
+            (down.at[:, cols_of(t ^ m, deep.shape[1])], deep),
+        ):
+            copies.append(pltpu.make_async_copy(source, target, sems.at[len(copies)]))
+    for copy in copies:
+        copy.start()
+    for copy in copies:
+        copy.wait()
 
 
 def route_kernel(experts, routes, group_weight, logits, z, w, share0, share1, padded):
@@ -198,12 +215,11 @@
     return jnp.sum(block.astype(F32), axis=0, keepdims=True)
 
 
-def pack_kernel(capacity, tokens, p0, p1, p2, p3, z, *refs):
-    resid16, packed, wide = refs[-3:]
+def pack_kernel(capacity, tokens, own, came, last, z, resid16, packed, wide):
     t = lax.axis_index("tp")
-    quarter = p0.shape[1]
+    quarter = last.shape[1]
     total = tokens[:, cols_of(t, quarter)].astype(F32) + (
-        (p0[...].astype(F32) + p1[...].astype(F32)) + (p2[...].astype(F32) + p3[...].astype(F32))
+        (own[:, 0:quarter].astype(F32) + came[:, 0:quarter].astype(F32)) + last[...].astype(F32)
     )
     short = total.astype(BF16)
     resid16[...] = short
@@ -407,9 +423,9 @@
         sequence_state_imaginary,
         out_weight,
     )
-    *mix, new_re, new_im = call(
+    own, beside, new_re, new_im = call(
         state_kernel,
-        [piece] * 4 + [states] * 2,
+        [((rows, 2 * quarter), BF16)] * 2 + [states] * 2,
         [pltpu.SMEM(log_step.shape, F32)]
         + [pltpu.VMEM(x.shape, x.dtype) for x in state_inputs[1:]]
         + [pltpu.VMEM(states[0], F32)] * 2
@@ -417,15 +433,22 @@
         + [pltpu.SemaphoreType.DMA((15,))],
         20,
         [HBM] * 13,
-        [VMEM] * 4 + [HBM] * 2,
+        [VMEM] * 2 + [HBM] * 2,
     )(*state_inputs)
-    mix = [mix[0]] + [exchanged(mix[m], m) for m in (1, 2, 3)]
-    pieces = call(
-        reshard_kernel, [((quarter, 2 * hid), BF16)] * 4 + [((hid, quarter), BF16)] * 4
-    )(gate, up, down)
+    came_mix = exchanged(beside, 1)
+    (onward,) = call(half_kernel, [piece])(own, came_mix)
+    last_mix = exchanged(onward, 2)
+    reshard = call(
+        reshard_kernel,
+        [((quarter, 2 * hid), BF16)] * 4 + [((hid, quarter), BF16)] * 4,
+        [pltpu.SemaphoreType.DMA((12,))],
+        in_specs=[HBM] * 3,
+    )
+    pieces = reshard(gate, up, down)
     wide2 = exchanged(pieces[2], 2)
     wide3 = exchanged(pieces[3], 3)
-    moved = [pieces[0], exchanged(pieces[1], 1), wide2, wide3]
+    wide1 = exchanged(pieces[1], 1)
+    moved = [pieces[0], wide1, wide2, wide3]
     downs = [pieces[4]] + [exchanged(pieces[4 + m], m) for m in (1, 2, 3)]
     z, w, share0, share1 = call(
         functools.partial(route_kernel, ep),
@@ -439,7 +462,7 @@
         [wide],
         8,
         out_specs=[VMEM, FREE],
-    )(tokens, *mix, z)
+    )(tokens, own, came_mix, last_mix, z)
     across = exchanged(resid16, 2)
     arrived = lax.all_to_all(
         packed.reshape(ep, capacity * blocks, lanes), "ep", 0, 0, tiled=True

time: 99.3 us -> 99 us (level)
  Pallas kernels: 13.1 us -> 14.3 us
    pallas_call x10 -> x11, Pallas kernels: 13.1 us -> 14.3 us  [run(): pl.pallas_call(kernel, out_shape=tuple(out_shape), in_specs=specs, out_sp...]
    ppermute x20 -> x19, waiting for transfers between devices: 40.9 us -> 40.2 us  [exchanged(): return lax.ppermute(value, 'tp', [(i, i ^ mask) for i in range(4)])]
    ppermute x20 -> x19, starting transfers between devices: 19.8 us -> 19.2 us  [exchanged(): return lax.ppermute(value, 'tp', [(i, i ^ mask) for i in range(4)])]
  transfers between devices with their start and end apart: 22 -> 21, of which waited for: 12 -> 12; matrix products, arithmetic and copies ran while one was open for 0% -> 0% of each run, Pallas kernels for 4% -> 5%
where the time goes in v3:
time: 99 us; the launch traced here: 98.7 us
  starting transfers between devices  43.4 us (44%)
  waiting for transfers between devices  40.2 us (41%)
  Pallas kernels  14.3 us (14%)
    ppermute x19, waiting for transfers between devices, exchanged(): return lax.ppermute(value, 'tp', [(i, i ^ mask) for i in range(4)])  40.2 us
    ppermute x19, starting transfers between devices, exchanged(): return lax.ppermute(value, 'tp', [(i, i ^ mask) for i in range(4)])  19.2 us
    pallas_call x11, Pallas kernels, run(): pl.pallas_call(kernel, out_shape=tuple(out_shape), in_specs=specs, out_sp...  14.3 us
    all_to_all x1, starting transfers between devices, per_device(): lax.all_to_all(packed.reshape(ep, capacity * blocks, lanes), 'ep', 0, 0,...  12.6 us
    all_to_all x1, starting transfers between devices, per_device(): lax.all_to_all(sent.reshape(ep, capacity * blocks, lanes), 'ep', 0, 0, ti...  11.6 us
  transfers between devices with their start and end apart: 21, of which 12 were waited for; matrix products, arithmetic and copies ran while one was open for 0% of the time, Pallas kernels for 5%

profile of v3, /device:TPU:1, one launch (start us, length us, event | category | flops | bytes accessed | tf_op | source)
XLA Modules:
  0.0 98.7 jit_solution(15625408768040706145)
XLA Ops:
  0.7 4.1 %shard_map.247 = (bf16[96,1024]{1,0:T(8,128)(2,1)S(1)}, bf16[96,1024]{1,0:T(8,128)(2,1)S(1)}, f32[96,1024]{1,0:T(8,128)}, f32[96,1024]{1,0:T(8,128)}) custom-call(f32[16]{0:T(128)} %refs_0_.1, f32[16,64]{1,0:T(8,128)} %refs_1_.1, f32[16,16]{1,0:T(8,128)} %refs_2_.1, f32[256,64]{1,0:T(8,128)} %bitcast.26, f32[256,64]{1,0:T(8,128)} %bitcast.27, ...), custom_call_target="tpu_custom_call" | custom-call | tf_op jit(solution)/shard_map/pallas_call | solution.py:354
  4.8 3.3 %collective-permute-start = (bf16[96,1024]{1,0:T(8,128)(2,1)S(1)}, bf16[96,1024]{1,0:T(8,128)(2,1)S(1)}, u32[]{:S(2)}, u32[]{:S(2)}) collective-permute-start(bf16[96,1024]{1,0:T(8,128)(2,1)S(1)} %get-tuple-element.29), channel_id=1, source_target_pairs={{0,1},{1,0},{2,3},{3,2},{4,5},{5,4},{6,7},{7,6},{8,9},{9,8},{10,11... | collective-permute-start | bytes 589832 | tf_op jit(solution)/shard_map/ppermute | solution.py:42
  9.6 3.6 %collective-permute-done.1.last = bf16[96,512]{1,0:T(8,128)(2,1)S(1)} collective-permute-done((bf16[96,512]{1,0:T(8,128)(2,1)S(1)}, bf16[96,512]{1,0:T(8,128)(2,1)S(1)}, u32[]{:S(2)}, u32[]{:S(2)}) %collective-permute-start.1) | collective-permute-done | bytes 98336 | tf_op jit(solution)/shard_map/ppermute | solution.py:42
  13.2 1.1 %shard_map.250 = (bf16[96,512]{1,0:T(8,128)(2,1)S(1)}, bf16[1536,128]{1,0:T(8,128)(2,1)}) custom-call(bf16[96,2048]{1,0:T(8,128)(2,1)S(1)} %copy-done, bf16[96,1024]{1,0:T(8,128)(2,1)S(1)} %get-tuple-element.28.own, bf16[96,1024]{1,0:T(8,128)(2,1)S(1)} %collective-permute-done.came, bf16[96,512]{1,0:T(8,128)(2,1)S(1)} %collective-permute-done.1.last, ...), custom_call_target="tpu_custom_call" | custom-call | tf_op jit(solution)/shard_map/pallas_call | solution.py:354
  14.3 12.6 %all-to-all-start = ((bf16[64,24,128]{2,1,0:T(8,128)(2,1)}), bf16[64,24,128]{2,1,0:T(8,128)(2,1)S(1)}, u32[]{:S(2)}, u32[]{:S(2)}) async-start(bf16[64,24,128]{2,1,0:T(8,128)(2,1)} %bitcast.9), calls=%async_computation | async-start | bytes 786432 | tf_op jit(solution)/shard_map/all_to_all | solution.py:467
  26.9 1.6 %shard_map.251 = (bf16[512,256]{1,0:T(8,128)(2,1)S(1)}, bf16[512,256]{1,0:T(8,128)(2,1)S(1)}, bf16[512,256]{1,0:T(8,128)(2,1)S(1)}, bf16[512,256]{1,0:T(8,128)(2...) custom-call(bf16[2048,128]{1,0:T(8,128)(2,1)} %bitcast.23, ...), custom_call_target="tpu_custom_call" | custom-call | tf_op jit(solution)/shard_map/pallas_call | solution.py:354
  28.4 1.6 %collective-permute-start.2 = (bf16[512,256]{1,0:T(8,128)(2,1)S(1)}, bf16[512,256]{1,0:T(8,128)(2,1)S(1)}, u32[]{:S(2)}, u32[]{:S(2)}) collective-permute-start(bf16[512,256]{1,0:T(8,128)(2,1)S(1)} %get-tuple-element.33), channel_id=1, source_target_pairs={{0,1},{1,0},{2,3},{3,2},{4,5},{5,4},{6,7},{7,6},{8,9},{9,8},{10,11... | collective-permute-start | bytes 786440 | tf_op jit(solution)/shard_map/ppermute | solution.py:42
  30.4 1.4 %collective-permute-start.4 = (bf16[512,256]{1,0:T(8,128)(2,1)S(1)}, bf16[512,256]{1,0:T(8,128)(2,1)S(1)}, u32[]{:S(2)}, u32[]{:S(2)}) collective-permute-start(bf16[512,256]{1,0:T(8,128)(2,1)S(1)} %get-tuple-element.35), channel_id=1, source_target_pairs={{0,3},{1,2},{2,1},{3,0},{4,7},{5,6},{6,5},{7,4},{8,11},{9,10},{10,... | collective-permute-start | bytes 786440 | tf_op jit(solution)/shard_map/ppermute | solution.py:42
  31.8 8.9 %collective-permute-done.3.w2 = bf16[512,256]{1,0:T(8,128)(2,1)S(1)} collective-permute-done((bf16[512,256]{1,0:T(8,128)(2,1)S(1)}, bf16[512,256]{1,0:T(8,128)(2,1)S(1)}, u32[]{:S(2)}, u32[]{:S(2)}) %collective-permute-start.3) | collective-permute-done | bytes 262176 | tf_op jit(solution)/shard_map/ppermute | solution.py:42
  40.7 5.6 %collective-permute-done.4.w3 = bf16[512,256]{1,0:T(8,128)(2,1)S(1)} collective-permute-done((bf16[512,256]{1,0:T(8,128)(2,1)S(1)}, bf16[512,256]{1,0:T(8,128)(2,1)S(1)}, u32[]{:S(2)}, u32[]{:S(2)}) %collective-permute-start.4) | collective-permute-done | bytes 262176 | tf_op jit(solution)/shard_map/ppermute | solution.py:42
  47.7 1.4 %collective-permute-done.5.came = bf16[392,512]{1,0:T(8,128)(2,1)S(1)} collective-permute-done((bf16[392,512]{1,0:T(8,128)(2,1)S(1)}, bf16[392,512]{1,0:T(8,128)(2,1)S(1)}, u32[]{:S(2)}, u32[]{:S(2)}) %collective-permute-start.5) | collective-permute-done | bytes 401440 | tf_op jit(solution)/shard_map/ppermute | solution.py:42
  49.8 5.7 %collective-permute-done.6.last = bf16[400,256]{1,0:T(8,128)(2,1)S(1)} collective-permute-done((bf16[400,256]{1,0:T(8,128)(2,1)S(1)}, bf16[400,256]{1,0:T(8,128)(2,1)S(1)}, u32[]{:S(2)}, u32[]{:S(2)}) %collective-permute-start.6) | collective-permute-done | bytes 204832 | tf_op jit(solution)/shard_map/ppermute | solution.py:42
  56.5 1.4 %collective-permute-start.10 = (bf16[128,512]{1,0:T(8,128)(2,1)S(1)}, bf16[128,512]{1,0:T(8,128)(2,1)S(1)}, u32[]{:S(2)}, u32[]{:S(2)}) collective-permute-start(bf16[128,512]{1,0:T(8,128)(2,1)S(1)} %get-tuple-element.39), channel_id=1, source_target_pairs={{0,1},{1,0},{2,3},{3,2},{4,5},{5,4},{6,7},{7,6},{8,9},{9,8},{10,11... | collective-permute-start | bytes 393224 | tf_op jit(solution)/shard_map/ppermute | solution.py:42
  59.8 2.6 %collective-permute-start.9 = (bf16[384,128]{1,0:T(8,128)(2,1)S(1)}, bf16[384,128]{1,0:T(8,128)(2,1)S(1)}, u32[]{:S(2)}, u32[]{:S(2)}) collective-permute-start(bf16[384,128]{1,0:T(8,128)(2,1)S(1)} %collective-permute-done.8.h2), channel_id=1, source_target_pairs={{0,1},{1,0},{2,3},{3,2},{4,5},{5,4},{6,7},{7,6},{8,9},{9,8},{10,11... | collective-permute-start | bytes 294920 | tf_op jit(solution)/shard_map/ppermute | solution.py:42
  63.5 3.2 %collective-permute-done.12.w3 = bf16[128,512]{1,0:T(8,128)(2,1)S(1)} collective-permute-done((bf16[128,512]{1,0:T(8,128)(2,1)S(1)}, bf16[128,512]{1,0:T(8,128)(2,1)S(1)}, u32[]{:S(2)}, u32[]{:S(2)}) %collective-permute-start.12) | collective-permute-done | bytes 131104 | tf_op jit(solution)/shard_map/ppermute | solution.py:42
  66.7 1.4 %shard_map.255 = bf16[1536,128]{1,0:T(8,128)(2,1)} custom-call(bf16[384,128]{1,0:T(8,128)(2,1)S(1)} %shard_map.254.h0, bf16[384,128]{1,0:T(8,128)(2,1)S(1)} %collective-permute-done.7.h1, bf16[384,128]{1,0:T(8,128)(2,1)S(1)} %collective-permute-done.8.h2, bf16[384,128]{1,0:T(8,128)(2,1)S(1)} %collective-permute-done.9.h3, ...), custom_call_target="tpu_custom_call" | custom-call | tf_op jit(solution)/shard_map/pallas_call | solution.py:354
  68.1 11.6 %all-to-all-start.1 = ((bf16[64,24,128]{2,1,0:T(8,128)(2,1)}), bf16[64,24,128]{2,1,0:T(8,128)(2,1)S(1)}, u32[]{:S(2)}, u32[]{:S(2)}) async-start(bf16[64,24,128]{2,1,0:T(8,128)(2,1)} %bitcast.14), calls=%async_computation.1 | async-start | bytes 786432 | tf_op jit(solution)/shard_map/all_to_all | solution.py:503
  80.7 3.9 %collective-permute-done.14.a2 = bf16[96,512]{1,0:T(8,128)(2,1)S(1)} collective-permute-done((bf16[96,512]{1,0:T(8,128)(2,1)S(1)}, bf16[96,512]{1,0:T(8,128)(2,1)S(1)}, u32[]{:S(2)}, u32[]{:S(2)}) %collective-permute-start.14) | collective-permute-done | bytes 98336 | tf_op jit(solution)/shard_map/ppermute | solution.py:42
  84.6 1.6 %collective-permute-start.15 = (bf16[96,512]{1,0:T(8,128)(2,1)S(1)}, bf16[96,512]{1,0:T(8,128)(2,1)S(1)}, u32[]{:S(2)}, u32[]{:S(2)}) collective-permute-start(bf16[96,512]{1,0:T(8,128)(2,1)S(1)} %collective-permute-done.14.a2), channel_id=1, source_target_pairs={{0,1},{1,0},{2,3},{3,2},{4,5},{5,4},{6,7},{7,6},{8,9},{9,8},{10,11... | collective-permute-start | bytes 294920 | tf_op jit(solution)/shard_map/ppermute | solution.py:42
  87.1 3.4 %shard_map.256 = (bf16[96,512]{1,0:T(8,128)(2,1)S(1)}, bf16[96,512]{1,0:T(8,128)(2,1)S(1)}, bf16[96,512]{1,0:T(8,128)(2,1)S(1)}, bf16[96,512]{1,0:T(8,128)(2,1)S(1)}, f32[96,128]{1,0:T(8,128)S(1)}) custom-call(bf16[1,2048]{1,0:T(2,128)(2,1)S(1)} %reshape.55.gains, bf16[96,512]{1,0:T(8,128)(2,1)S(1)} %get-tuple-element.45.a0.resid, ...), custom_call_target="tpu_custom_call" | custom-call | tf_op jit(solution)/shard_map/pallas_call | solution.py:354
  91.2 1.5 %collective-permute-start.18 = (bf16[96,512]{1,0:T(8,128)(2,1)S(1)}, bf16[96,512]{1,0:T(8,128)(2,1)S(1)}, u32[]{:S(2)}, u32[]{:S(2)}) collective-permute-start(bf16[96,512]{1,0:T(8,128)(2,1)S(1)} %get-tuple-element.50), channel_id=1, source_target_pairs={{0,3},{1,2},{2,1},{3,0},{4,7},{5,6},{6,5},{7,4},{8,11},{9,10},{10,... | collective-permute-start | bytes 294920 | tf_op jit(solution)/shard_map/ppermute | solution.py:42
  92.8 2.4 %collective-permute-done.17.p2 = bf16[96,512]{1,0:T(8,128)(2,1)S(1)} collective-permute-done((bf16[96,512]{1,0:T(8,128)(2,1)S(1)}, bf16[96,512]{1,0:T(8,128)(2,1)S(1)}, u32[]{:S(2)}, u32[]{:S(2)}) %collective-permute-start.17) | collective-permute-done | bytes 98336 | tf_op jit(solution)/shard_map/ppermute | solution.py:42
  95.2 2.4 %collective-permute-done.18.p3 = bf16[96,512]{1,0:T(8,128)(2,1)S(1)} collective-permute-done((bf16[96,512]{1,0:T(8,128)(2,1)S(1)}, bf16[96,512]{1,0:T(8,128)(2,1)S(1)}, u32[]{:S(2)}, u32[]{:S(2)}) %collective-permute-start.18) | collective-permute-done | bytes 98336 | tf_op jit(solution)/shard_map/ppermute | solution.py:42
  97.6 1.1 %shard_map.257 = bf16[96,512]{1,0:T(8,128)(2,1)} custom-call(bf16[1536,128]{1,0:T(8,128)(2,1)S(1)} %bitcast.18, bf16[192,384]{1,0:T(8,128)(2,1)S(1)} %get-tuple-element.42.w, f32[96,128]{1,0:T(8,128)S(1)} %get-tuple-element.43.share0, f32[96,128]{1,0:T(8,128)S(1)} %get-tuple-element.44.share1, bf16[96,512]{1,0:T(8,128)(2,1)S(1)} %get-tuple-element.45.a0.resid, ...), custom_call_target="tpu_custom_call" | custom-call | tf_op jit(solution)/shard_map/pallas_call | solution.py:354
  (43 shorter events, 10.5 us)
Async XLA Ops:
  0.7 12.6 %copy-start = (bf16[96,2048]{1,0:T(8,128)(2,1)S(1)}, bf16[96,2048]{1,0:T(8,128)(2,1)}, u32[]{:S(2)}) copy-start(bf16[96,2048]{1,0:T(8,128)(2,1)} %tokens.1) | copy-start | bytes 1179652
  4.7 27.0 %copy-start.4 = (bf16[2048]{0:T(1024)(128)(2,1)S(1)}, bf16[2048]{0:T(1024)(128)(2,1)}, u32[]{:S(2)}) copy-start(bf16[2048]{0:T(1024)(128)(2,1)} %param.37) | copy-start | bytes 12292
  4.8 4.4 %collective-permute-start = (bf16[96,1024]{1,0:T(8,128)(2,1)S(1)}, bf16[96,1024]{1,0:T(8,128)(2,1)S(1)}, u32[]{:S(2)}, u32[]{:S(2)}) collective-permute-start(bf16[96,1024]{1,0:T(8,128)(2,1)S(1)} %get-tuple-element.29), channel_id=1, source_target_pairs={{0,1},{1,0},{2,3},{3,2},{4,5},{5,4},{6,7},{7,6},{8,9},{9,8},{10,11... | collective-permute-start | bytes 589832 | tf_op jit(solution)/shard_map/ppermute | solution.py:42
  9.1 4.1 %collective-permute-start.1 = (bf16[96,512]{1,0:T(8,128)(2,1)S(1)}, bf16[96,512]{1,0:T(8,128)(2,1)S(1)}, u32[]{:S(2)}, u32[]{:S(2)}) collective-permute-start(bf16[96,512]{1,0:T(8,128)(2,1)S(1)} %shard_map.248), channel_id=1, source_target_pairs={{0,2},{1,3},{2,0},{3,1},{4,6},{5,7},{6,4},{7,5},{8,10},{9,11},{10,... | collective-permute-start | bytes 294920 | tf_op jit(solution)/shard_map/ppermute | solution.py:42
  14.3 32.0 %all-to-all-start = ((bf16[64,24,128]{2,1,0:T(8,128)(2,1)}), bf16[64,24,128]{2,1,0:T(8,128)(2,1)S(1)}, u32[]{:S(2)}, u32[]{:S(2)}) async-start(bf16[64,24,128]{2,1,0:T(8,128)(2,1)} %bitcast.9), calls=%async_computation | async-start | bytes 786432 | tf_op jit(solution)/shard_map/all_to_all | solution.py:467
  28.4 3.3 %collective-permute-start.2 = (bf16[512,256]{1,0:T(8,128)(2,1)S(1)}, bf16[512,256]{1,0:T(8,128)(2,1)S(1)}, u32[]{:S(2)}, u32[]{:S(2)}) collective-permute-start(bf16[512,256]{1,0:T(8,128)(2,1)S(1)} %get-tuple-element.33), channel_id=1, source_target_pairs={{0,1},{1,0},{2,3},{3,2},{4,5},{5,4},{6,7},{7,6},{8,9},{9,8},{10,11... | collective-permute-start | bytes 786440 | tf_op jit(solution)/shard_map/ppermute | solution.py:42
  30.0 10.6 %collective-permute-start.3 = (bf16[512,256]{1,0:T(8,128)(2,1)S(1)}, bf16[512,256]{1,0:T(8,128)(2,1)S(1)}, u32[]{:S(2)}, u32[]{:S(2)}) collective-permute-start(bf16[512,256]{1,0:T(8,128)(2,1)S(1)} %get-tuple-element.34), channel_id=1, source_target_pairs={{0,2},{1,3},{2,0},{3,1},{4,6},{5,7},{6,4},{7,5},{8,10},{9,11},{10,... | collective-permute-start | bytes 786440 | tf_op jit(solution)/shard_map/ppermute | solution.py:42
  30.4 15.9 %collective-permute-start.4 = (bf16[512,256]{1,0:T(8,128)(2,1)S(1)}, bf16[512,256]{1,0:T(8,128)(2,1)S(1)}, u32[]{:S(2)}, u32[]{:S(2)}) collective-permute-start(bf16[512,256]{1,0:T(8,128)(2,1)S(1)} %get-tuple-element.35), channel_id=1, source_target_pairs={{0,3},{1,2},{2,1},{3,0},{4,7},{5,6},{6,5},{7,4},{8,11},{9,10},{10,... | collective-permute-start | bytes 786440 | tf_op jit(solution)/shard_map/ppermute | solution.py:42
  47.2 1.8 %collective-permute-start.5 = (bf16[392,512]{1,0:T(8,128)(2,1)S(1)}, bf16[392,512]{1,0:T(8,128)(2,1)S(1)}, u32[]{:S(2)}, u32[]{:S(2)}) collective-permute-start(bf16[392,512]{1,0:T(8,128)(2,1)S(1)} %get-tuple-element.37), channel_id=1, source_target_pairs={{0,1},{1,0},{2,3},{3,2},{4,5},{5,4},{6,7},{7,6},{8,9},{9,8},{10,11... | collective-permute-start | bytes 1204232 | tf_op jit(solution)/shard_map/ppermute | solution.py:42
  49.2 37.0 %copy-start.5 = (bf16[2048]{0:T(1024)(128)(2,1)S(1)}, bf16[2048]{0:T(1024)(128)(2,1)}, u32[]{:S(2)}) copy-start(bf16[2048]{0:T(1024)(128)(2,1)} %param.47) | copy-start | bytes 12292
  49.2 6.4 %collective-permute-start.6 = (bf16[400,256]{1,0:T(8,128)(2,1)S(1)}, bf16[400,256]{1,0:T(8,128)(2,1)S(1)}, u32[]{:S(2)}, u32[]{:S(2)}) collective-permute-start(bf16[400,256]{1,0:T(8,128)(2,1)S(1)} %shard_map.253), channel_id=1, source_target_pairs={{0,2},{1,3},{2,0},{3,1},{4,6},{5,7},{6,4},{7,5},{8,10},{9,11},{10,... | collective-permute-start | bytes 614408 | tf_op jit(solution)/shard_map/ppermute | solution.py:42
  55.8 4.0 %collective-permute-start.8 = (bf16[384,128]{1,0:T(8,128)(2,1)S(1)}, bf16[384,128]{1,0:T(8,128)(2,1)S(1)}, u32[]{:S(2)}, u32[]{:S(2)}) collective-permute-start(bf16[384,128]{1,0:T(8,128)(2,1)S(1)} %shard_map.254.h0), channel_id=1, source_target_pairs={{0,2},{1,3},{2,0},{3,1},{4,6},{5,7},{6,4},{7,5},{8,10},{9,11},{10,... | collective-permute-start | bytes 294920 | tf_op jit(solution)/shard_map/ppermute | solution.py:42
  56.5 5.9 %collective-permute-start.10 = (bf16[128,512]{1,0:T(8,128)(2,1)S(1)}, bf16[128,512]{1,0:T(8,128)(2,1)S(1)}, u32[]{:S(2)}, u32[]{:S(2)}) collective-permute-start(bf16[128,512]{1,0:T(8,128)(2,1)S(1)} %get-tuple-element.39), channel_id=1, source_target_pairs={{0,1},{1,0},{2,3},{3,2},{4,5},{5,4},{6,7},{7,6},{8,9},{9,8},{10,11... | collective-permute-start | bytes 393224 | tf_op jit(solution)/shard_map/ppermute | solution.py:42
  58.0 5.5 %collective-permute-start.11 = (bf16[128,512]{1,0:T(8,128)(2,1)S(1)}, bf16[128,512]{1,0:T(8,128)(2,1)S(1)}, u32[]{:S(2)}, u32[]{:S(2)}) collective-permute-start(bf16[128,512]{1,0:T(8,128)(2,1)S(1)} %get-tuple-element.40), channel_id=1, source_target_pairs={{0,2},{1,3},{2,0},{3,1},{4,6},{5,7},{6,4},{7,5},{8,10},{9,11},{10,... | collective-permute-start | bytes 393224 | tf_op jit(solution)/shard_map/ppermute | solution.py:42
  58.9 7.8 %collective-permute-start.12 = (bf16[128,512]{1,0:T(8,128)(2,1)S(1)}, bf16[128,512]{1,0:T(8,128)(2,1)S(1)}, u32[]{:S(2)}, u32[]{:S(2)}) collective-permute-start(bf16[128,512]{1,0:T(8,128)(2,1)S(1)} %get-tuple-element.41), channel_id=1, source_target_pairs={{0,3},{1,2},{2,1},{3,0},{4,7},{5,6},{6,5},{7,4},{8,11},{9,10},{10,... | collective-permute-start | bytes 393224 | tf_op jit(solution)/shard_map/ppermute | solution.py:42
  59.6 7.1 %collective-permute-start.7 = (bf16[384,128]{1,0:T(8,128)(2,1)S(1)}, bf16[384,128]{1,0:T(8,128)(2,1)S(1)}, u32[]{:S(2)}, u32[]{:S(2)}) collective-permute-start(bf16[384,128]{1,0:T(8,128)(2,1)S(1)} %shard_map.254.h0), channel_id=1, source_target_pairs={{0,1},{1,0},{2,3},{3,2},{4,5},{5,4},{6,7},{7,6},{8,9},{9,8},{10,11... | collective-permute-start | bytes 294920 | tf_op jit(solution)/shard_map/ppermute | solution.py:42
  59.8 6.9 %collective-permute-start.9 = (bf16[384,128]{1,0:T(8,128)(2,1)S(1)}, bf16[384,128]{1,0:T(8,128)(2,1)S(1)}, u32[]{:S(2)}, u32[]{:S(2)}) collective-permute-start(bf16[384,128]{1,0:T(8,128)(2,1)S(1)} %collective-permute-done.8.h2), channel_id=1, source_target_pairs={{0,1},{1,0},{2,3},{3,2},{4,5},{5,4},{6,7},{7,6},{8,9},{9,8},{10,11... | collective-permute-start | bytes 294920 | tf_op jit(solution)/shard_map/ppermute | solution.py:42
  68.1 29.5 %all-to-all-start.1 = ((bf16[64,24,128]{2,1,0:T(8,128)(2,1)}), bf16[64,24,128]{2,1,0:T(8,128)(2,1)S(1)}, u32[]{:S(2)}, u32[]{:S(2)}) async-start(bf16[64,24,128]{2,1,0:T(8,128)(2,1)} %bitcast.14), calls=%async_computation.1 | async-start | bytes 786432 | tf_op jit(solution)/shard_map/all_to_all | solution.py:503
  79.7 4.9 %collective-permute-start.14 = (bf16[96,512]{1,0:T(8,128)(2,1)S(1)}, bf16[96,512]{1,0:T(8,128)(2,1)S(1)}, u32[]{:S(2)}, u32[]{:S(2)}) collective-permute-start(bf16[96,512]{1,0:T(8,128)(2,1)S(1)} %get-tuple-element.45.a0.resid), channel_id=1, source_target_pairs={{0,2},{1,3},{2,0},{3,1},{4,6},{5,7},{6,4},{7,5},{8,10},{9,11},{10,... | collective-permute-start | bytes 294920 | tf_op jit(solution)/shard_map/ppermute | solution.py:42
  80.0 6.2 %collective-permute-start.13 = (bf16[96,512]{1,0:T(8,128)(2,1)S(1)}, bf16[96,512]{1,0:T(8,128)(2,1)S(1)}, u32[]{:S(2)}, u32[]{:S(2)}) collective-permute-start(bf16[96,512]{1,0:T(8,128)(2,1)S(1)} %get-tuple-element.45.a0.resid), channel_id=1, source_target_pairs={{0,1},{1,0},{2,3},{3,2},{4,5},{5,4},{6,7},{7,6},{8,9},{9,8},{10,11... | collective-permute-start | bytes 294920 | tf_op jit(solution)/shard_map/ppermute | solution.py:42
  84.6 2.5 %collective-permute-start.15 = (bf16[96,512]{1,0:T(8,128)(2,1)S(1)}, bf16[96,512]{1,0:T(8,128)(2,1)S(1)}, u32[]{:S(2)}, u32[]{:S(2)}) collective-permute-start(bf16[96,512]{1,0:T(8,128)(2,1)S(1)} %collective-permute-done.14.a2), channel_id=1, source_target_pairs={{0,1},{1,0},{2,3},{3,2},{4,5},{5,4},{6,7},{7,6},{8,9},{9,8},{10,11... | collective-permute-start | bytes 294920 | tf_op jit(solution)/shard_map/ppermute | solution.py:42
  90.5 2.2 %collective-permute-start.16 = (bf16[96,512]{1,0:T(8,128)(2,1)S(1)}, bf16[96,512]{1,0:T(8,128)(2,1)S(1)}, u32[]{:S(2)}, u32[]{:S(2)}) collective-permute-start(bf16[96,512]{1,0:T(8,128)(2,1)S(1)} %get-tuple-element.48), channel_id=1, source_target_pairs={{0,1},{1,0},{2,3},{3,2},{4,5},{5,4},{6,7},{7,6},{8,9},{9,8},{10,11... | collective-permute-start | bytes 294920 | tf_op jit(solution)/shard_map/ppermute | solution.py:42
  91.0 4.2 %collective-permute-start.17 = (bf16[96,512]{1,0:T(8,128)(2,1)S(1)}, bf16[96,512]{1,0:T(8,128)(2,1)S(1)}, u32[]{:S(2)}, u32[]{:S(2)}) collective-permute-start(bf16[96,512]{1,0:T(8,128)(2,1)S(1)} %get-tuple-element.49), channel_id=1, source_target_pairs={{0,2},{1,3},{2,0},{3,1},{4,6},{5,7},{6,4},{7,5},{8,10},{9,11},{10,... | collective-permute-start | bytes 294920 | tf_op jit(solution)/shard_map/ppermute | solution.py:42
  91.2 6.4 %collective-permute-start.18 = (bf16[96,512]{1,0:T(8,128)(2,1)S(1)}, bf16[96,512]{1,0:T(8,128)(2,1)S(1)}, u32[]{:S(2)}, u32[]{:S(2)}) collective-permute-start(bf16[96,512]{1,0:T(8,128)(2,1)S(1)} %get-tuple-element.50), channel_id=1, source_target_pairs={{0,3},{1,2},{2,1},{3,0},{4,7},{5,6},{6,5},{7,4},{8,11},{9,10},{10,... | collective-permute-start | bytes 294920 | tf_op jit(solution)/shard_map/ppermute | solution.py:42
  (3 other events, 25.8 us)

commit v4 on v3

--- a/solution.py
+++ b/solution.py
@@ -142,24 +142,14 @@
     onward[...] = (own[:, quarter:].astype(F32) + came[:, quarter:].astype(F32)).astype(BF16)
 
 
-def reshard_kernel(gate, up, down, *refs):
-    pieces, sems = refs[:8], refs[8]
+def reshard_kernel(gate, up, down, *pieces):
     t = lax.axis_index("tp")
     hid = gate.shape[1]
-    copies = []
-    for m in (3, 2, 1, 0):
-        wide, deep = pieces[m], pieces[4 + m]
+    for m, (wide, deep) in enumerate(zip(pieces[:4], pieces[4:])):
         part = cols_of(t ^ m, wide.shape[0])
-        for source, target in (
-            (gate.at[part, :], wide.at[:, pl.ds(0, hid)]),
-            (up.at[part, :], wide.at[:, pl.ds(hid, hid)]),
-            (down.at[:, cols_of(t ^ m, deep.shape[1])], deep),
-        ):
-            copies.append(pltpu.make_async_copy(source, target, sems.at[len(copies)]))
-    for copy in copies:
-        copy.start()
-    for copy in copies:
-        copy.wait()
+        wide[:, 0:hid] = gate[part, :]
+        wide[:, hid:] = up[part, :]
+        deep[...] = down[:, cols_of(t ^ m, deep.shape[1])]
 
 
 def route_kernel(experts, routes, group_weight, logits, z, w, share0, share1, padded):
@@ -438,12 +428,7 @@
     came_mix = exchanged(beside, 1)
     (onward,) = call(half_kernel, [piece])(own, came_mix)
     last_mix = exchanged(onward, 2)
-    reshard = call(
-        reshard_kernel,
-        [((quarter, 2 * hid), BF16)] * 4 + [((hid, quarter), BF16)] * 4,
-        [pltpu.SemaphoreType.DMA((12,))],
-        in_specs=[HBM] * 3,
-    )
+    reshard = call(reshard_kernel, [((quarter, 2 * hid), BF16)] * 4 + [((hid, quarter), BF16)] * 4)
     pieces = reshard(gate, up, down)
     wide2 = exchanged(pieces[2], 2)
     wide3 = exchanged(pieces[3], 3)

time: 99 us -> 98.2 us (level)
  Pallas kernels: 14.3 us -> 12.9 us
    pallas_call x11, Pallas kernels: 14.3 us -> 12.9 us  [run(): pl.pallas_call(kernel, out_shape=tuple(out_shape), in_specs=specs, out_sp...]
  transfers between devices with their start and end apart: 21 -> 21, of which waited for: 12 -> 12; matrix products, arithmetic and copies ran while one was open for 0% -> 0% of each run, Pallas kernels for 5% -> 4%
where the time goes in v4:
time: 98.2 us; the launch traced here: 98 us
  starting transfers between devices  43.5 us (44%)
  waiting for transfers between devices  40.6 us (41%)
  Pallas kernels  12.9 us (13%)
    ppermute x19, waiting for transfers between devices, exchanged(): return lax.ppermute(value, 'tp', [(i, i ^ mask) for i in range(4)])  40.6 us
    ppermute x19, starting transfers between devices, exchanged(): return lax.ppermute(value, 'tp', [(i, i ^ mask) for i in range(4)])  19.1 us
    pallas_call x11, Pallas kernels, run(): pl.pallas_call(kernel, out_shape=tuple(out_shape), in_specs=specs, out_sp...  12.9 us
    all_to_all x1, starting transfers between devices, per_device(): lax.all_to_all(packed.reshape(ep, capacity * blocks, lanes), 'ep', 0, 0,...  12.6 us
    all_to_all x1, starting transfers between devices, per_device(): lax.all_to_all(sent.reshape(ep, capacity * blocks, lanes), 'ep', 0, 0, ti...  11.8 us
  transfers between devices with their start and end apart: 21, of which 12 were waited for; matrix products, arithmetic and copies ran while one was open for 0% of the time, Pallas kernels for 4%

profile of v4, /device:TPU:1, one launch (start us, length us, event | category | flops | bytes accessed | tf_op | source)
XLA Modules:
  0.0 98.0 jit_solution(3966926815523870381)
XLA Ops:
  0.7 4.1 %shard_map.247 = (bf16[96,1024]{1,0:T(8,128)(2,1)S(1)}, bf16[96,1024]{1,0:T(8,128)(2,1)S(1)}, f32[96,1024]{1,0:T(8,128)}, f32[96,1024]{1,0:T(8,128)}) custom-call(f32[16]{0:T(128)} %refs_0_.1, f32[16,64]{1,0:T(8,128)} %refs_1_.1, f32[16,16]{1,0:T(8,128)} %refs_2_.1, f32[256,64]{1,0:T(8,128)} %bitcast.26, f32[256,64]{1,0:T(8,128)} %bitcast.27, ...), custom_call_target="tpu_custom_call" | custom-call | tf_op jit(solution)/shard_map/pallas_call | solution.py:344
  4.8 3.3 %collective-permute-start = (bf16[96,1024]{1,0:T(8,128)(2,1)S(1)}, bf16[96,1024]{1,0:T(8,128)(2,1)S(1)}, u32[]{:S(2)}, u32[]{:S(2)}) collective-permute-start(bf16[96,1024]{1,0:T(8,128)(2,1)S(1)} %get-tuple-element.29), channel_id=1, source_target_pairs={{0,1},{1,0},{2,3},{3,2},{4,5},{5,4},{6,7},{7,6},{8,9},{9,8},{10,11... | collective-permute-start | bytes 589832 | tf_op jit(solution)/shard_map/ppermute | solution.py:42
  9.6 3.6 %collective-permute-done.1.last = bf16[96,512]{1,0:T(8,128)(2,1)S(1)} collective-permute-done((bf16[96,512]{1,0:T(8,128)(2,1)S(1)}, bf16[96,512]{1,0:T(8,128)(2,1)S(1)}, u32[]{:S(2)}, u32[]{:S(2)}) %collective-permute-start.1) | collective-permute-done | bytes 98336 | tf_op jit(solution)/shard_map/ppermute | solution.py:42
  13.3 1.1 %shard_map.250 = (bf16[96,512]{1,0:T(8,128)(2,1)S(1)}, bf16[1536,128]{1,0:T(8,128)(2,1)}) custom-call(bf16[96,2048]{1,0:T(8,128)(2,1)S(1)} %copy-done, bf16[96,1024]{1,0:T(8,128)(2,1)S(1)} %get-tuple-element.28.own, bf16[96,1024]{1,0:T(8,128)(2,1)S(1)} %collective-permute-done.came, bf16[96,512]{1,0:T(8,128)(2,1)S(1)} %collective-permute-done.1.last, ...), custom_call_target="tpu_custom_call" | custom-call | tf_op jit(solution)/shard_map/pallas_call | solution.py:344
  14.3 12.6 %all-to-all-start = ((bf16[64,24,128]{2,1,0:T(8,128)(2,1)}), bf16[64,24,128]{2,1,0:T(8,128)(2,1)S(1)}, u32[]{:S(2)}, u32[]{:S(2)}) async-start(bf16[64,24,128]{2,1,0:T(8,128)(2,1)} %bitcast.9), calls=%async_computation | async-start | bytes 786432 | tf_op jit(solution)/shard_map/all_to_all | solution.py:452
  27.2 1.6 %collective-permute-start.2 = (bf16[512,256]{1,0:T(8,128)(2,1)S(1)}, bf16[512,256]{1,0:T(8,128)(2,1)S(1)}, u32[]{:S(2)}, u32[]{:S(2)}) collective-permute-start(bf16[512,256]{1,0:T(8,128)(2,1)S(1)} %get-tuple-element.33), channel_id=1, source_target_pairs={{0,1},{1,0},{2,3},{3,2},{4,5},{5,4},{6,7},{7,6},{8,9},{9,8},{10,11... | collective-permute-start | bytes 786440 | tf_op jit(solution)/shard_map/ppermute | solution.py:42
  29.1 1.4 %collective-permute-start.4 = (bf16[512,256]{1,0:T(8,128)(2,1)S(1)}, bf16[512,256]{1,0:T(8,128)(2,1)S(1)}, u32[]{:S(2)}, u32[]{:S(2)}) collective-permute-start(bf16[512,256]{1,0:T(8,128)(2,1)S(1)} %get-tuple-element.35), channel_id=1, source_target_pairs={{0,3},{1,2},{2,1},{3,0},{4,7},{5,6},{6,5},{7,4},{8,11},{9,10},{10,... | collective-permute-start | bytes 786440 | tf_op jit(solution)/shard_map/ppermute | solution.py:42
  30.5 9.2 %collective-permute-done.3.w2 = bf16[512,256]{1,0:T(8,128)(2,1)S(1)} collective-permute-done((bf16[512,256]{1,0:T(8,128)(2,1)S(1)}, bf16[512,256]{1,0:T(8,128)(2,1)S(1)}, u32[]{:S(2)}, u32[]{:S(2)}) %collective-permute-start.3) | collective-permute-done | bytes 262176 | tf_op jit(solution)/shard_map/ppermute | solution.py:42
  39.7 5.7 %collective-permute-done.4.w3 = bf16[512,256]{1,0:T(8,128)(2,1)S(1)} collective-permute-done((bf16[512,256]{1,0:T(8,128)(2,1)S(1)}, bf16[512,256]{1,0:T(8,128)(2,1)S(1)}, u32[]{:S(2)}, u32[]{:S(2)}) %collective-permute-start.4) | collective-permute-done | bytes 262176 | tf_op jit(solution)/shard_map/ppermute | solution.py:42
  46.8 1.4 %collective-permute-done.5.came = bf16[392,512]{1,0:T(8,128)(2,1)S(1)} collective-permute-done((bf16[392,512]{1,0:T(8,128)(2,1)S(1)}, bf16[392,512]{1,0:T(8,128)(2,1)S(1)}, u32[]{:S(2)}, u32[]{:S(2)}) %collective-permute-start.5) | collective-permute-done | bytes 401440 | tf_op jit(solution)/shard_map/ppermute | solution.py:42
  49.2 5.4 %collective-permute-done.6.last = bf16[400,256]{1,0:T(8,128)(2,1)S(1)} collective-permute-done((bf16[400,256]{1,0:T(8,128)(2,1)S(1)}, bf16[400,256]{1,0:T(8,128)(2,1)S(1)}, u32[]{:S(2)}, u32[]{:S(2)}) %collective-permute-start.6) | collective-permute-done | bytes 204832 | tf_op jit(solution)/shard_map/ppermute | solution.py:42
  55.9 1.5 %collective-permute-start.10 = (bf16[128,512]{1,0:T(8,128)(2,1)S(1)}, bf16[128,512]{1,0:T(8,128)(2,1)S(1)}, u32[]{:S(2)}, u32[]{:S(2)}) collective-permute-start(bf16[128,512]{1,0:T(8,128)(2,1)S(1)} %get-tuple-element.39), channel_id=1, source_target_pairs={{0,1},{1,0},{2,3},{3,2},{4,5},{5,4},{6,7},{7,6},{8,9},{9,8},{10,11... | collective-permute-start | bytes 393224 | tf_op jit(solution)/shard_map/ppermute | solution.py:42
  59.2 2.0 %collective-permute-start.9 = (bf16[384,128]{1,0:T(8,128)(2,1)S(1)}, bf16[384,128]{1,0:T(8,128)(2,1)S(1)}, u32[]{:S(2)}, u32[]{:S(2)}) collective-permute-start(bf16[384,128]{1,0:T(8,128)(2,1)S(1)} %collective-permute-done.8.h2), channel_id=1, source_target_pairs={{0,1},{1,0},{2,3},{3,2},{4,5},{5,4},{6,7},{7,6},{8,9},{9,8},{10,11... | collective-permute-start | bytes 294920 | tf_op jit(solution)/shard_map/ppermute | solution.py:42
  61.2 1.7 %collective-permute-done.11.w2 = bf16[128,512]{1,0:T(8,128)(2,1)S(1)} collective-permute-done((bf16[128,512]{1,0:T(8,128)(2,1)S(1)}, bf16[128,512]{1,0:T(8,128)(2,1)S(1)}, u32[]{:S(2)}, u32[]{:S(2)}) %collective-permute-start.11) | collective-permute-done | bytes 131104 | tf_op jit(solution)/shard_map/ppermute | solution.py:42
  62.9 2.9 %collective-permute-done.12.w3 = bf16[128,512]{1,0:T(8,128)(2,1)S(1)} collective-permute-done((bf16[128,512]{1,0:T(8,128)(2,1)S(1)}, bf16[128,512]{1,0:T(8,128)(2,1)S(1)}, u32[]{:S(2)}, u32[]{:S(2)}) %collective-permute-start.12) | collective-permute-done | bytes 131104 | tf_op jit(solution)/shard_map/ppermute | solution.py:42
  65.8 1.4 %shard_map.255 = bf16[1536,128]{1,0:T(8,128)(2,1)} custom-call(bf16[384,128]{1,0:T(8,128)(2,1)S(1)} %shard_map.254.h0, bf16[384,128]{1,0:T(8,128)(2,1)S(1)} %collective-permute-done.7.h1, bf16[384,128]{1,0:T(8,128)(2,1)S(1)} %collective-permute-done.8.h2, bf16[384,128]{1,0:T(8,128)(2,1)S(1)} %collective-permute-done.9.h3, ...), custom_call_target="tpu_custom_call" | custom-call | tf_op jit(solution)/shard_map/pallas_call | solution.py:344
  67.2 11.8 %all-to-all-start.1 = ((bf16[64,24,128]{2,1,0:T(8,128)(2,1)}), bf16[64,24,128]{2,1,0:T(8,128)(2,1)S(1)}, u32[]{:S(2)}, u32[]{:S(2)}) async-start(bf16[64,24,128]{2,1,0:T(8,128)(2,1)} %bitcast.14), calls=%async_computation.1 | async-start | bytes 786432 | tf_op jit(solution)/shard_map/all_to_all | solution.py:488
  80.0 3.9 %collective-permute-done.14.a2 = bf16[96,512]{1,0:T(8,128)(2,1)S(1)} collective-permute-done((bf16[96,512]{1,0:T(8,128)(2,1)S(1)}, bf16[96,512]{1,0:T(8,128)(2,1)S(1)}, u32[]{:S(2)}, u32[]{:S(2)}) %collective-permute-start.14) | collective-permute-done | bytes 98336 | tf_op jit(solution)/shard_map/ppermute | solution.py:42
  83.9 1.5 %collective-permute-start.15 = (bf16[96,512]{1,0:T(8,128)(2,1)S(1)}, bf16[96,512]{1,0:T(8,128)(2,1)S(1)}, u32[]{:S(2)}, u32[]{:S(2)}) collective-permute-start(bf16[96,512]{1,0:T(8,128)(2,1)S(1)} %collective-permute-done.14.a2), channel_id=1, source_target_pairs={{0,1},{1,0},{2,3},{3,2},{4,5},{5,4},{6,7},{7,6},{8,9},{9,8},{10,11... | collective-permute-start | bytes 294920 | tf_op jit(solution)/shard_map/ppermute | solution.py:42
  86.4 3.4 %shard_map.256 = (bf16[96,512]{1,0:T(8,128)(2,1)S(1)}, bf16[96,512]{1,0:T(8,128)(2,1)S(1)}, bf16[96,512]{1,0:T(8,128)(2,1)S(1)}, bf16[96,512]{1,0:T(8,128)(2,1)S(1)}, f32[96,128]{1,0:T(8,128)S(1)}) custom-call(bf16[1,2048]{1,0:T(2,128)(2,1)S(1)} %reshape.55.gains, bf16[96,512]{1,0:T(8,128)(2,1)S(1)} %get-tuple-element.45.a0.resid, ...), custom_call_target="tpu_custom_call" | custom-call | tf_op jit(solution)/shard_map/pallas_call | solution.py:344
  90.4 1.6 %collective-permute-start.18 = (bf16[96,512]{1,0:T(8,128)(2,1)S(1)}, bf16[96,512]{1,0:T(8,128)(2,1)S(1)}, u32[]{:S(2)}, u32[]{:S(2)}) collective-permute-start(bf16[96,512]{1,0:T(8,128)(2,1)S(1)} %get-tuple-element.50), channel_id=1, source_target_pairs={{0,3},{1,2},{2,1},{3,0},{4,7},{5,6},{6,5},{7,4},{8,11},{9,10},{10,... | collective-permute-start | bytes 294920 | tf_op jit(solution)/shard_map/ppermute | solution.py:42
  92.0 2.4 %collective-permute-done.17.p2 = bf16[96,512]{1,0:T(8,128)(2,1)S(1)} collective-permute-done((bf16[96,512]{1,0:T(8,128)(2,1)S(1)}, bf16[96,512]{1,0:T(8,128)(2,1)S(1)}, u32[]{:S(2)}, u32[]{:S(2)}) %collective-permute-start.17) | collective-permute-done | bytes 98336 | tf_op jit(solution)/shard_map/ppermute | solution.py:42
  94.4 2.4 %collective-permute-done.18.p3 = bf16[96,512]{1,0:T(8,128)(2,1)S(1)} collective-permute-done((bf16[96,512]{1,0:T(8,128)(2,1)S(1)}, bf16[96,512]{1,0:T(8,128)(2,1)S(1)}, u32[]{:S(2)}, u32[]{:S(2)}) %collective-permute-start.18) | collective-permute-done | bytes 98336 | tf_op jit(solution)/shard_map/ppermute | solution.py:42
  96.9 1.1 %shard_map.257 = bf16[96,512]{1,0:T(8,128)(2,1)} custom-call(bf16[1536,128]{1,0:T(8,128)(2,1)S(1)} %bitcast.18, bf16[192,384]{1,0:T(8,128)(2,1)S(1)} %get-tuple-element.42.w, f32[96,128]{1,0:T(8,128)S(1)} %get-tuple-element.43.share0, f32[96,128]{1,0:T(8,128)S(1)} %get-tuple-element.44.share1, bf16[96,512]{1,0:T(8,128)(2,1)S(1)} %get-tuple-element.45.a0.resid, ...), custom_call_target="tpu_custom_call" | custom-call | tf_op jit(solution)/shard_map/pallas_call | solution.py:344
  (49 shorter events, 10.2 us)
Async XLA Ops:
  4.7 22.2 %copy-start.1 = (bf16[1,2048,128]{2,1,0:T(8,128)(2,1)S(1)}, bf16[1,2048,128]{2,1,0:T(8,128)(2,1)}, u32[]{:S(2)}) copy-start(bf16[1,2048,128]{2,1,0:T(8,128)(2,1)} %param.41) | copy-start | bytes 1572868
  4.8 25.7 %copy-start.7 = (bf16[2048]{0:T(1024)(128)(2,1)S(1)}, bf16[2048]{0:T(1024)(128)(2,1)}, u32[]{:S(2)}) copy-start(bf16[2048]{0:T(1024)(128)(2,1)} %param.37) | copy-start | bytes 12292
  4.8 4.4 %collective-permute-start = (bf16[96,1024]{1,0:T(8,128)(2,1)S(1)}, bf16[96,1024]{1,0:T(8,128)(2,1)S(1)}, u32[]{:S(2)}, u32[]{:S(2)}) collective-permute-start(bf16[96,1024]{1,0:T(8,128)(2,1)S(1)} %get-tuple-element.29), channel_id=1, source_target_pairs={{0,1},{1,0},{2,3},{3,2},{4,5},{5,4},{6,7},{7,6},{8,9},{9,8},{10,11... | collective-permute-start | bytes 589832 | tf_op jit(solution)/shard_map/ppermute | solution.py:42
  9.2 4.1 %collective-permute-start.1 = (bf16[96,512]{1,0:T(8,128)(2,1)S(1)}, bf16[96,512]{1,0:T(8,128)(2,1)S(1)}, u32[]{:S(2)}, u32[]{:S(2)}) collective-permute-start(bf16[96,512]{1,0:T(8,128)(2,1)S(1)} %shard_map.248), channel_id=1, source_target_pairs={{0,2},{1,3},{2,0},{3,1},{4,6},{5,7},{6,4},{7,5},{8,10},{9,11},{10,... | collective-permute-start | bytes 294920 | tf_op jit(solution)/shard_map/ppermute | solution.py:42
  14.3 31.1 %all-to-all-start = ((bf16[64,24,128]{2,1,0:T(8,128)(2,1)}), bf16[64,24,128]{2,1,0:T(8,128)(2,1)S(1)}, u32[]{:S(2)}, u32[]{:S(2)}) async-start(bf16[64,24,128]{2,1,0:T(8,128)(2,1)} %bitcast.9), calls=%async_computation | async-start | bytes 786432 | tf_op jit(solution)/shard_map/all_to_all | solution.py:452
  27.2 3.3 %collective-permute-start.2 = (bf16[512,256]{1,0:T(8,128)(2,1)S(1)}, bf16[512,256]{1,0:T(8,128)(2,1)S(1)}, u32[]{:S(2)}, u32[]{:S(2)}) collective-permute-start(bf16[512,256]{1,0:T(8,128)(2,1)S(1)} %get-tuple-element.33), channel_id=1, source_target_pairs={{0,1},{1,0},{2,3},{3,2},{4,5},{5,4},{6,7},{7,6},{8,9},{9,8},{10,11... | collective-permute-start | bytes 786440 | tf_op jit(solution)/shard_map/ppermute | solution.py:42
  28.8 10.9 %collective-permute-start.3 = (bf16[512,256]{1,0:T(8,128)(2,1)S(1)}, bf16[512,256]{1,0:T(8,128)(2,1)S(1)}, u32[]{:S(2)}, u32[]{:S(2)}) collective-permute-start(bf16[512,256]{1,0:T(8,128)(2,1)S(1)} %get-tuple-element.34), channel_id=1, source_target_pairs={{0,2},{1,3},{2,0},{3,1},{4,6},{5,7},{6,4},{7,5},{8,10},{9,11},{10,... | collective-permute-start | bytes 786440 | tf_op jit(solution)/shard_map/ppermute | solution.py:42
  29.1 16.3 %collective-permute-start.4 = (bf16[512,256]{1,0:T(8,128)(2,1)S(1)}, bf16[512,256]{1,0:T(8,128)(2,1)S(1)}, u32[]{:S(2)}, u32[]{:S(2)}) collective-permute-start(bf16[512,256]{1,0:T(8,128)(2,1)S(1)} %get-tuple-element.35), channel_id=1, source_target_pairs={{0,3},{1,2},{2,1},{3,0},{4,7},{5,6},{6,5},{7,4},{8,11},{9,10},{10,... | collective-permute-start | bytes 786440 | tf_op jit(solution)/shard_map/ppermute | solution.py:42
  46.3 1.8 %collective-permute-start.5 = (bf16[392,512]{1,0:T(8,128)(2,1)S(1)}, bf16[392,512]{1,0:T(8,128)(2,1)S(1)}, u32[]{:S(2)}, u32[]{:S(2)}) collective-permute-start(bf16[392,512]{1,0:T(8,128)(2,1)S(1)} %get-tuple-element.37), channel_id=1, source_target_pairs={{0,1},{1,0},{2,3},{3,2},{4,5},{5,4},{6,7},{7,6},{8,9},{9,8},{10,11... | collective-permute-start | bytes 1204232 | tf_op jit(solution)/shard_map/ppermute | solution.py:42
  48.3 37.2 %copy-start.8 = (bf16[2048]{0:T(1024)(128)(2,1)S(1)}, bf16[2048]{0:T(1024)(128)(2,1)}, u32[]{:S(2)}) copy-start(bf16[2048]{0:T(1024)(128)(2,1)} %param.47) | copy-start | bytes 12292
  48.3 6.4 %collective-permute-start.6 = (bf16[400,256]{1,0:T(8,128)(2,1)S(1)}, bf16[400,256]{1,0:T(8,128)(2,1)S(1)}, u32[]{:S(2)}, u32[]{:S(2)}) collective-permute-start(bf16[400,256]{1,0:T(8,128)(2,1)S(1)} %shard_map.253), channel_id=1, source_target_pairs={{0,2},{1,3},{2,0},{3,1},{4,6},{5,7},{6,4},{7,5},{8,10},{9,11},{10,... | collective-permute-start | bytes 614408 | tf_op jit(solution)/shard_map/ppermute | solution.py:42
  54.9 4.3 %collective-permute-start.8 = (bf16[384,128]{1,0:T(8,128)(2,1)S(1)}, bf16[384,128]{1,0:T(8,128)(2,1)S(1)}, u32[]{:S(2)}, u32[]{:S(2)}) collective-permute-start(bf16[384,128]{1,0:T(8,128)(2,1)S(1)} %shard_map.254.h0), channel_id=1, source_target_pairs={{0,2},{1,3},{2,0},{3,1},{4,6},{5,7},{6,4},{7,5},{8,10},{9,11},{10,... | collective-permute-start | bytes 294920 | tf_op jit(solution)/shard_map/ppermute | solution.py:42
  55.9 5.4 %collective-permute-start.10 = (bf16[128,512]{1,0:T(8,128)(2,1)S(1)}, bf16[128,512]{1,0:T(8,128)(2,1)S(1)}, u32[]{:S(2)}, u32[]{:S(2)}) collective-permute-start(bf16[128,512]{1,0:T(8,128)(2,1)S(1)} %get-tuple-element.39), channel_id=1, source_target_pairs={{0,1},{1,0},{2,3},{3,2},{4,5},{5,4},{6,7},{7,6},{8,9},{9,8},{10,11... | collective-permute-start | bytes 393224 | tf_op jit(solution)/shard_map/ppermute | solution.py:42
  57.4 5.5 %collective-permute-start.11 = (bf16[128,512]{1,0:T(8,128)(2,1)S(1)}, bf16[128,512]{1,0:T(8,128)(2,1)S(1)}, u32[]{:S(2)}, u32[]{:S(2)}) collective-permute-start(bf16[128,512]{1,0:T(8,128)(2,1)S(1)} %get-tuple-element.40), channel_id=1, source_target_pairs={{0,2},{1,3},{2,0},{3,1},{4,6},{5,7},{6,4},{7,5},{8,10},{9,11},{10,... | collective-permute-start | bytes 393224 | tf_op jit(solution)/shard_map/ppermute | solution.py:42
  58.0 7.8 %collective-permute-start.12 = (bf16[128,512]{1,0:T(8,128)(2,1)S(1)}, bf16[128,512]{1,0:T(8,128)(2,1)S(1)}, u32[]{:S(2)}, u32[]{:S(2)}) collective-permute-start(bf16[128,512]{1,0:T(8,128)(2,1)S(1)} %get-tuple-element.41), channel_id=1, source_target_pairs={{0,3},{1,2},{2,1},{3,0},{4,7},{5,6},{6,5},{7,4},{8,11},{9,10},{10,... | collective-permute-start | bytes 393224 | tf_op jit(solution)/shard_map/ppermute | solution.py:42
  59.0 6.8 %collective-permute-start.7 = (bf16[384,128]{1,0:T(8,128)(2,1)S(1)}, bf16[384,128]{1,0:T(8,128)(2,1)S(1)}, u32[]{:S(2)}, u32[]{:S(2)}) collective-permute-start(bf16[384,128]{1,0:T(8,128)(2,1)S(1)} %shard_map.254.h0), channel_id=1, source_target_pairs={{0,1},{1,0},{2,3},{3,2},{4,5},{5,4},{6,7},{7,6},{8,9},{9,8},{10,11... | collective-permute-start | bytes 294920 | tf_op jit(solution)/shard_map/ppermute | solution.py:42
  59.2 6.5 %collective-permute-start.9 = (bf16[384,128]{1,0:T(8,128)(2,1)S(1)}, bf16[384,128]{1,0:T(8,128)(2,1)S(1)}, u32[]{:S(2)}, u32[]{:S(2)}) collective-permute-start(bf16[384,128]{1,0:T(8,128)(2,1)S(1)} %collective-permute-done.8.h2), channel_id=1, source_target_pairs={{0,1},{1,0},{2,3},{3,2},{4,5},{5,4},{6,7},{7,6},{8,9},{9,8},{10,11... | collective-permute-start | bytes 294920 | tf_op jit(solution)/shard_map/ppermute | solution.py:42
  67.2 29.7 %all-to-all-start.1 = ((bf16[64,24,128]{2,1,0:T(8,128)(2,1)}), bf16[64,24,128]{2,1,0:T(8,128)(2,1)S(1)}, u32[]{:S(2)}, u32[]{:S(2)}) async-start(bf16[64,24,128]{2,1,0:T(8,128)(2,1)} %bitcast.14), calls=%async_computation.1 | async-start | bytes 786432 | tf_op jit(solution)/shard_map/all_to_all | solution.py:488
  79.0 4.9 %collective-permute-start.14 = (bf16[96,512]{1,0:T(8,128)(2,1)S(1)}, bf16[96,512]{1,0:T(8,128)(2,1)S(1)}, u32[]{:S(2)}, u32[]{:S(2)}) collective-permute-start(bf16[96,512]{1,0:T(8,128)(2,1)S(1)} %get-tuple-element.45.a0.resid), channel_id=1, source_target_pairs={{0,2},{1,3},{2,0},{3,1},{4,6},{5,7},{6,4},{7,5},{8,10},{9,11},{10,... | collective-permute-start | bytes 294920 | tf_op jit(solution)/shard_map/ppermute | solution.py:42
  79.3 6.2 %collective-permute-start.13 = (bf16[96,512]{1,0:T(8,128)(2,1)S(1)}, bf16[96,512]{1,0:T(8,128)(2,1)S(1)}, u32[]{:S(2)}, u32[]{:S(2)}) collective-permute-start(bf16[96,512]{1,0:T(8,128)(2,1)S(1)} %get-tuple-element.45.a0.resid), channel_id=1, source_target_pairs={{0,1},{1,0},{2,3},{3,2},{4,5},{5,4},{6,7},{7,6},{8,9},{9,8},{10,11... | collective-permute-start | bytes 294920 | tf_op jit(solution)/shard_map/ppermute | solution.py:42
  83.9 2.5 %collective-permute-start.15 = (bf16[96,512]{1,0:T(8,128)(2,1)S(1)}, bf16[96,512]{1,0:T(8,128)(2,1)S(1)}, u32[]{:S(2)}, u32[]{:S(2)}) collective-permute-start(bf16[96,512]{1,0:T(8,128)(2,1)S(1)} %collective-permute-done.14.a2), channel_id=1, source_target_pairs={{0,1},{1,0},{2,3},{3,2},{4,5},{5,4},{6,7},{7,6},{8,9},{9,8},{10,11... | collective-permute-start | bytes 294920 | tf_op jit(solution)/shard_map/ppermute | solution.py:42
  89.8 2.2 %collective-permute-start.16 = (bf16[96,512]{1,0:T(8,128)(2,1)S(1)}, bf16[96,512]{1,0:T(8,128)(2,1)S(1)}, u32[]{:S(2)}, u32[]{:S(2)}) collective-permute-start(bf16[96,512]{1,0:T(8,128)(2,1)S(1)} %get-tuple-element.48), channel_id=1, source_target_pairs={{0,1},{1,0},{2,3},{3,2},{4,5},{5,4},{6,7},{7,6},{8,9},{9,8},{10,11... | collective-permute-start | bytes 294920 | tf_op jit(solution)/shard_map/ppermute | solution.py:42
  90.2 4.2 %collective-permute-start.17 = (bf16[96,512]{1,0:T(8,128)(2,1)S(1)}, bf16[96,512]{1,0:T(8,128)(2,1)S(1)}, u32[]{:S(2)}, u32[]{:S(2)}) collective-permute-start(bf16[96,512]{1,0:T(8,128)(2,1)S(1)} %get-tuple-element.49), channel_id=1, source_target_pairs={{0,2},{1,3},{2,0},{3,1},{4,6},{5,7},{6,4},{7,5},{8,10},{9,11},{10,... | collective-permute-start | bytes 294920 | tf_op jit(solution)/shard_map/ppermute | solution.py:42
  90.4 6.5 %collective-permute-start.18 = (bf16[96,512]{1,0:T(8,128)(2,1)S(1)}, bf16[96,512]{1,0:T(8,128)(2,1)S(1)}, u32[]{:S(2)}, u32[]{:S(2)}) collective-permute-start(bf16[96,512]{1,0:T(8,128)(2,1)S(1)} %get-tuple-element.50), channel_id=1, source_target_pairs={{0,3},{1,2},{2,1},{3,0},{4,7},{5,6},{6,5},{7,4},{8,11},{9,10},{10,... | collective-permute-start | bytes 294920 | tf_op jit(solution)/shard_map/ppermute | solution.py:42
  (6 other events, 82.9 us)

commit v5 on v4

--- a/solution.py
+++ b/solution.py
@@ -18,6 +18,7 @@
 ANY = pl.BlockSpec(memory_space=pl.ANY)
 HBM = pl.BlockSpec(memory_space=pltpu.HBM)
 FREE = pl.BlockSpec(memory_space=pltpu.VMEM)
+OUT = pl.BlockSpec()
 
 
 def iota(shape, dim):
@@ -68,7 +69,7 @@
 
 def state_kernel(*refs):
     inputs, (own, beside, new_re, new_im), held = refs[0:13], refs[13:17], refs[17:30]
-    fresh_re_v, fresh_im_v, blocks_v, sems = refs[30:]
+    blocks_v, sems = refs[30:]
     t = lax.axis_index("tp")
     loads = [
         pltpu.make_async_copy(a, b, sems.at[i]) for i, (a, b) in enumerate(zip(inputs, held))
@@ -114,14 +115,8 @@
     was_re, was_im = re_v[...], im_v[...]
     fresh_re = lam_re * was_re - lam_im * was_im + (fac_re * in_re - fac_im * in_im)
     fresh_im = lam_re * was_im + lam_im * was_re + (fac_re * in_im + fac_im * in_re)
-    fresh_re_v[...] = fresh_re
-    fresh_im_v[...] = fresh_im
-    stores = [
-        pltpu.make_async_copy(fresh_re_v, new_re, sems.at[13]),
-        pltpu.make_async_copy(fresh_im_v, new_im, sems.at[14]),
-    ]
-    for store in stores:
-        store.start()
+    new_re[...] = fresh_re
+    new_im[...] = fresh_im
     mixed = (
         nt_dot(fresh_re.astype(BF16), blocks_v[2])
         - nt_dot(fresh_im.astype(BF16), blocks_v[3])
@@ -133,8 +128,6 @@
     for m, pair in ((1, beside), (3, beside), (0, own), (2, own)):
         near = pl.ds((m // 2) * quarter, quarter)
         pair[:, near] = dot(act, out_v[:, cols_of(t ^ m, quarter)]).astype(BF16)
-    for store in stores:
-        store.wait()
 
 
 def half_kernel(own, came, onward):
@@ -329,9 +322,9 @@
 
 def call(kernel, outs, scratch=(), limit=4, in_specs=None, out_specs=None):
     out_specs = out_specs or [VMEM] * len(outs)
+    kinds = {id(VMEM): pltpu.VMEM, id(OUT): pltpu.HBM}
     out_shape = [
-        pltpu.VMEM(s, d) if spec is VMEM else jax.ShapeDtypeStruct(s, d)
-        for (s, d), spec in zip(outs, out_specs)
+        kinds.get(id(spec), jax.ShapeDtypeStruct)(s, d) for (s, d), spec in zip(outs, out_specs)
     ]
 
     def run(*args):
@@ -418,12 +411,11 @@
         [((rows, 2 * quarter), BF16)] * 2 + [states] * 2,
         [pltpu.SMEM(log_step.shape, F32)]
         + [pltpu.VMEM(x.shape, x.dtype) for x in state_inputs[1:]]
-        + [pltpu.VMEM(states[0], F32)] * 2
         + [pltpu.VMEM((4, groups * channels, groups * entries), BF16)]
-        + [pltpu.SemaphoreType.DMA((15,))],
+        + [pltpu.SemaphoreType.DMA((13,))],
         20,
         [HBM] * 13,
-        [VMEM] * 2 + [HBM] * 2,
+        [VMEM] * 4,
     )(*state_inputs)
     came_mix = exchanged(beside, 1)
     (onward,) = call(half_kernel, [piece])(own, came_mix)
@@ -462,7 +454,7 @@
         + [pltpu.SemaphoreType.DMA((3,))],
         12,
         [VMEM] * 6 + [HBM] * 3,
-        [FREE] * 5,
+        [OUT] * 5,
     )(gains, *near, blend_weight.reshape(1, width), dense_gate, dense_up, dense_down)
     dense = [dense[0]] + [exchanged(dense[m], m) for m in (1, 2, 3)]
     keep, send = call(

time: 98.2 us -> 102 us (1.039)
  local copies, waits for them, and re-layouts: 0.06 us -> 5.2 us
  waiting for transfers between devices: 40.6 us -> 39.1 us
    unnamed x18 -> x36, local copies, waits for them, and re-layouts: 0.05 us -> 5.18 us
    ppermute x19, waiting for transfers between devices: 40.6 us -> 39.1 us  [exchanged(): return lax.ppermute(value, 'tp', [(i, i ^ mask) for i in range(4)])]
  transfers between devices with their start and end apart: 21 -> 21, of which waited for: 12 -> 12; matrix products, arithmetic and copies ran while one was open for 0% -> 1% of each run, Pallas kernels for 4% -> 5%
where the time goes in v5:
time: 102 us
  starting transfers between devices  43.2 us (42%)
  waiting for transfers between devices  39.1 us (38%)
  Pallas kernels  13.3 us (13%)
  local copies, waits for them, and re-layouts  5.2 us (5%)
    ppermute x19, waiting for transfers between devices, exchanged(): return lax.ppermute(value, 'tp', [(i, i ^ mask) for i in range(4)])  39.1 us
    ppermute x19, starting transfers between devices, exchanged(): return lax.ppermute(value, 'tp', [(i, i ^ mask) for i in range(4)])  18.8 us
    pallas_call x11, Pallas kernels, run(): pl.pallas_call(kernel, out_shape=tuple(out_shape), in_specs=specs, out_sp...  13.3 us
    all_to_all x1, starting transfers between devices, per_device(): lax.all_to_all(packed.reshape(ep, capacity * blocks, lanes), 'ep', 0, 0,...  12.6 us
    all_to_all x1, starting transfers between devices, per_device(): lax.all_to_all(sent.reshape(ep, capacity * blocks, lanes), 'ep', 0, 0, ti...  11.8 us
    unnamed x36, local copies, waits for them, and re-layouts  5.18 us
  transfers between devices with their start and end apart: 21, of which 12 were waited for; matrix products, arithmetic and copies ran while one was open for 1% of the time, Pallas kernels for 5%

profile of v5, /device:TPU:1, one launch (start us, length us, event | category | flops | bytes accessed | tf_op | source)
XLA Modules:
  0.0 101.7 jit_solution(6259945290825184389)
XLA Ops:
  0.7 3.7 %shard_map.247 = (bf16[96,1024]{1,0:T(8,128)(2,1)S(1)}, bf16[96,1024]{1,0:T(8,128)(2,1)S(1)}, f32[96,1024]{1,0:T(8,128)S(1)}, f32[96,1024]{1,0:T(8,128)S(1)}) custom-call(f32[16]{0:T(128)} %refs_0_.1, f32[16,64]{1,0:T(8,128)} %refs_1_.1, f32[16,16]{1,0:T(8,128)} %refs_2_.1, f32[256,64]{1,0:T(8,128)} %bitcast.26, f32[256,64]{1,0:T(8,128)} %bitcast.27, ...), custom_call_target="tpu_custom_call" | custom-call | tf_op jit(solution)/shard_map/pallas_call | solution.py:337
  4.4 3.3 %collective-permute-start = (bf16[96,1024]{1,0:T(8,128)(2,1)S(1)}, bf16[96,1024]{1,0:T(8,128)(2,1)S(1)}, u32[]{:S(2)}, u32[]{:S(2)}) collective-permute-start(bf16[96,1024]{1,0:T(8,128)(2,1)S(1)} %get-tuple-element.29), channel_id=1, source_target_pairs={{0,1},{1,0},{2,3},{3,2},{4,5},{5,4},{6,7},{7,6},{8,9},{9,8},{10,11... | collective-permute-start | bytes 589832 | tf_op jit(solution)/shard_map/ppermute | solution.py:43
  9.2 3.6 %collective-permute-done.1.last = bf16[96,512]{1,0:T(8,128)(2,1)S(1)} collective-permute-done((bf16[96,512]{1,0:T(8,128)(2,1)S(1)}, bf16[96,512]{1,0:T(8,128)(2,1)S(1)}, u32[]{:S(2)}, u32[]{:S(2)}) %collective-permute-start.1) | collective-permute-done | bytes 98336 | tf_op jit(solution)/shard_map/ppermute | solution.py:43
  12.9 1.1 %shard_map.250 = (bf16[96,512]{1,0:T(8,128)(2,1)S(1)}, bf16[1536,128]{1,0:T(8,128)(2,1)}) custom-call(bf16[96,2048]{1,0:T(8,128)(2,1)S(1)} %copy-done, bf16[96,1024]{1,0:T(8,128)(2,1)S(1)} %get-tuple-element.28.own, bf16[96,1024]{1,0:T(8,128)(2,1)S(1)} %collective-permute-done.came, bf16[96,512]{1,0:T(8,128)(2,1)S(1)} %collective-permute-done.1.last, ...), custom_call_target="tpu_custom_call" | custom-call | tf_op jit(solution)/shard_map/pallas_call | solution.py:337
  13.9 12.6 %all-to-all-start = ((bf16[64,24,128]{2,1,0:T(8,128)(2,1)}), bf16[64,24,128]{2,1,0:T(8,128)(2,1)S(1)}, u32[]{:S(2)}, u32[]{:S(2)}) async-start(bf16[64,24,128]{2,1,0:T(8,128)(2,1)} %bitcast.9), calls=%async_computation | async-start | bytes 786432 | tf_op jit(solution)/shard_map/all_to_all | solution.py:444
  28.7 1.5 %collective-permute-start.2 = (bf16[512,256]{1,0:T(8,128)(2,1)S(1)}, bf16[512,256]{1,0:T(8,128)(2,1)S(1)}, u32[]{:S(2)}, u32[]{:S(2)}) collective-permute-start(bf16[512,256]{1,0:T(8,128)(2,1)S(1)} %get-tuple-element.33), channel_id=1, source_target_pairs={{0,1},{1,0},{2,3},{3,2},{4,5},{5,4},{6,7},{7,6},{8,9},{9,8},{10,11... | collective-permute-start | bytes 786440 | tf_op jit(solution)/shard_map/ppermute | solution.py:43
  30.6 1.3 %collective-permute-start.4 = (bf16[512,256]{1,0:T(8,128)(2,1)S(1)}, bf16[512,256]{1,0:T(8,128)(2,1)S(1)}, u32[]{:S(2)}, u32[]{:S(2)}) collective-permute-start(bf16[512,256]{1,0:T(8,128)(2,1)S(1)} %get-tuple-element.35), channel_id=1, source_target_pairs={{0,3},{1,2},{2,1},{3,0},{4,7},{5,6},{6,5},{7,4},{8,11},{9,10},{10,... | collective-permute-start | bytes 786440 | tf_op jit(solution)/shard_map/ppermute | solution.py:43
  31.9 8.6 %collective-permute-done.3.w2 = bf16[512,256]{1,0:T(8,128)(2,1)S(1)} collective-permute-done((bf16[512,256]{1,0:T(8,128)(2,1)S(1)}, bf16[512,256]{1,0:T(8,128)(2,1)S(1)}, u32[]{:S(2)}, u32[]{:S(2)}) %collective-permute-start.3) | collective-permute-done | bytes 262176 | tf_op jit(solution)/shard_map/ppermute | solution.py:43
  40.5 5.7 %collective-permute-done.4.w3 = bf16[512,256]{1,0:T(8,128)(2,1)S(1)} collective-permute-done((bf16[512,256]{1,0:T(8,128)(2,1)S(1)}, bf16[512,256]{1,0:T(8,128)(2,1)S(1)}, u32[]{:S(2)}, u32[]{:S(2)}) %collective-permute-start.4) | collective-permute-done | bytes 262176 | tf_op jit(solution)/shard_map/ppermute | solution.py:43
  47.6 1.4 %collective-permute-done.5.came = bf16[392,512]{1,0:T(8,128)(2,1)S(1)} collective-permute-done((bf16[392,512]{1,0:T(8,128)(2,1)S(1)}, bf16[392,512]{1,0:T(8,128)(2,1)S(1)}, u32[]{:S(2)}, u32[]{:S(2)}) %collective-permute-start.5) | collective-permute-done | bytes 401440 | tf_op jit(solution)/shard_map/ppermute | solution.py:43
  49.9 5.6 %collective-permute-done.6.last = bf16[400,256]{1,0:T(8,128)(2,1)S(1)} collective-permute-done((bf16[400,256]{1,0:T(8,128)(2,1)S(1)}, bf16[400,256]{1,0:T(8,128)(2,1)S(1)}, u32[]{:S(2)}, u32[]{:S(2)}) %collective-permute-start.6) | collective-permute-done | bytes 204832 | tf_op jit(solution)/shard_map/ppermute | solution.py:43
  56.5 1.5 %collective-permute-start.10 = (bf16[128,512]{1,0:T(8,128)(2,1)S(1)}, bf16[128,512]{1,0:T(8,128)(2,1)S(1)}, u32[]{:S(2)}, u32[]{:S(2)}) collective-permute-start(bf16[128,512]{1,0:T(8,128)(2,1)S(1)} %copy-done.14), channel_id=1, source_target_pairs={{0,1},{1,0},{2,3},{3,2},{4,5},{5,4},{6,7},{7,6},{8,9},{9,8},{10,11... | collective-permute-start | bytes 393224 | tf_op jit(solution)/shard_map/ppermute | solution.py:43
  59.9 2.3 %collective-permute-start.9 = (bf16[384,128]{1,0:T(8,128)(2,1)S(1)}, bf16[384,128]{1,0:T(8,128)(2,1)S(1)}, u32[]{:S(2)}, u32[]{:S(2)}) collective-permute-start(bf16[384,128]{1,0:T(8,128)(2,1)S(1)} %collective-permute-done.8.h2), channel_id=1, source_target_pairs={{0,1},{1,0},{2,3},{3,2},{4,5},{5,4},{6,7},{7,6},{8,9},{9,8},{10,11... | collective-permute-start | bytes 294920 | tf_op jit(solution)/shard_map/ppermute | solution.py:43
  62.2 1.4 %collective-permute-done.11.w2 = bf16[128,512]{1,0:T(8,128)(2,1)S(1)} collective-permute-done((bf16[128,512]{1,0:T(8,128)(2,1)S(1)}, bf16[128,512]{1,0:T(8,128)(2,1)S(1)}, u32[]{:S(2)}, u32[]{:S(2)}) %collective-permute-start.11) | collective-permute-done | bytes 131104 | tf_op jit(solution)/shard_map/ppermute | solution.py:43
  63.6 3.0 %collective-permute-done.12.w3 = bf16[128,512]{1,0:T(8,128)(2,1)S(1)} collective-permute-done((bf16[128,512]{1,0:T(8,128)(2,1)S(1)}, bf16[128,512]{1,0:T(8,128)(2,1)S(1)}, u32[]{:S(2)}, u32[]{:S(2)}) %collective-permute-start.12) | collective-permute-done | bytes 131104 | tf_op jit(solution)/shard_map/ppermute | solution.py:43
  66.6 1.4 %shard_map.255 = bf16[1536,128]{1,0:T(8,128)(2,1)} custom-call(bf16[384,128]{1,0:T(8,128)(2,1)S(1)} %shard_map.254.h0, bf16[384,128]{1,0:T(8,128)(2,1)S(1)} %collective-permute-done.7.h1, bf16[384,128]{1,0:T(8,128)(2,1)S(1)} %collective-permute-done.8.h2, bf16[384,128]{1,0:T(8,128)(2,1)S(1)} %collective-permute-done.9.h3, ...), custom_call_target="tpu_custom_call" | custom-call | tf_op jit(solution)/shard_map/pallas_call | solution.py:337
  68.0 11.8 %all-to-all-start.1 = ((bf16[64,24,128]{2,1,0:T(8,128)(2,1)}), bf16[64,24,128]{2,1,0:T(8,128)(2,1)S(1)}, u32[]{:S(2)}, u32[]{:S(2)}) async-start(bf16[64,24,128]{2,1,0:T(8,128)(2,1)} %bitcast.14), calls=%async_computation.1 | async-start | bytes 786432 | tf_op jit(solution)/shard_map/all_to_all | solution.py:480
  80.8 4.3 %collective-permute-done.14.a2 = bf16[96,512]{1,0:T(8,128)(2,1)S(1)} collective-permute-done((bf16[96,512]{1,0:T(8,128)(2,1)S(1)}, bf16[96,512]{1,0:T(8,128)(2,1)S(1)}, u32[]{:S(2)}, u32[]{:S(2)}) %collective-permute-start.14) | collective-permute-done | bytes 98336 | tf_op jit(solution)/shard_map/ppermute | solution.py:43
  85.1 1.5 %collective-permute-start.15 = (bf16[96,512]{1,0:T(8,128)(2,1)S(1)}, bf16[96,512]{1,0:T(8,128)(2,1)S(1)}, u32[]{:S(2)}, u32[]{:S(2)}) collective-permute-start(bf16[96,512]{1,0:T(8,128)(2,1)S(1)} %collective-permute-done.14.a2), channel_id=1, source_target_pairs={{0,1},{1,0},{2,3},{3,2},{4,5},{5,4},{6,7},{7,6},{8,9},{9,8},{10,11... | collective-permute-start | bytes 294920 | tf_op jit(solution)/shard_map/ppermute | solution.py:43
  87.5 4.1 %shard_map.256 = (bf16[96,512]{1,0:T(8,128)(2,1)}, bf16[96,512]{1,0:T(8,128)(2,1)}, bf16[96,512]{1,0:T(8,128)(2,1)}, bf16[96,512]{1,0:T(8,128)(2,1)}, f32[96,128]{1,0:T(8,128)}) custom-call(bf16[1,2048]{1,0:T(2,128)(2,1)S(1)} %reshape.55.gains, bf16[96,512]{1,0:T(8,128)(2,1)S(1)} %get-tuple-element.45.a0.resid, ...), custom_call_target="tpu_custom_call" | custom-call | tf_op jit(solution)/shard_map/pallas_call | solution.py:337
  92.1 1.8 %collective-permute-start.18 = (bf16[96,512]{1,0:T(8,128)(2,1)}, bf16[96,512]{1,0:T(8,128)(2,1)S(1)}, u32[]{:S(2)}, u32[]{:S(2)}) collective-permute-start(bf16[96,512]{1,0:T(8,128)(2,1)} %get-tuple-element.50), channel_id=1, source_target_pairs={{0,3},{1,2},{2,1},{3,0},{4,7},{5,6},{6,5},{7,4},{8,11},{9,10},{10,... | collective-permute-start | bytes 294920 | tf_op jit(solution)/shard_map/ppermute | solution.py:43
  95.3 1.2 %collective-permute-done.17.p2 = bf16[96,512]{1,0:T(8,128)(2,1)S(1)} collective-permute-done((bf16[96,512]{1,0:T(8,128)(2,1)}, bf16[96,512]{1,0:T(8,128)(2,1)S(1)}, u32[]{:S(2)}, u32[]{:S(2)}) %collective-permute-start.17) | collective-permute-done | bytes 98336 | tf_op jit(solution)/shard_map/ppermute | solution.py:43
  96.5 2.4 %collective-permute-done.18.p3 = bf16[96,512]{1,0:T(8,128)(2,1)S(1)} collective-permute-done((bf16[96,512]{1,0:T(8,128)(2,1)}, bf16[96,512]{1,0:T(8,128)(2,1)S(1)}, u32[]{:S(2)}, u32[]{:S(2)}) %collective-permute-start.18) | collective-permute-done | bytes 98336 | tf_op jit(solution)/shard_map/ppermute | solution.py:43
  100.6 1.1 %shard_map.257 = bf16[96,512]{1,0:T(8,128)(2,1)} custom-call(bf16[1536,128]{1,0:T(8,128)(2,1)S(1)} %bitcast.18, bf16[192,384]{1,0:T(8,128)(2,1)S(1)} %get-tuple-element.42.w, f32[96,128]{1,0:T(8,128)S(1)} %get-tuple-element.43.share0, f32[96,128]{1,0:T(8,128)S(1)} %get-tuple-element.44.share1, bf16[96,512]{1,0:T(8,128)(2,1)S(1)} %get-tuple-element.45.a0.resid, ...), custom_call_target="tpu_custom_call" | custom-call | tf_op jit(solution)/shard_map/pallas_call | solution.py:337
  (67 shorter events, 14.8 us)
Async XLA Ops:
  4.4 22.2 %copy-start.1 = (bf16[1,2048,128]{2,1,0:T(8,128)(2,1)S(1)}, bf16[1,2048,128]{2,1,0:T(8,128)(2,1)}, u32[]{:S(2)}) copy-start(bf16[1,2048,128]{2,1,0:T(8,128)(2,1)} %param.41) | copy-start | bytes 1572868
  4.4 27.5 %copy-start.15 = (bf16[2048]{0:T(1024)(128)(2,1)S(1)}, bf16[2048]{0:T(1024)(128)(2,1)}, u32[]{:S(2)}) copy-start(bf16[2048]{0:T(1024)(128)(2,1)} %param.37) | copy-start | bytes 12292
  4.4 4.3 %collective-permute-start = (bf16[96,1024]{1,0:T(8,128)(2,1)S(1)}, bf16[96,1024]{1,0:T(8,128)(2,1)S(1)}, u32[]{:S(2)}, u32[]{:S(2)}) collective-permute-start(bf16[96,1024]{1,0:T(8,128)(2,1)S(1)} %get-tuple-element.29), channel_id=1, source_target_pairs={{0,1},{1,0},{2,3},{3,2},{4,5},{5,4},{6,7},{7,6},{8,9},{9,8},{10,11... | collective-permute-start | bytes 589832 | tf_op jit(solution)/shard_map/ppermute | solution.py:43
  8.8 4.1 %collective-permute-start.1 = (bf16[96,512]{1,0:T(8,128)(2,1)S(1)}, bf16[96,512]{1,0:T(8,128)(2,1)S(1)}, u32[]{:S(2)}, u32[]{:S(2)}) collective-permute-start(bf16[96,512]{1,0:T(8,128)(2,1)S(1)} %shard_map.248), channel_id=1, source_target_pairs={{0,2},{1,3},{2,0},{3,1},{4,6},{5,7},{6,4},{7,5},{8,10},{9,11},{10,... | collective-permute-start | bytes 294920 | tf_op jit(solution)/shard_map/ppermute | solution.py:43
  13.9 32.2 %all-to-all-start = ((bf16[64,24,128]{2,1,0:T(8,128)(2,1)}), bf16[64,24,128]{2,1,0:T(8,128)(2,1)S(1)}, u32[]{:S(2)}, u32[]{:S(2)}) async-start(bf16[64,24,128]{2,1,0:T(8,128)(2,1)} %bitcast.9), calls=%async_computation | async-start | bytes 786432 | tf_op jit(solution)/shard_map/all_to_all | solution.py:444
  28.7 3.2 %collective-permute-start.2 = (bf16[512,256]{1,0:T(8,128)(2,1)S(1)}, bf16[512,256]{1,0:T(8,128)(2,1)S(1)}, u32[]{:S(2)}, u32[]{:S(2)}) collective-permute-start(bf16[512,256]{1,0:T(8,128)(2,1)S(1)} %get-tuple-element.33), channel_id=1, source_target_pairs={{0,1},{1,0},{2,3},{3,2},{4,5},{5,4},{6,7},{7,6},{8,9},{9,8},{10,11... | collective-permute-start | bytes 786440 | tf_op jit(solution)/shard_map/ppermute | solution.py:43
  30.2 10.3 %collective-permute-start.3 = (bf16[512,256]{1,0:T(8,128)(2,1)S(1)}, bf16[512,256]{1,0:T(8,128)(2,1)S(1)}, u32[]{:S(2)}, u32[]{:S(2)}) collective-permute-start(bf16[512,256]{1,0:T(8,128)(2,1)S(1)} %get-tuple-element.34), channel_id=1, source_target_pairs={{0,2},{1,3},{2,0},{3,1},{4,6},{5,7},{6,4},{7,5},{8,10},{9,11},{10,... | collective-permute-start | bytes 786440 | tf_op jit(solution)/shard_map/ppermute | solution.py:43
  30.6 15.6 %collective-permute-start.4 = (bf16[512,256]{1,0:T(8,128)(2,1)S(1)}, bf16[512,256]{1,0:T(8,128)(2,1)S(1)}, u32[]{:S(2)}, u32[]{:S(2)}) collective-permute-start(bf16[512,256]{1,0:T(8,128)(2,1)S(1)} %get-tuple-element.35), channel_id=1, source_target_pairs={{0,3},{1,2},{2,1},{3,0},{4,7},{5,6},{6,5},{7,4},{8,11},{9,10},{10,... | collective-permute-start | bytes 786440 | tf_op jit(solution)/shard_map/ppermute | solution.py:43
  47.1 1.8 %collective-permute-start.5 = (bf16[392,512]{1,0:T(8,128)(2,1)S(1)}, bf16[392,512]{1,0:T(8,128)(2,1)S(1)}, u32[]{:S(2)}, u32[]{:S(2)}) collective-permute-start(bf16[392,512]{1,0:T(8,128)(2,1)S(1)} %get-tuple-element.37), channel_id=1, source_target_pairs={{0,1},{1,0},{2,3},{3,2},{4,5},{5,4},{6,7},{7,6},{8,9},{9,8},{10,11... | collective-permute-start | bytes 1204232 | tf_op jit(solution)/shard_map/ppermute | solution.py:43
  49.1 37.5 %copy-start.16 = (bf16[2048]{0:T(1024)(128)(2,1)S(1)}, bf16[2048]{0:T(1024)(128)(2,1)}, u32[]{:S(2)}) copy-start(bf16[2048]{0:T(1024)(128)(2,1)} %param.47) | copy-start | bytes 12292
  49.1 6.4 %collective-permute-start.6 = (bf16[400,256]{1,0:T(8,128)(2,1)S(1)}, bf16[400,256]{1,0:T(8,128)(2,1)S(1)}, u32[]{:S(2)}, u32[]{:S(2)}) collective-permute-start(bf16[400,256]{1,0:T(8,128)(2,1)S(1)} %shard_map.253), channel_id=1, source_target_pairs={{0,2},{1,3},{2,0},{3,1},{4,6},{5,7},{6,4},{7,5},{8,10},{9,11},{10,... | collective-permute-start | bytes 614408 | tf_op jit(solution)/shard_map/ppermute | solution.py:43
  55.7 4.2 %collective-permute-start.8 = (bf16[384,128]{1,0:T(8,128)(2,1)S(1)}, bf16[384,128]{1,0:T(8,128)(2,1)S(1)}, u32[]{:S(2)}, u32[]{:S(2)}) collective-permute-start(bf16[384,128]{1,0:T(8,128)(2,1)S(1)} %shard_map.254.h0), channel_id=1, source_target_pairs={{0,2},{1,3},{2,0},{3,1},{4,6},{5,7},{6,4},{7,5},{8,10},{9,11},{10,... | collective-permute-start | bytes 294920 | tf_op jit(solution)/shard_map/ppermute | solution.py:43
  56.5 5.6 %collective-permute-start.10 = (bf16[128,512]{1,0:T(8,128)(2,1)S(1)}, bf16[128,512]{1,0:T(8,128)(2,1)S(1)}, u32[]{:S(2)}, u32[]{:S(2)}) collective-permute-start(bf16[128,512]{1,0:T(8,128)(2,1)S(1)} %copy-done.14), channel_id=1, source_target_pairs={{0,1},{1,0},{2,3},{3,2},{4,5},{5,4},{6,7},{7,6},{8,9},{9,8},{10,11... | collective-permute-start | bytes 393224 | tf_op jit(solution)/shard_map/ppermute | solution.py:43
  58.0 5.5 %collective-permute-start.11 = (bf16[128,512]{1,0:T(8,128)(2,1)S(1)}, bf16[128,512]{1,0:T(8,128)(2,1)S(1)}, u32[]{:S(2)}, u32[]{:S(2)}) collective-permute-start(bf16[128,512]{1,0:T(8,128)(2,1)S(1)} %copy-done.12), channel_id=1, source_target_pairs={{0,2},{1,3},{2,0},{3,1},{4,6},{5,7},{6,4},{7,5},{8,10},{9,11},{10,... | collective-permute-start | bytes 393224 | tf_op jit(solution)/shard_map/ppermute | solution.py:43
  58.8 7.8 %collective-permute-start.12 = (bf16[128,512]{1,0:T(8,128)(2,1)S(1)}, bf16[128,512]{1,0:T(8,128)(2,1)S(1)}, u32[]{:S(2)}, u32[]{:S(2)}) collective-permute-start(bf16[128,512]{1,0:T(8,128)(2,1)S(1)} %copy-done.10), channel_id=1, source_target_pairs={{0,3},{1,2},{2,1},{3,0},{4,7},{5,6},{6,5},{7,4},{8,11},{9,10},{10,... | collective-permute-start | bytes 393224 | tf_op jit(solution)/shard_map/ppermute | solution.py:43
  59.8 6.8 %collective-permute-start.7 = (bf16[384,128]{1,0:T(8,128)(2,1)S(1)}, bf16[384,128]{1,0:T(8,128)(2,1)S(1)}, u32[]{:S(2)}, u32[]{:S(2)}) collective-permute-start(bf16[384,128]{1,0:T(8,128)(2,1)S(1)} %shard_map.254.h0), channel_id=1, source_target_pairs={{0,1},{1,0},{2,3},{3,2},{4,5},{5,4},{6,7},{7,6},{8,9},{9,8},{10,11... | collective-permute-start | bytes 294920 | tf_op jit(solution)/shard_map/ppermute | solution.py:43
  59.9 6.7 %collective-permute-start.9 = (bf16[384,128]{1,0:T(8,128)(2,1)S(1)}, bf16[384,128]{1,0:T(8,128)(2,1)S(1)}, u32[]{:S(2)}, u32[]{:S(2)}) collective-permute-start(bf16[384,128]{1,0:T(8,128)(2,1)S(1)} %collective-permute-done.8.h2), channel_id=1, source_target_pairs={{0,1},{1,0},{2,3},{3,2},{4,5},{5,4},{6,7},{7,6},{8,9},{9,8},{10,11... | collective-permute-start | bytes 294920 | tf_op jit(solution)/shard_map/ppermute | solution.py:43
  68.0 30.9 %all-to-all-start.1 = ((bf16[64,24,128]{2,1,0:T(8,128)(2,1)}), bf16[64,24,128]{2,1,0:T(8,128)(2,1)S(1)}, u32[]{:S(2)}, u32[]{:S(2)}) async-start(bf16[64,24,128]{2,1,0:T(8,128)(2,1)} %bitcast.14), calls=%async_computation.1 | async-start | bytes 786432 | tf_op jit(solution)/shard_map/all_to_all | solution.py:480
  79.8 5.3 %collective-permute-start.14 = (bf16[96,512]{1,0:T(8,128)(2,1)S(1)}, bf16[96,512]{1,0:T(8,128)(2,1)S(1)}, u32[]{:S(2)}, u32[]{:S(2)}) collective-permute-start(bf16[96,512]{1,0:T(8,128)(2,1)S(1)} %get-tuple-element.45.a0.resid), channel_id=1, source_target_pairs={{0,2},{1,3},{2,0},{3,1},{4,6},{5,7},{6,4},{7,5},{8,10},{9,11},{10,... | collective-permute-start | bytes 294920 | tf_op jit(solution)/shard_map/ppermute | solution.py:43
  79.9 6.7 %collective-permute-start.13 = (bf16[96,512]{1,0:T(8,128)(2,1)S(1)}, bf16[96,512]{1,0:T(8,128)(2,1)S(1)}, u32[]{:S(2)}, u32[]{:S(2)}) collective-permute-start(bf16[96,512]{1,0:T(8,128)(2,1)S(1)} %get-tuple-element.45.a0.resid), channel_id=1, source_target_pairs={{0,1},{1,0},{2,3},{3,2},{4,5},{5,4},{6,7},{7,6},{8,9},{9,8},{10,11... | collective-permute-start | bytes 294920 | tf_op jit(solution)/shard_map/ppermute | solution.py:43
  85.1 2.4 %collective-permute-start.15 = (bf16[96,512]{1,0:T(8,128)(2,1)S(1)}, bf16[96,512]{1,0:T(8,128)(2,1)S(1)}, u32[]{:S(2)}, u32[]{:S(2)}) collective-permute-start(bf16[96,512]{1,0:T(8,128)(2,1)S(1)} %collective-permute-done.14.a2), channel_id=1, source_target_pairs={{0,1},{1,0},{2,3},{3,2},{4,5},{5,4},{6,7},{7,6},{8,9},{9,8},{10,11... | collective-permute-start | bytes 294920 | tf_op jit(solution)/shard_map/ppermute | solution.py:43
  91.6 3.7 %collective-permute-start.16 = (bf16[96,512]{1,0:T(8,128)(2,1)}, bf16[96,512]{1,0:T(8,128)(2,1)S(1)}, u32[]{:S(2)}, u32[]{:S(2)}) collective-permute-start(bf16[96,512]{1,0:T(8,128)(2,1)} %get-tuple-element.48), channel_id=1, source_target_pairs={{0,1},{1,0},{2,3},{3,2},{4,5},{5,4},{6,7},{7,6},{8,9},{9,8},{10,11... | collective-permute-start | bytes 294920 | tf_op jit(solution)/shard_map/ppermute | solution.py:43
  92.1 4.4 %collective-permute-start.17 = (bf16[96,512]{1,0:T(8,128)(2,1)}, bf16[96,512]{1,0:T(8,128)(2,1)S(1)}, u32[]{:S(2)}, u32[]{:S(2)}) collective-permute-start(bf16[96,512]{1,0:T(8,128)(2,1)} %get-tuple-element.49), channel_id=1, source_target_pairs={{0,2},{1,3},{2,0},{3,1},{4,6},{5,7},{6,4},{7,5},{8,10},{9,11},{10,... | collective-permute-start | bytes 294920 | tf_op jit(solution)/shard_map/ppermute | solution.py:43
  92.1 6.8 %collective-permute-start.18 = (bf16[96,512]{1,0:T(8,128)(2,1)}, bf16[96,512]{1,0:T(8,128)(2,1)S(1)}, u32[]{:S(2)}, u32[]{:S(2)}) collective-permute-start(bf16[96,512]{1,0:T(8,128)(2,1)} %get-tuple-element.50), channel_id=1, source_target_pairs={{0,3},{1,2},{2,1},{3,0},{4,7},{5,6},{6,5},{7,4},{8,11},{9,10},{10,... | collective-permute-start | bytes 294920 | tf_op jit(solution)/shard_map/ppermute | solution.py:43
  (14 other events, 119.7 us)

commit v6 on v5

--- a/solution.py
+++ b/solution.py
@@ -214,7 +214,7 @@
 
 
 def dense_kernel(
-    gains, a0, a1, a2, a3, blend_weight, gate, up, down, p0, p1, p2, p3, blend,
+    gains, a0, a1, a2, a3, blend_weight, gate, up, down, own, beside, blend,
     full, gate_v, up_v, down_v, sems,
 ):
     t = lax.axis_index("tp")
@@ -240,8 +240,9 @@
     pre_up = dot(normed, up_v[...])
     hidden = (jax.nn.silu(pre_gate) * pre_up).astype(BF16)
     loads[2].wait()
-    for m, p in enumerate((p0, p1, p2, p3)):
-        p[...] = dot(hidden, down_v[:, cols_of(t ^ m, quarter)]).astype(BF16)
+    for m, pair in ((1, beside), (3, beside), (0, own), (2, own)):
+        near = pl.ds((m // 2) * quarter, quarter)
+        pair[:, near] = dot(hidden, down_v[:, cols_of(t ^ m, quarter)]).astype(BF16)
 
 
 def enter_kernel(capacity, arrived, gains, w0, w1, w2, w3, keep, send, wide, rows, sums):
@@ -303,7 +304,7 @@
 
 
 def final_kernel(
-    capacity, returned, w, share0, share1, resid, blend, p0, p1, p2, p3, out, wide, rows
+    capacity, returned, w, share0, share1, resid, blend, own, came, last, out, wide, rows
 ):
     count, quarter = resid.shape
     wide[...] = returned[...].astype(F32)
@@ -314,9 +315,7 @@
     for c in range(quarter // lanes):
         cols = slice(c * lanes, (c + 1) * lanes)
         moe = share0[...] * picked[0:count, cols] + share1[...] * picked[count:, cols]
-        dense = (p0[:, cols].astype(F32) + p1[:, cols].astype(F32)) + (
-            p2[:, cols].astype(F32) + p3[:, cols].astype(F32)
-        )
+        dense = (own[:, cols].astype(F32) + came[:, cols].astype(F32)) + last[:, cols].astype(F32)
         out[:, cols] = (resid[:, cols].astype(F32) + moe + blend[...] * dense).astype(BF16)
 
 
@@ -446,17 +445,17 @@
     ).reshape(slots * blocks, lanes)
     near = [resid16, exchanged(resid16, 1), across, exchanged(across, 1)]
     gains = ffn_gain.reshape(1, width)
-    *dense, blend = call(
+    dense_own, dense_beside, blend = call(
         dense_kernel,
-        [piece] * 4 + [((rows, lanes), F32)],
+        [((rows, 2 * quarter), BF16)] * 2 + [((rows, lanes), F32)],
         [pltpu.VMEM((rows, width), BF16)]
         + [pltpu.VMEM(x.shape, BF16) for x in (dense_gate, dense_up, dense_down)]
         + [pltpu.SemaphoreType.DMA((3,))],
         12,
         [VMEM] * 6 + [HBM] * 3,
-        [OUT] * 5,
+        [OUT] * 3,
     )(gains, *near, blend_weight.reshape(1, width), dense_gate, dense_up, dense_down)
-    dense = [dense[0]] + [exchanged(dense[m], m) for m in (1, 2, 3)]
+    dense_came = exchanged(dense_beside, 1)
     keep, send = call(
         functools.partial(enter_kernel, capacity),
         [((slots + 8, 4 * hid), F32), ((slots + 8, 4 * hid), BF16)],
@@ -466,6 +465,8 @@
     came = exchanged(send, 1)
     (onward,) = call(relay_kernel, [((slots + 16, 2 * hid), BF16)])(keep, came)
     last = exchanged(onward, 2)
+    (dense_onward,) = call(half_kernel, [piece], out_specs=[OUT])(dense_own, dense_came)
+    dense_last = exchanged(dense_onward, 2)
     (hidden,) = call(
         functools.partial(hidden_kernel, float(width)), [((slots, hid), BF16)]
     )(keep, came, last)
@@ -486,7 +487,7 @@
         [wide, pltpu.VMEM((slots, quarter), BF16)],
         8,
         out_specs=[FREE],
-    )(returned, w, share0, share1, resid16, blend, *dense)
+    )(returned, w, share0, share1, resid16, blend, dense_own, dense_came, dense_last)
     return (new_tokens, new_re, new_im)
 
 

time: 102 us -> 101 us (level)
  the two profiles are of different devices: /device:TPU:1 before, /device:TPU:32 now
where the time goes in v6:
time: 101 us; the launch traced here: 98.9 us
  waiting for transfers between devices  43.8 us (43%)
  starting transfers between devices  35.9 us (36%)
  Pallas kernels  13.9 us (14%)
  local copies, waits for them, and re-layouts  4.44 us (4%)
    ppermute x18, waiting for transfers between devices, exchanged(): return lax.ppermute(value, 'tp', [(i, i ^ mask) for i in range(4)])  43.8 us
    all_to_all x1, starting transfers between devices, per_device(): lax.all_to_all(packed.reshape(ep, capacity * blocks, lanes), 'ep', 0, 0,...  14.2 us
    pallas_call x12, Pallas kernels, run(): pl.pallas_call(kernel, out_shape=tuple(out_shape), in_specs=specs, out_sp...  13.9 us
    all_to_all x1, starting transfers between devices, per_device(): lax.all_to_all(sent.reshape(ep, capacity * blocks, lanes), 'ep', 0, 0, ti...  12.2 us
    ppermute x18, starting transfers between devices, exchanged(): return lax.ppermute(value, 'tp', [(i, i ^ mask) for i in range(4)])  9.48 us
    unnamed x38, local copies, waits for them, and re-layouts  4.43 us
  transfers between devices with their start and end apart: 20, of which 13 were waited for; matrix products, arithmetic and copies ran while one was open for 2% of the time, Pallas kernels for 5%

profile of v6, /device:TPU:32, one launch (start us, length us, event | category | flops | bytes accessed | tf_op | source)
XLA Modules:
  0.0 98.9 jit_solution(7277341108720907947)
XLA Ops:
  0.7 3.6 %shard_map.247 = (bf16[96,1024]{1,0:T(8,128)(2,1)S(1)}, bf16[96,1024]{1,0:T(8,128)(2,1)S(1)}, f32[96,1024]{1,0:T(8,128)S(1)}, f32[96,1024]{1,0:T(8,128)S(1)}) custom-call(f32[16]{0:T(128)} %refs_0_.1, f32[16,64]{1,0:T(8,128)} %refs_1_.1, f32[16,16]{1,0:T(8,128)} %refs_2_.1, f32[256,64]{1,0:T(8,128)} %bitcast.26, f32[256,64]{1,0:T(8,128)} %bitcast.27, ...), custom_call_target="tpu_custom_call" | custom-call | tf_op jit(solution)/shard_map/pallas_call | solution.py:336
  4.5 1.4 %collective-permute-done.came = bf16[96,1024]{1,0:T(8,128)(2,1)S(1)} collective-permute-done((bf16[96,1024]{1,0:T(8,128)(2,1)S(1)}, bf16[96,1024]{1,0:T(8,128)(2,1)S(1)}, u32[]{:S(2)}, u32[]{:S(2)}) %collective-permute-start) | collective-permute-done | bytes 196640 | tf_op jit(solution)/shard_map/ppermute | solution.py:43
  5.9 1.6 %collective-permute-start.1 = (bf16[96,512]{1,0:T(8,128)(2,1)S(1)}, bf16[96,512]{1,0:T(8,128)(2,1)S(1)}, u32[]{:S(2)}, u32[]{:S(2)}) collective-permute-start(bf16[96,512]{1,0:T(8,128)(2,1)S(1)} %shard_map.248), channel_id=1, source_target_pairs={{0,2},{1,3},{2,0},{3,1},{4,6},{5,7},{6,4},{7,5},{8,10},{9,11},{10,... | collective-permute-start | bytes 294920 | tf_op jit(solution)/shard_map/ppermute | solution.py:43
  7.9 3.0 %collective-permute-done.1.last = bf16[96,512]{1,0:T(8,128)(2,1)S(1)} collective-permute-done((bf16[96,512]{1,0:T(8,128)(2,1)S(1)}, bf16[96,512]{1,0:T(8,128)(2,1)S(1)}, u32[]{:S(2)}, u32[]{:S(2)}) %collective-permute-start.1) | collective-permute-done | bytes 98336 | tf_op jit(solution)/shard_map/ppermute | solution.py:43
  10.9 1.1 %shard_map.250 = (bf16[96,512]{1,0:T(8,128)(2,1)S(1)}, bf16[1536,128]{1,0:T(8,128)(2,1)}) custom-call(bf16[96,2048]{1,0:T(8,128)(2,1)S(1)} %copy-done, bf16[96,1024]{1,0:T(8,128)(2,1)S(1)} %get-tuple-element.26.own, bf16[96,1024]{1,0:T(8,128)(2,1)S(1)} %collective-permute-done.came, bf16[96,512]{1,0:T(8,128)(2,1)S(1)} %collective-permute-done.1.last, ...), custom_call_target="tpu_custom_call" | custom-call | tf_op jit(solution)/shard_map/pallas_call | solution.py:336
  11.9 14.2 %all-to-all-start = ((bf16[64,24,128]{2,1,0:T(8,128)(2,1)}), bf16[64,24,128]{2,1,0:T(8,128)(2,1)S(1)}, u32[]{:S(2)}, u32[]{:S(2)}) async-start(bf16[64,24,128]{2,1,0:T(8,128)(2,1)} %bitcast.9), calls=%async_computation | async-start | bytes 786432 | tf_op jit(solution)/shard_map/all_to_all | solution.py:443
  29.0 1.3 %collective-permute-start.4 = (bf16[512,256]{1,0:T(8,128)(2,1)S(1)}, bf16[512,256]{1,0:T(8,128)(2,1)S(1)}, u32[]{:S(2)}, u32[]{:S(2)}) collective-permute-start(bf16[512,256]{1,0:T(8,128)(2,1)S(1)} %get-tuple-element.33), channel_id=1, source_target_pairs={{0,3},{1,2},{2,1},{3,0},{4,7},{5,6},{6,5},{7,4},{8,11},{9,10},{10,... | collective-permute-start | bytes 786440 | tf_op jit(solution)/shard_map/ppermute | solution.py:43
  30.3 9.0 %collective-permute-done.3.w2 = bf16[512,256]{1,0:T(8,128)(2,1)S(1)} collective-permute-done((bf16[512,256]{1,0:T(8,128)(2,1)S(1)}, bf16[512,256]{1,0:T(8,128)(2,1)S(1)}, u32[]{:S(2)}, u32[]{:S(2)}) %collective-permute-start.3) | collective-permute-done | bytes 262176 | tf_op jit(solution)/shard_map/ppermute | solution.py:43
  39.3 5.3 %collective-permute-done.4.w3 = bf16[512,256]{1,0:T(8,128)(2,1)S(1)} collective-permute-done((bf16[512,256]{1,0:T(8,128)(2,1)S(1)}, bf16[512,256]{1,0:T(8,128)(2,1)S(1)}, u32[]{:S(2)}, u32[]{:S(2)}) %collective-permute-start.4) | collective-permute-done | bytes 262176 | tf_op jit(solution)/shard_map/ppermute | solution.py:43
  45.8 1.6 %collective-permute-done.5.came = bf16[392,512]{1,0:T(8,128)(2,1)S(1)} collective-permute-done((bf16[392,512]{1,0:T(8,128)(2,1)S(1)}, bf16[392,512]{1,0:T(8,128)(2,1)S(1)}, u32[]{:S(2)}, u32[]{:S(2)}) %collective-permute-start.5) | collective-permute-done | bytes 401440 | tf_op jit(solution)/shard_map/ppermute | solution.py:43
  47.5 1.0 collective-permute-start.6
  48.5 6.2 %collective-permute-done.6.last = bf16[400,256]{1,0:T(8,128)(2,1)S(1)} collective-permute-done((bf16[400,256]{1,0:T(8,128)(2,1)S(1)}, bf16[400,256]{1,0:T(8,128)(2,1)S(1)}, u32[]{:S(2)}, u32[]{:S(2)}) %collective-permute-start.6) | collective-permute-done | bytes 204832 | tf_op jit(solution)/shard_map/ppermute | solution.py:43
  56.0 1.2 %collective-permute-start.11 = (bf16[128,512]{1,0:T(8,128)(2,1)S(1)}, bf16[128,512]{1,0:T(8,128)(2,1)S(1)}, u32[]{:S(2)}, u32[]{:S(2)}) collective-permute-start(bf16[128,512]{1,0:T(8,128)(2,1)S(1)} %copy-done.13), channel_id=1, source_target_pairs={{0,2},{1,3},{2,0},{3,1},{4,6},{5,7},{6,4},{7,5},{8,10},{9,11},{10,... | collective-permute-start | bytes 393224 | tf_op jit(solution)/shard_map/ppermute | solution.py:43
  58.3 2.1 %collective-permute-done.8.h2 = bf16[384,128]{1,0:T(8,128)(2,1)S(1)} collective-permute-done((bf16[384,128]{1,0:T(8,128)(2,1)S(1)}, bf16[384,128]{1,0:T(8,128)(2,1)S(1)}, u32[]{:S(2)}, u32[]{:S(2)}) %collective-permute-start.8) | collective-permute-done | bytes 98336 | tf_op jit(solution)/shard_map/ppermute | solution.py:43
  60.4 2.8 %collective-permute-done.11.w2 = bf16[128,512]{1,0:T(8,128)(2,1)S(1)} collective-permute-done((bf16[128,512]{1,0:T(8,128)(2,1)S(1)}, bf16[128,512]{1,0:T(8,128)(2,1)S(1)}, u32[]{:S(2)}, u32[]{:S(2)}) %collective-permute-start.11) | collective-permute-done | bytes 131104 | tf_op jit(solution)/shard_map/ppermute | solution.py:43
  63.2 1.6 %collective-permute-done.12.w3 = bf16[128,512]{1,0:T(8,128)(2,1)S(1)} collective-permute-done((bf16[128,512]{1,0:T(8,128)(2,1)S(1)}, bf16[128,512]{1,0:T(8,128)(2,1)S(1)}, u32[]{:S(2)}, u32[]{:S(2)}) %collective-permute-start.12) | collective-permute-done | bytes 131104 | tf_op jit(solution)/shard_map/ppermute | solution.py:43
  64.8 1.4 %shard_map.255 = bf16[1536,128]{1,0:T(8,128)(2,1)} custom-call(bf16[384,128]{1,0:T(8,128)(2,1)S(1)} %shard_map.254.h0, bf16[384,128]{1,0:T(8,128)(2,1)S(1)} %collective-permute-done.7.h1, bf16[384,128]{1,0:T(8,128)(2,1)S(1)} %collective-permute-done.8.h2, bf16[384,128]{1,0:T(8,128)(2,1)S(1)} %collective-permute-done.9.h3, ...), custom_call_target="tpu_custom_call" | custom-call | tf_op jit(solution)/shard_map/pallas_call | solution.py:336
  66.1 12.2 %all-to-all-start.1 = ((bf16[64,24,128]{2,1,0:T(8,128)(2,1)}), bf16[64,24,128]{2,1,0:T(8,128)(2,1)S(1)}, u32[]{:S(2)}, u32[]{:S(2)}) async-start(bf16[64,24,128]{2,1,0:T(8,128)(2,1)} %bitcast.14), calls=%async_computation.1 | async-start | bytes 786432 | tf_op jit(solution)/shard_map/all_to_all | solution.py:481
  78.9 5.0 %collective-permute-done.14.a2 = bf16[96,512]{1,0:T(8,128)(2,1)S(1)} collective-permute-done((bf16[96,512]{1,0:T(8,128)(2,1)S(1)}, bf16[96,512]{1,0:T(8,128)(2,1)S(1)}, u32[]{:S(2)}, u32[]{:S(2)}) %collective-permute-start.14) | collective-permute-done | bytes 98336 | tf_op jit(solution)/shard_map/ppermute | solution.py:43
  84.0 1.3 %collective-permute-done.15.a3 = bf16[96,512]{1,0:T(8,128)(2,1)S(1)} collective-permute-done((bf16[96,512]{1,0:T(8,128)(2,1)S(1)}, bf16[96,512]{1,0:T(8,128)(2,1)S(1)}, u32[]{:S(2)}, u32[]{:S(2)}) %collective-permute-start.15) | collective-permute-done | bytes 98336 | tf_op jit(solution)/shard_map/ppermute | solution.py:43
  85.3 4.2 %shard_map.256 = (bf16[96,1024]{1,0:T(8,128)(2,1)}, bf16[96,1024]{1,0:T(8,128)(2,1)}, f32[96,128]{1,0:T(8,128)}) custom-call(bf16[1,2048]{1,0:T(2,128)(2,1)S(1)} %reshape.55.gains, bf16[96,512]{1,0:T(8,128)(2,1)S(1)} %get-tuple-element.43.a0.resid, bf16[96,512]{1,0:T(8,128)(2,1)S(1)} %collective-permute-done.13.a1, ...), custom_call_target="tpu_custom_call" | custom-call | tf_op jit(solution)/shard_map/pallas_call | solution.py:336
  89.7 1.5 %collective-permute-done.16.came = bf16[96,1024]{1,0:T(8,128)(2,1)S(1)} collective-permute-done((bf16[96,1024]{1,0:T(8,128)(2,1)}, bf16[96,1024]{1,0:T(8,128)(2,1)S(1)}, u32[]{:S(2)}, u32[]{:S(2)}) %collective-permute-start.16) | collective-permute-done | bytes 196640 | tf_op jit(solution)/shard_map/ppermute | solution.py:43
  94.9 2.9 %collective-permute-done.17.last = bf16[96,512]{1,0:T(8,128)(2,1)S(1)} collective-permute-done((bf16[96,512]{1,0:T(8,128)(2,1)}, bf16[96,512]{1,0:T(8,128)(2,1)S(1)}, u32[]{:S(2)}, u32[]{:S(2)}) %collective-permute-start.17) | collective-permute-done | bytes 98336 | tf_op jit(solution)/shard_map/ppermute | solution.py:43
  97.8 1.1 %shard_map.258 = bf16[96,512]{1,0:T(8,128)(2,1)} custom-call(bf16[1536,128]{1,0:T(8,128)(2,1)S(1)} %bitcast.18, bf16[192,384]{1,0:T(8,128)(2,1)S(1)} %get-tuple-element.40.w, f32[96,128]{1,0:T(8,128)S(1)} %get-tuple-element.41.share0, f32[96,128]{1,0:T(8,128)S(1)} %get-tuple-element.42.share1, bf16[96,512]{1,0:T(8,128)(2,1)S(1)} %get-tuple-element.43.a0.resid, ...), custom_call_target="tpu_custom_call" | custom-call | tf_op jit(solution)/shard_map/pallas_call | solution.py:336
  (68 shorter events, 11.4 us)
Async XLA Ops:
  4.3 21.9 %copy-start.3 = (bf16[1,2048,128]{2,1,0:T(8,128)(2,1)S(1)}, bf16[1,2048,128]{2,1,0:T(8,128)(2,1)}, u32[]{:S(2)}) copy-start(bf16[1,2048,128]{2,1,0:T(8,128)(2,1)} %param.41) | copy-start | bytes 1572868
  4.3 21.9 %copy-start.4 = (bf16[1,2048,128]{2,1,0:T(8,128)(2,1)S(1)}, bf16[1,2048,128]{2,1,0:T(8,128)(2,1)}, u32[]{:S(2)}) copy-start(bf16[1,2048,128]{2,1,0:T(8,128)(2,1)} %param.42) | copy-start | bytes 1572868
  4.4 25.9 %copy-start.16 = (bf16[2048]{0:T(1024)(128)(2,1)S(1)}, bf16[2048]{0:T(1024)(128)(2,1)}, u32[]{:S(2)}) copy-start(bf16[2048]{0:T(1024)(128)(2,1)} %param.37) | copy-start | bytes 12292
  4.4 1.5 %collective-permute-start = (bf16[96,1024]{1,0:T(8,128)(2,1)S(1)}, bf16[96,1024]{1,0:T(8,128)(2,1)S(1)}, u32[]{:S(2)}, u32[]{:S(2)}) collective-permute-start(bf16[96,1024]{1,0:T(8,128)(2,1)S(1)} %get-tuple-element.27), channel_id=1, source_target_pairs={{0,1},{1,0},{2,3},{3,2},{4,5},{5,4},{6,7},{7,6},{8,9},{9,8},{10,11... | collective-permute-start | bytes 589832 | tf_op jit(solution)/shard_map/ppermute | solution.py:43
  5.9 4.9 %collective-permute-start.1 = (bf16[96,512]{1,0:T(8,128)(2,1)S(1)}, bf16[96,512]{1,0:T(8,128)(2,1)S(1)}, u32[]{:S(2)}, u32[]{:S(2)}) collective-permute-start(bf16[96,512]{1,0:T(8,128)(2,1)S(1)} %shard_map.248), channel_id=1, source_target_pairs={{0,2},{1,3},{2,0},{3,1},{4,6},{5,7},{6,4},{7,5},{8,10},{9,11},{10,... | collective-permute-start | bytes 294920 | tf_op jit(solution)/shard_map/ppermute | solution.py:43
  11.9 32.7 %all-to-all-start = ((bf16[64,24,128]{2,1,0:T(8,128)(2,1)}), bf16[64,24,128]{2,1,0:T(8,128)(2,1)S(1)}, u32[]{:S(2)}, u32[]{:S(2)}) async-start(bf16[64,24,128]{2,1,0:T(8,128)(2,1)} %bitcast.9), calls=%async_computation | async-start | bytes 786432 | tf_op jit(solution)/shard_map/all_to_all | solution.py:443
  28.4 1.9 %collective-permute-start.2 = (bf16[512,256]{1,0:T(8,128)(2,1)S(1)}, bf16[512,256]{1,0:T(8,128)(2,1)S(1)}, u32[]{:S(2)}, u32[]{:S(2)}) collective-permute-start(bf16[512,256]{1,0:T(8,128)(2,1)S(1)} %get-tuple-element.31), channel_id=1, source_target_pairs={{0,1},{1,0},{2,3},{3,2},{4,5},{5,4},{6,7},{7,6},{8,9},{9,8},{10,11... | collective-permute-start | bytes 786440 | tf_op jit(solution)/shard_map/ppermute | solution.py:43
  28.4 10.9 %collective-permute-start.3 = (bf16[512,256]{1,0:T(8,128)(2,1)S(1)}, bf16[512,256]{1,0:T(8,128)(2,1)S(1)}, u32[]{:S(2)}, u32[]{:S(2)}) collective-permute-start(bf16[512,256]{1,0:T(8,128)(2,1)S(1)} %get-tuple-element.32), channel_id=1, source_target_pairs={{0,2},{1,3},{2,0},{3,1},{4,6},{5,7},{6,4},{7,5},{8,10},{9,11},{10,... | collective-permute-start | bytes 786440 | tf_op jit(solution)/shard_map/ppermute | solution.py:43
  29.0 15.6 %collective-permute-start.4 = (bf16[512,256]{1,0:T(8,128)(2,1)S(1)}, bf16[512,256]{1,0:T(8,128)(2,1)S(1)}, u32[]{:S(2)}, u32[]{:S(2)}) collective-permute-start(bf16[512,256]{1,0:T(8,128)(2,1)S(1)} %get-tuple-element.33), channel_id=1, source_target_pairs={{0,3},{1,2},{2,1},{3,0},{4,7},{5,6},{6,5},{7,4},{8,11},{9,10},{10,... | collective-permute-start | bytes 786440 | tf_op jit(solution)/shard_map/ppermute | solution.py:43
  45.6 1.8 %collective-permute-start.5 = (bf16[392,512]{1,0:T(8,128)(2,1)S(1)}, bf16[392,512]{1,0:T(8,128)(2,1)S(1)}, u32[]{:S(2)}, u32[]{:S(2)}) collective-permute-start(bf16[392,512]{1,0:T(8,128)(2,1)S(1)} %get-tuple-element.35), channel_id=1, source_target_pairs={{0,1},{1,0},{2,3},{3,2},{4,5},{5,4},{6,7},{7,6},{8,9},{9,8},{10,11... | collective-permute-start | bytes 1204232 | tf_op jit(solution)/shard_map/ppermute | solution.py:43
  47.5 36.4 %copy-start.17 = (bf16[2048]{0:T(1024)(128)(2,1)S(1)}, bf16[2048]{0:T(1024)(128)(2,1)}, u32[]{:S(2)}) copy-start(bf16[2048]{0:T(1024)(128)(2,1)} %param.47) | copy-start | bytes 12292
  47.5 7.2 %collective-permute-start.6 = (bf16[400,256]{1,0:T(8,128)(2,1)S(1)}, bf16[400,256]{1,0:T(8,128)(2,1)S(1)}, u32[]{:S(2)}, u32[]{:S(2)}) collective-permute-start(bf16[400,256]{1,0:T(8,128)(2,1)S(1)} %shard_map.253), channel_id=1, source_target_pairs={{0,2},{1,3},{2,0},{3,1},{4,6},{5,7},{6,4},{7,5},{8,10},{9,11},{10,... | collective-permute-start | bytes 614408 | tf_op jit(solution)/shard_map/ppermute | solution.py:43
  55.0 5.3 %collective-permute-start.8 = (bf16[384,128]{1,0:T(8,128)(2,1)S(1)}, bf16[384,128]{1,0:T(8,128)(2,1)S(1)}, u32[]{:S(2)}, u32[]{:S(2)}) collective-permute-start(bf16[384,128]{1,0:T(8,128)(2,1)S(1)} %shard_map.254.h0), channel_id=1, source_target_pairs={{0,2},{1,3},{2,0},{3,1},{4,6},{5,7},{6,4},{7,5},{8,10},{9,11},{10,... | collective-permute-start | bytes 294920 | tf_op jit(solution)/shard_map/ppermute | solution.py:43
  56.0 4.3 %collective-permute-start.10 = (bf16[128,512]{1,0:T(8,128)(2,1)S(1)}, bf16[128,512]{1,0:T(8,128)(2,1)S(1)}, u32[]{:S(2)}, u32[]{:S(2)}) collective-permute-start(bf16[128,512]{1,0:T(8,128)(2,1)S(1)} %copy-done.15), channel_id=1, source_target_pairs={{0,1},{1,0},{2,3},{3,2},{4,5},{5,4},{6,7},{7,6},{8,9},{9,8},{10,11... | collective-permute-start | bytes 393224 | tf_op jit(solution)/shard_map/ppermute | solution.py:43
  56.0 7.1 %collective-permute-start.11 = (bf16[128,512]{1,0:T(8,128)(2,1)S(1)}, bf16[128,512]{1,0:T(8,128)(2,1)S(1)}, u32[]{:S(2)}, u32[]{:S(2)}) collective-permute-start(bf16[128,512]{1,0:T(8,128)(2,1)S(1)} %copy-done.13), channel_id=1, source_target_pairs={{0,2},{1,3},{2,0},{3,1},{4,6},{5,7},{6,4},{7,5},{8,10},{9,11},{10,... | collective-permute-start | bytes 393224 | tf_op jit(solution)/shard_map/ppermute | solution.py:43
  57.3 7.5 %collective-permute-start.12 = (bf16[128,512]{1,0:T(8,128)(2,1)S(1)}, bf16[128,512]{1,0:T(8,128)(2,1)S(1)}, u32[]{:S(2)}, u32[]{:S(2)}) collective-permute-start(bf16[128,512]{1,0:T(8,128)(2,1)S(1)} %copy-done.11), channel_id=1, source_target_pairs={{0,3},{1,2},{2,1},{3,0},{4,7},{5,6},{6,5},{7,4},{8,11},{9,10},{10,... | collective-permute-start | bytes 393224 | tf_op jit(solution)/shard_map/ppermute | solution.py:43
  57.9 6.9 %collective-permute-start.7 = (bf16[384,128]{1,0:T(8,128)(2,1)S(1)}, bf16[384,128]{1,0:T(8,128)(2,1)S(1)}, u32[]{:S(2)}, u32[]{:S(2)}) collective-permute-start(bf16[384,128]{1,0:T(8,128)(2,1)S(1)} %shard_map.254.h0), channel_id=1, source_target_pairs={{0,1},{1,0},{2,3},{3,2},{4,5},{5,4},{6,7},{7,6},{8,9},{9,8},{10,11... | collective-permute-start | bytes 294920 | tf_op jit(solution)/shard_map/ppermute | solution.py:43
  60.4 4.4 %collective-permute-start.9 = (bf16[384,128]{1,0:T(8,128)(2,1)S(1)}, bf16[384,128]{1,0:T(8,128)(2,1)S(1)}, u32[]{:S(2)}, u32[]{:S(2)}) collective-permute-start(bf16[384,128]{1,0:T(8,128)(2,1)S(1)} %collective-permute-done.8.h2), channel_id=1, source_target_pairs={{0,1},{1,0},{2,3},{3,2},{4,5},{5,4},{6,7},{7,6},{8,9},{9,8},{10,11... | collective-permute-start | bytes 294920 | tf_op jit(solution)/shard_map/ppermute | solution.py:43
  66.1 31.7 %all-to-all-start.1 = ((bf16[64,24,128]{2,1,0:T(8,128)(2,1)}), bf16[64,24,128]{2,1,0:T(8,128)(2,1)S(1)}, u32[]{:S(2)}, u32[]{:S(2)}) async-start(bf16[64,24,128]{2,1,0:T(8,128)(2,1)} %bitcast.14), calls=%async_computation.1 | async-start | bytes 786432 | tf_op jit(solution)/shard_map/all_to_all | solution.py:481
  78.3 5.7 %collective-permute-start.14 = (bf16[96,512]{1,0:T(8,128)(2,1)S(1)}, bf16[96,512]{1,0:T(8,128)(2,1)S(1)}, u32[]{:S(2)}, u32[]{:S(2)}) collective-permute-start(bf16[96,512]{1,0:T(8,128)(2,1)S(1)} %get-tuple-element.43.a0.resid), channel_id=1, source_target_pairs={{0,2},{1,3},{2,0},{3,1},{4,6},{5,7},{6,4},{7,5},{8,10},{9,11},{10,... | collective-permute-start | bytes 294920 | tf_op jit(solution)/shard_map/ppermute | solution.py:43
  78.9 5.1 %collective-permute-start.13 = (bf16[96,512]{1,0:T(8,128)(2,1)S(1)}, bf16[96,512]{1,0:T(8,128)(2,1)S(1)}, u32[]{:S(2)}, u32[]{:S(2)}) collective-permute-start(bf16[96,512]{1,0:T(8,128)(2,1)S(1)} %get-tuple-element.43.a0.resid), channel_id=1, source_target_pairs={{0,1},{1,0},{2,3},{3,2},{4,5},{5,4},{6,7},{7,6},{8,9},{9,8},{10,11... | collective-permute-start | bytes 294920 | tf_op jit(solution)/shard_map/ppermute | solution.py:43
  84.0 1.3 %collective-permute-start.15 = (bf16[96,512]{1,0:T(8,128)(2,1)S(1)}, bf16[96,512]{1,0:T(8,128)(2,1)S(1)}, u32[]{:S(2)}, u32[]{:S(2)}) collective-permute-start(bf16[96,512]{1,0:T(8,128)(2,1)S(1)} %collective-permute-done.14.a2), channel_id=1, source_target_pairs={{0,1},{1,0},{2,3},{3,2},{4,5},{5,4},{6,7},{7,6},{8,9},{9,8},{10,11... | collective-permute-start | bytes 294920 | tf_op jit(solution)/shard_map/ppermute | solution.py:43
  89.4 1.7 %collective-permute-start.16 = (bf16[96,1024]{1,0:T(8,128)(2,1)}, bf16[96,1024]{1,0:T(8,128)(2,1)S(1)}, u32[]{:S(2)}, u32[]{:S(2)}) collective-permute-start(bf16[96,1024]{1,0:T(8,128)(2,1)} %get-tuple-element.46), channel_id=1, source_target_pairs={{0,1},{1,0},{2,3},{3,2},{4,5},{5,4},{6,7},{7,6},{8,9},{9,8},{10,11... | collective-permute-start | bytes 589832 | tf_op jit(solution)/shard_map/ppermute | solution.py:43
  92.8 5.1 %collective-permute-start.17 = (bf16[96,512]{1,0:T(8,128)(2,1)}, bf16[96,512]{1,0:T(8,128)(2,1)S(1)}, u32[]{:S(2)}, u32[]{:S(2)}) collective-permute-start(bf16[96,512]{1,0:T(8,128)(2,1)} %shard_map.257), channel_id=1, source_target_pairs={{0,2},{1,3},{2,0},{3,1},{4,6},{5,7},{6,4},{7,5},{8,10},{9,11},{10,... | collective-permute-start | bytes 294920 | tf_op jit(solution)/shard_map/ppermute | solution.py:43
  (14 other events, 102.5 us)

commit v7 on v6

--- a/solution.py
+++ b/solution.py
@@ -48,14 +48,17 @@
     return [value, exchanged(value, 1), across, exchanged(across, 1)]
 
 
-def spread_blocks(small, channels):
+def spread_blocks(out, small, channels):
     rows, entries = small.shape
-    groups = rows // channels
-    width = groups * entries
+    width = 2 * entries
     tiler = (iota((entries, width), 1) % entries == iota((entries, width), 0)).astype(BF16)
     tiled = dot(small.astype(BF16), tiler)
-    mine = iota((rows, width), 0) // channels == iota((rows, width), 1) // entries
-    return jnp.where(mine, tiled, 0.0).astype(BF16)
+    mine = iota((rows, width), 0) // channels % 2 == iota((rows, width), 1) // entries
+    tiled = jnp.where(mine, tiled, 0.0).astype(BF16)
+    out[...] = jnp.zeros(out.shape, BF16)
+    for pair in range(rows // (2 * channels)):
+        near = slice(2 * channels * pair, 2 * channels * (pair + 1))
+        out[near, width * pair : width * (pair + 1)] = tiled[near, :]
 
 
 def row_of(small):
@@ -100,7 +103,7 @@
     for load in loads[3:7]:
         load.wait()
     for k, small in enumerate((b_re, b_im, c_re, c_im)):
-        blocks_v[k] = spread_blocks(small[...], channels)
+        spread_blocks(blocks_v.at[k], small[...], channels)
     loads[7].wait()
     loads[8].wait()
     x = tokens_v[...].astype(F32)
@@ -245,29 +248,33 @@
         pair[:, near] = dot(hidden, down_v[:, cols_of(t ^ m, quarter)]).astype(BF16)
 
 
-def enter_kernel(capacity, arrived, gains, w0, w1, w2, w3, keep, send, wide, rows, sums):
+def enter_kernel(capacity, arrived, gains, w1, w3, send, rows, squares, wide, sums):
     t = lax.axis_index("tp")
     lanes = arrived.shape[1]
-    quarter = rows.shape[1]
+    count, quarter = rows.shape
     wide[...] = arrived[...].astype(F32)
     gain = gains[:, cols_of(t, quarter)].astype(F32)
     for strided, near, cols in places(capacity, wide, quarter):
         x = wide[strided, :]
         sums[near, :] = x * x if cols.start == 0 else sums[near, :] + x * x
         rows[near, cols] = (x * gain[:, cols]).astype(BF16)
-    squares = nt_dot(jnp.ones((8, lanes), F32), sums[...], HIGHEST)[0:1]
+    total = nt_dot(jnp.ones((8, lanes), F32), sums[...], HIGHEST)
+    squares[...] = total
+    send[count:, :] = three_terms(total[0:1], send.shape[1])
+    pair = w1.shape[1]
+    x = rows[...]
+    send[0:count, 0:pair] = dot(x, w1[...]).astype(BF16)
+    send[0:count, pair:] = dot(x, w3[...]).astype(BF16)
+
+
+def stay_kernel(rows, squares, w0, w2, keep):
     count = rows.shape[0]
-    keep[count:, :] = jnp.broadcast_to(
-        jnp.concatenate([squares, jnp.zeros((1, keep.shape[1] - count), F32)], axis=1),
-        (8, keep.shape[1]),
-    )
-    send[count:, :] = three_terms(squares, send.shape[1])
+    gap = jnp.zeros((8, keep.shape[1] - count), F32)
+    keep[count:, :] = jnp.concatenate([squares[...], gap], axis=1)
+    pair = w0.shape[1]
     x = rows[...]
-    pair = w0.shape[1]
     keep[0:count, 0:pair] = dot(x, w0[...])
-    send[0:count, 0:pair] = dot(x, w1[...]).astype(BF16)
     keep[0:count, pair:] = dot(x, w2[...])
-    send[0:count, pair:] = dot(x, w3[...]).astype(BF16)
 
 
 def relay_kernel(keep, came, onward):
@@ -445,6 +452,16 @@
     ).reshape(slots * blocks, lanes)
     near = [resid16, exchanged(resid16, 1), across, exchanged(across, 1)]
     gains = ffn_gain.reshape(1, width)
+    send, x_rows, squares = call(
+        functools.partial(enter_kernel, capacity),
+        [((slots + 8, 4 * hid), BF16), ((slots, quarter), BF16), ((8, slots), F32)],
+        [wide, pltpu.VMEM((slots, lanes), F32)],
+        8,
+    )(arrived, gains, moved[1], moved[3])
+    came = exchanged(send, 1)
+    (keep,) = call(stay_kernel, [((slots + 8, 4 * hid), F32)])(x_rows, squares, moved[0], moved[2])
+    (onward,) = call(relay_kernel, [((slots + 16, 2 * hid), BF16)])(keep, came)
+    last = exchanged(onward, 2)
     dense_own, dense_beside, blend = call(
         dense_kernel,
         [((rows, 2 * quarter), BF16)] * 2 + [((rows, lanes), F32)],
@@ -456,15 +473,6 @@
         [OUT] * 3,
     )(gains, *near, blend_weight.reshape(1, width), dense_gate, dense_up, dense_down)
     dense_came = exchanged(dense_beside, 1)
-    keep, send = call(
-        functools.partial(enter_kernel, capacity),
-        [((slots + 8, 4 * hid), F32), ((slots + 8, 4 * hid), BF16)],
-        [wide, pltpu.VMEM((slots, quarter), BF16), pltpu.VMEM((slots, lanes), F32)],
-        8,
-    )(arrived, gains, *moved)
-    came = exchanged(send, 1)
-    (onward,) = call(relay_kernel, [((slots + 16, 2 * hid), BF16)])(keep, came)
-    last = exchanged(onward, 2)
     (dense_onward,) = call(half_kernel, [piece], out_specs=[OUT])(dense_own, dense_came)
     dense_last = exchanged(dense_onward, 2)
     (hidden,) = call(

time: 101 us -> 102 us (level)
  waiting for transfers between devices: 43.8 us -> 48.1 us
  starting transfers between devices: 35.9 us -> 32.1 us
    all_to_all x1, waiting for transfers between devices: 0.01 us -> 3.11 us  [per_device(): lax.all_to_all(packed.reshape(ep, capacity * blocks, lanes), 'ep', 0, 0,...]
    all_to_all x1, starting transfers between devices: 12.2 us -> 9.68 us  [per_device(): lax.all_to_all(sent.reshape(ep, capacity * blocks, lanes), 'ep', 0, 0, ti...]
    ppermute x18, starting transfers between devices: 9.48 us -> 8.18 us  [exchanged(): return lax.ppermute(value, 'tp', [(i, i ^ mask) for i in range(4)])]
    ppermute x18, waiting for transfers between devices: 43.8 us -> 45 us  [exchanged(): return lax.ppermute(value, 'tp', [(i, i ^ mask) for i in range(4)])]
    unnamed x38 -> x40, local copies, waits for them, and re-layouts: 4.43 us -> 5.13 us
    pallas_call x12 -> x13, Pallas kernels: 13.9 us -> 13.9 us  [run(): pl.pallas_call(kernel, out_shape=tuple(out_shape), in_specs=specs, out_sp...]
  transfers between devices with their start and end apart: 20 -> 20, of which waited for: 13 -> 14; matrix products, arithmetic and copies ran while one was open for 2% -> 2% of each run, Pallas kernels for 5% -> 6%
where the time goes in v7:
time: 102 us; the launch traced here: 100 us
  waiting for transfers between devices  48.1 us (47%)
  starting transfers between devices  32.1 us (31%)
  Pallas kernels  13.9 us (14%)
  local copies, waits for them, and re-layouts  5.14 us (5%)
    ppermute x18, waiting for transfers between devices, exchanged(): return lax.ppermute(value, 'tp', [(i, i ^ mask) for i in range(4)])  45 us
    all_to_all x1, starting transfers between devices, per_device(): lax.all_to_all(packed.reshape(ep, capacity * blocks, lanes), 'ep', 0, 0,...  14.2 us
    pallas_call x13, Pallas kernels, run(): pl.pallas_call(kernel, out_shape=tuple(out_shape), in_specs=specs, out_sp...  13.9 us
    all_to_all x1, starting transfers between devices, per_device(): lax.all_to_all(sent.reshape(ep, capacity * blocks, lanes), 'ep', 0, 0, ti...  9.68 us
    ppermute x18, starting transfers between devices, exchanged(): return lax.ppermute(value, 'tp', [(i, i ^ mask) for i in range(4)])  8.18 us
    unnamed x40, local copies, waits for them, and re-layouts  5.13 us
    all_to_all x1, waiting for transfers between devices, per_device(): lax.all_to_all(packed.reshape(ep, capacity * blocks, lanes), 'ep', 0, 0,...  3.11 us
  transfers between devices with their start and end apart: 20, of which 14 were waited for; matrix products, arithmetic and copies ran while one was open for 2% of the time, Pallas kernels for 6%

profile of v7, /device:TPU:32, one launch (start us, length us, event | category | flops | bytes accessed | tf_op | source)
XLA Modules:
  0.0 100.1 jit_solution(1862127704403605848)
XLA Ops:
  0.7 3.4 %shard_map.247 = (bf16[96,1024]{1,0:T(8,128)(2,1)S(1)}, bf16[96,1024]{1,0:T(8,128)(2,1)S(1)}, f32[96,1024]{1,0:T(8,128)S(1)}, f32[96,1024]{1,0:T(8,128)S(1)}) custom-call(f32[16]{0:T(128)} %refs_0_.1, f32[16,64]{1,0:T(8,128)} %refs_1_.1, f32[16,16]{1,0:T(8,128)} %refs_2_.1, f32[256,64]{1,0:T(8,128)} %bitcast.26, f32[256,64]{1,0:T(8,128)} %bitcast.27, ...), custom_call_target="tpu_custom_call" | custom-call | tf_op jit(solution)/shard_map/pallas_call | solution.py:343
  4.2 1.4 %collective-permute-done.came = bf16[96,1024]{1,0:T(8,128)(2,1)S(1)} collective-permute-done((bf16[96,1024]{1,0:T(8,128)(2,1)S(1)}, bf16[96,1024]{1,0:T(8,128)(2,1)S(1)}, u32[]{:S(2)}, u32[]{:S(2)}) %collective-permute-start) | collective-permute-done | bytes 196640 | tf_op jit(solution)/shard_map/ppermute | solution.py:43
  5.7 1.6 %collective-permute-start.1 = (bf16[96,512]{1,0:T(8,128)(2,1)S(1)}, bf16[96,512]{1,0:T(8,128)(2,1)S(1)}, u32[]{:S(2)}, u32[]{:S(2)}) collective-permute-start(bf16[96,512]{1,0:T(8,128)(2,1)S(1)} %shard_map.248), channel_id=1, source_target_pairs={{0,2},{1,3},{2,0},{3,1},{4,6},{5,7},{6,4},{7,5},{8,10},{9,11},{10,... | collective-permute-start | bytes 294920 | tf_op jit(solution)/shard_map/ppermute | solution.py:43
  7.6 3.0 %collective-permute-done.1.last = bf16[96,512]{1,0:T(8,128)(2,1)S(1)} collective-permute-done((bf16[96,512]{1,0:T(8,128)(2,1)S(1)}, bf16[96,512]{1,0:T(8,128)(2,1)S(1)}, u32[]{:S(2)}, u32[]{:S(2)}) %collective-permute-start.1) | collective-permute-done | bytes 98336 | tf_op jit(solution)/shard_map/ppermute | solution.py:43
  10.6 1.1 %shard_map.250 = (bf16[96,512]{1,0:T(8,128)(2,1)S(1)}, bf16[1536,128]{1,0:T(8,128)(2,1)}) custom-call(bf16[96,2048]{1,0:T(8,128)(2,1)S(1)} %copy-done, bf16[96,1024]{1,0:T(8,128)(2,1)S(1)} %get-tuple-element.27.own, bf16[96,1024]{1,0:T(8,128)(2,1)S(1)} %collective-permute-done.came, bf16[96,512]{1,0:T(8,128)(2,1)S(1)} %collective-permute-done.1.last, ...), custom_call_target="tpu_custom_call" | custom-call | tf_op jit(solution)/shard_map/pallas_call | solution.py:343
  11.7 14.2 %all-to-all-start = ((bf16[64,24,128]{2,1,0:T(8,128)(2,1)}), bf16[64,24,128]{2,1,0:T(8,128)(2,1)S(1)}, u32[]{:S(2)}, u32[]{:S(2)}) async-start(bf16[64,24,128]{2,1,0:T(8,128)(2,1)} %bitcast.9), calls=%async_computation | async-start | bytes 786432 | tf_op jit(solution)/shard_map/all_to_all | solution.py:450
  29.6 0.8 collective-permute-done.2.w1
  30.4 8.4 %collective-permute-done.3.w3 = bf16[512,256]{1,0:T(8,128)(2,1)S(1)} collective-permute-done((bf16[512,256]{1,0:T(8,128)(2,1)S(1)}, bf16[512,256]{1,0:T(8,128)(2,1)S(1)}, u32[]{:S(2)}, u32[]{:S(2)}) %collective-permute-start.3) | collective-permute-done | bytes 262176 | tf_op jit(solution)/shard_map/ppermute | solution.py:43
  38.8 3.1 %all-to-all-done = bf16[64,24,128]{2,1,0:T(8,128)(2,1)S(1)} async-done(((bf16[64,24,128]{2,1,0:T(8,128)(2,1)}), bf16[64,24,128]{2,1,0:T(8,128)(2,1)S(1)}, u32[]{:S(2)}, u32[]{:S(2)}) %all-to-all-start) | async-done | bytes 393248 | tf_op jit(solution)/shard_map/all_to_all | solution.py:450
  43.5 8.2 %collective-permute-done.4.w2 = bf16[512,256]{1,0:T(8,128)(2,1)S(1)} collective-permute-done((bf16[512,256]{1,0:T(8,128)(2,1)}, bf16[512,256]{1,0:T(8,128)(2,1)S(1)}, u32[]{:S(2)}, u32[]{:S(2)}) %collective-permute-start.4) | collective-permute-done | bytes 262176 | tf_op jit(solution)/shard_map/ppermute | solution.py:43
  52.9 5.9 %collective-permute-done.6.last = bf16[400,256]{1,0:T(8,128)(2,1)S(1)} collective-permute-done((bf16[400,256]{1,0:T(8,128)(2,1)S(1)}, bf16[400,256]{1,0:T(8,128)(2,1)S(1)}, u32[]{:S(2)}, u32[]{:S(2)}) %collective-permute-start.6) | collective-permute-done | bytes 204832 | tf_op jit(solution)/shard_map/ppermute | solution.py:43
  59.8 1.5 %collective-permute-start.11 = (bf16[128,512]{1,0:T(8,128)(2,1)S(1)}, bf16[128,512]{1,0:T(8,128)(2,1)S(1)}, u32[]{:S(2)}, u32[]{:S(2)}) collective-permute-start(bf16[128,512]{1,0:T(8,128)(2,1)S(1)} %copy-done.14), channel_id=1, source_target_pairs={{0,2},{1,3},{2,0},{3,1},{4,6},{5,7},{6,4},{7,5},{8,10},{9,11},{10,... | collective-permute-start | bytes 393224 | tf_op jit(solution)/shard_map/ppermute | solution.py:43
  62.1 2.7 %collective-permute-done.8.h2 = bf16[384,128]{1,0:T(8,128)(2,1)S(1)} collective-permute-done((bf16[384,128]{1,0:T(8,128)(2,1)S(1)}, bf16[384,128]{1,0:T(8,128)(2,1)S(1)}, u32[]{:S(2)}, u32[]{:S(2)}) %collective-permute-start.8) | collective-permute-done | bytes 98336 | tf_op jit(solution)/shard_map/ppermute | solution.py:43
  64.8 2.8 %collective-permute-done.11.w2 = bf16[128,512]{1,0:T(8,128)(2,1)S(1)} collective-permute-done((bf16[128,512]{1,0:T(8,128)(2,1)S(1)}, bf16[128,512]{1,0:T(8,128)(2,1)S(1)}, u32[]{:S(2)}, u32[]{:S(2)}) %collective-permute-start.11) | collective-permute-done | bytes 131104 | tf_op jit(solution)/shard_map/ppermute | solution.py:43
  67.6 1.0 collective-permute-done.12.w3
  68.6 1.4 %shard_map.256 = bf16[1536,128]{1,0:T(8,128)(2,1)} custom-call(bf16[384,128]{1,0:T(8,128)(2,1)S(1)} %shard_map.255.h0, bf16[384,128]{1,0:T(8,128)(2,1)S(1)} %collective-permute-done.7.h1, bf16[384,128]{1,0:T(8,128)(2,1)S(1)} %collective-permute-done.8.h2, bf16[384,128]{1,0:T(8,128)(2,1)S(1)} %collective-permute-done.9.h3, ...), custom_call_target="tpu_custom_call" | custom-call | tf_op jit(solution)/shard_map/pallas_call | solution.py:343
  69.9 9.7 %all-to-all-start.1 = ((bf16[64,24,128]{2,1,0:T(8,128)(2,1)}), bf16[64,24,128]{2,1,0:T(8,128)(2,1)S(1)}, u32[]{:S(2)}, u32[]{:S(2)}) async-start(bf16[64,24,128]{2,1,0:T(8,128)(2,1)} %bitcast.14), calls=%async_computation.1 | async-start | bytes 786432 | tf_op jit(solution)/shard_map/all_to_all | solution.py:489
  80.1 5.0 %collective-permute-done.14.a2 = bf16[96,512]{1,0:T(8,128)(2,1)S(1)} collective-permute-done((bf16[96,512]{1,0:T(8,128)(2,1)S(1)}, bf16[96,512]{1,0:T(8,128)(2,1)S(1)}, u32[]{:S(2)}, u32[]{:S(2)}) %collective-permute-start.14) | collective-permute-done | bytes 98336 | tf_op jit(solution)/shard_map/ppermute | solution.py:43
  85.1 1.3 %collective-permute-done.15.a3 = bf16[96,512]{1,0:T(8,128)(2,1)S(1)} collective-permute-done((bf16[96,512]{1,0:T(8,128)(2,1)S(1)}, bf16[96,512]{1,0:T(8,128)(2,1)S(1)}, u32[]{:S(2)}, u32[]{:S(2)}) %collective-permute-start.15) | collective-permute-done | bytes 98336 | tf_op jit(solution)/shard_map/ppermute | solution.py:43
  86.4 4.2 %shard_map.257 = (bf16[96,1024]{1,0:T(8,128)(2,1)}, bf16[96,1024]{1,0:T(8,128)(2,1)}, f32[96,128]{1,0:T(8,128)}) custom-call(bf16[1,2048]{1,0:T(2,128)(2,1)S(1)} %reshape.55.gains, bf16[96,512]{1,0:T(8,128)(2,1)S(1)} %get-tuple-element.45.a0.resid, bf16[96,512]{1,0:T(8,128)(2,1)S(1)} %collective-permute-done.13.a1, ...), custom_call_target="tpu_custom_call" | custom-call | tf_op jit(solution)/shard_map/pallas_call | solution.py:343
  90.8 1.5 %collective-permute-done.16.came = bf16[96,1024]{1,0:T(8,128)(2,1)S(1)} collective-permute-done((bf16[96,1024]{1,0:T(8,128)(2,1)}, bf16[96,1024]{1,0:T(8,128)(2,1)S(1)}, u32[]{:S(2)}, u32[]{:S(2)}) %collective-permute-start.16) | collective-permute-done | bytes 196640 | tf_op jit(solution)/shard_map/ppermute | solution.py:43
  92.3 0.9 copy-done.1
  96.1 2.9 %collective-permute-done.17.last = bf16[96,512]{1,0:T(8,128)(2,1)S(1)} collective-permute-done((bf16[96,512]{1,0:T(8,128)(2,1)}, bf16[96,512]{1,0:T(8,128)(2,1)S(1)}, u32[]{:S(2)}, u32[]{:S(2)}) %collective-permute-start.17) | collective-permute-done | bytes 98336 | tf_op jit(solution)/shard_map/ppermute | solution.py:43
  99.0 1.1 %shard_map.259 = bf16[96,512]{1,0:T(8,128)(2,1)} custom-call(bf16[1536,128]{1,0:T(8,128)(2,1)S(1)} %bitcast.19, bf16[192,384]{1,0:T(8,128)(2,1)S(1)} %get-tuple-element.42.w, f32[96,128]{1,0:T(8,128)S(1)} %get-tuple-element.43.share0, f32[96,128]{1,0:T(8,128)S(1)} %get-tuple-element.44.share1, bf16[96,512]{1,0:T(8,128)(2,1)S(1)} %get-tuple-element.45.a0.resid, ...), custom_call_target="tpu_custom_call" | custom-call | tf_op jit(solution)/shard_map/pallas_call | solution.py:343
  (71 shorter events, 12.1 us)
Async XLA Ops:
  4.1 21.8 %copy-start.3 = (bf16[1,2048,128]{2,1,0:T(8,128)(2,1)S(1)}, bf16[1,2048,128]{2,1,0:T(8,128)(2,1)}, u32[]{:S(2)}) copy-start(bf16[1,2048,128]{2,1,0:T(8,128)(2,1)} %param.41) | copy-start | bytes 1572868
  4.1 21.8 %copy-start.4 = (bf16[1,2048,128]{2,1,0:T(8,128)(2,1)S(1)}, bf16[1,2048,128]{2,1,0:T(8,128)(2,1)}, u32[]{:S(2)}) copy-start(bf16[1,2048,128]{2,1,0:T(8,128)(2,1)} %param.42) | copy-start | bytes 1572868
  4.1 25.4 %copy-start.17 = (bf16[2048]{0:T(1024)(128)(2,1)S(1)}, bf16[2048]{0:T(1024)(128)(2,1)}, u32[]{:S(2)}) copy-start(bf16[2048]{0:T(1024)(128)(2,1)} %param.37) | copy-start | bytes 12292
  4.1 1.5 %collective-permute-start = (bf16[96,1024]{1,0:T(8,128)(2,1)S(1)}, bf16[96,1024]{1,0:T(8,128)(2,1)S(1)}, u32[]{:S(2)}, u32[]{:S(2)}) collective-permute-start(bf16[96,1024]{1,0:T(8,128)(2,1)S(1)} %get-tuple-element.28), channel_id=1, source_target_pairs={{0,1},{1,0},{2,3},{3,2},{4,5},{5,4},{6,7},{7,6},{8,9},{9,8},{10,11... | collective-permute-start | bytes 589832 | tf_op jit(solution)/shard_map/ppermute | solution.py:43
  5.7 4.9 %collective-permute-start.1 = (bf16[96,512]{1,0:T(8,128)(2,1)S(1)}, bf16[96,512]{1,0:T(8,128)(2,1)S(1)}, u32[]{:S(2)}, u32[]{:S(2)}) collective-permute-start(bf16[96,512]{1,0:T(8,128)(2,1)S(1)} %shard_map.248), channel_id=1, source_target_pairs={{0,2},{1,3},{2,0},{3,1},{4,6},{5,7},{6,4},{7,5},{8,10},{9,11},{10,... | collective-permute-start | bytes 294920 | tf_op jit(solution)/shard_map/ppermute | solution.py:43
  11.7 30.2 %all-to-all-start = ((bf16[64,24,128]{2,1,0:T(8,128)(2,1)}), bf16[64,24,128]{2,1,0:T(8,128)(2,1)S(1)}, u32[]{:S(2)}, u32[]{:S(2)}) async-start(bf16[64,24,128]{2,1,0:T(8,128)(2,1)} %bitcast.9), calls=%async_computation | async-start | bytes 786432 | tf_op jit(solution)/shard_map/all_to_all | solution.py:450
  28.9 1.5 %collective-permute-start.2 = (bf16[512,256]{1,0:T(8,128)(2,1)S(1)}, bf16[512,256]{1,0:T(8,128)(2,1)S(1)}, u32[]{:S(2)}, u32[]{:S(2)}) collective-permute-start(bf16[512,256]{1,0:T(8,128)(2,1)S(1)} %get-tuple-element.31), channel_id=1, source_target_pairs={{0,1},{1,0},{2,3},{3,2},{4,5},{5,4},{6,7},{7,6},{8,9},{9,8},{10,11... | collective-permute-start | bytes 786440 | tf_op jit(solution)/shard_map/ppermute | solution.py:43
  28.9 10.0 %collective-permute-start.3 = (bf16[512,256]{1,0:T(8,128)(2,1)S(1)}, bf16[512,256]{1,0:T(8,128)(2,1)S(1)}, u32[]{:S(2)}, u32[]{:S(2)}) collective-permute-start(bf16[512,256]{1,0:T(8,128)(2,1)S(1)} %get-tuple-element.32), channel_id=1, source_target_pairs={{0,3},{1,2},{2,1},{3,0},{4,7},{5,6},{6,5},{7,4},{8,11},{9,10},{10,... | collective-permute-start | bytes 786440 | tf_op jit(solution)/shard_map/ppermute | solution.py:43
  42.7 9.4 %collective-permute-start.5 = (bf16[392,512]{1,0:T(8,128)(2,1)S(1)}, bf16[392,512]{1,0:T(8,128)(2,1)S(1)}, u32[]{:S(2)}, u32[]{:S(2)}) collective-permute-start(bf16[392,512]{1,0:T(8,128)(2,1)S(1)} %get-tuple-element.37), channel_id=1, source_target_pairs={{0,1},{1,0},{2,3},{3,2},{4,5},{5,4},{6,7},{7,6},{8,9},{9,8},{10,11... | collective-permute-start | bytes 1204232 | tf_op jit(solution)/shard_map/ppermute | solution.py:43
  42.8 8.9 %collective-permute-start.4 = (bf16[512,256]{1,0:T(8,128)(2,1)}, bf16[512,256]{1,0:T(8,128)(2,1)S(1)}, u32[]{:S(2)}, u32[]{:S(2)}) collective-permute-start(bf16[512,256]{1,0:T(8,128)(2,1)} %copy-done.10), channel_id=1, source_target_pairs={{0,2},{1,3},{2,0},{3,1},{4,6},{5,7},{6,4},{7,5},{8,10},{9,11},{10,... | collective-permute-start | bytes 786440 | tf_op jit(solution)/shard_map/ppermute | solution.py:43
  52.2 32.9 %copy-start.18 = (bf16[2048]{0:T(1024)(128)(2,1)S(1)}, bf16[2048]{0:T(1024)(128)(2,1)}, u32[]{:S(2)}) copy-start(bf16[2048]{0:T(1024)(128)(2,1)} %param.47) | copy-start | bytes 12292
  52.2 6.6 %collective-permute-start.6 = (bf16[400,256]{1,0:T(8,128)(2,1)S(1)}, bf16[400,256]{1,0:T(8,128)(2,1)S(1)}, u32[]{:S(2)}, u32[]{:S(2)}) collective-permute-start(bf16[400,256]{1,0:T(8,128)(2,1)S(1)} %shard_map.254), channel_id=1, source_target_pairs={{0,2},{1,3},{2,0},{3,1},{4,6},{5,7},{6,4},{7,5},{8,10},{9,11},{10,... | collective-permute-start | bytes 614408 | tf_op jit(solution)/shard_map/ppermute | solution.py:43
  59.1 5.6 %collective-permute-start.8 = (bf16[384,128]{1,0:T(8,128)(2,1)S(1)}, bf16[384,128]{1,0:T(8,128)(2,1)S(1)}, u32[]{:S(2)}, u32[]{:S(2)}) collective-permute-start(bf16[384,128]{1,0:T(8,128)(2,1)S(1)} %shard_map.255.h0), channel_id=1, source_target_pairs={{0,2},{1,3},{2,0},{3,1},{4,6},{5,7},{6,4},{7,5},{8,10},{9,11},{10,... | collective-permute-start | bytes 294920 | tf_op jit(solution)/shard_map/ppermute | solution.py:43
  59.8 4.9 %collective-permute-start.10 = (bf16[128,512]{1,0:T(8,128)(2,1)S(1)}, bf16[128,512]{1,0:T(8,128)(2,1)S(1)}, u32[]{:S(2)}, u32[]{:S(2)}) collective-permute-start(bf16[128,512]{1,0:T(8,128)(2,1)S(1)} %copy-done.16), channel_id=1, source_target_pairs={{0,1},{1,0},{2,3},{3,2},{4,5},{5,4},{6,7},{7,6},{8,9},{9,8},{10,11... | collective-permute-start | bytes 393224 | tf_op jit(solution)/shard_map/ppermute | solution.py:43
  59.8 7.7 %collective-permute-start.11 = (bf16[128,512]{1,0:T(8,128)(2,1)S(1)}, bf16[128,512]{1,0:T(8,128)(2,1)S(1)}, u32[]{:S(2)}, u32[]{:S(2)}) collective-permute-start(bf16[128,512]{1,0:T(8,128)(2,1)S(1)} %copy-done.14), channel_id=1, source_target_pairs={{0,2},{1,3},{2,0},{3,1},{4,6},{5,7},{6,4},{7,5},{8,10},{9,11},{10,... | collective-permute-start | bytes 393224 | tf_op jit(solution)/shard_map/ppermute | solution.py:43
  61.4 7.2 %collective-permute-start.12 = (bf16[128,512]{1,0:T(8,128)(2,1)S(1)}, bf16[128,512]{1,0:T(8,128)(2,1)S(1)}, u32[]{:S(2)}, u32[]{:S(2)}) collective-permute-start(bf16[128,512]{1,0:T(8,128)(2,1)S(1)} %copy-done.12), channel_id=1, source_target_pairs={{0,3},{1,2},{2,1},{3,0},{4,7},{5,6},{6,5},{7,4},{8,11},{9,10},{10,... | collective-permute-start | bytes 393224 | tf_op jit(solution)/shard_map/ppermute | solution.py:43
  61.7 6.9 %collective-permute-start.7 = (bf16[384,128]{1,0:T(8,128)(2,1)S(1)}, bf16[384,128]{1,0:T(8,128)(2,1)S(1)}, u32[]{:S(2)}, u32[]{:S(2)}) collective-permute-start(bf16[384,128]{1,0:T(8,128)(2,1)S(1)} %shard_map.255.h0), channel_id=1, source_target_pairs={{0,1},{1,0},{2,3},{3,2},{4,5},{5,4},{6,7},{7,6},{8,9},{9,8},{10,11... | collective-permute-start | bytes 294920 | tf_op jit(solution)/shard_map/ppermute | solution.py:43
  64.7 3.8 %collective-permute-start.9 = (bf16[384,128]{1,0:T(8,128)(2,1)S(1)}, bf16[384,128]{1,0:T(8,128)(2,1)S(1)}, u32[]{:S(2)}, u32[]{:S(2)}) collective-permute-start(bf16[384,128]{1,0:T(8,128)(2,1)S(1)} %collective-permute-done.8.h2), channel_id=1, source_target_pairs={{0,1},{1,0},{2,3},{3,2},{4,5},{5,4},{6,7},{7,6},{8,9},{9,8},{10,11... | collective-permute-start | bytes 294920 | tf_op jit(solution)/shard_map/ppermute | solution.py:43
  69.9 29.0 %all-to-all-start.1 = ((bf16[64,24,128]{2,1,0:T(8,128)(2,1)}), bf16[64,24,128]{2,1,0:T(8,128)(2,1)S(1)}, u32[]{:S(2)}, u32[]{:S(2)}) async-start(bf16[64,24,128]{2,1,0:T(8,128)(2,1)} %bitcast.14), calls=%async_computation.1 | async-start | bytes 786432 | tf_op jit(solution)/shard_map/all_to_all | solution.py:489
  79.6 5.5 %collective-permute-start.14 = (bf16[96,512]{1,0:T(8,128)(2,1)S(1)}, bf16[96,512]{1,0:T(8,128)(2,1)S(1)}, u32[]{:S(2)}, u32[]{:S(2)}) collective-permute-start(bf16[96,512]{1,0:T(8,128)(2,1)S(1)} %get-tuple-element.45.a0.resid), channel_id=1, source_target_pairs={{0,2},{1,3},{2,0},{3,1},{4,6},{5,7},{6,4},{7,5},{8,10},{9,11},{10,... | collective-permute-start | bytes 294920 | tf_op jit(solution)/shard_map/ppermute | solution.py:43
  80.1 5.0 %collective-permute-start.13 = (bf16[96,512]{1,0:T(8,128)(2,1)S(1)}, bf16[96,512]{1,0:T(8,128)(2,1)S(1)}, u32[]{:S(2)}, u32[]{:S(2)}) collective-permute-start(bf16[96,512]{1,0:T(8,128)(2,1)S(1)} %get-tuple-element.45.a0.resid), channel_id=1, source_target_pairs={{0,1},{1,0},{2,3},{3,2},{4,5},{5,4},{6,7},{7,6},{8,9},{9,8},{10,11... | collective-permute-start | bytes 294920 | tf_op jit(solution)/shard_map/ppermute | solution.py:43
  85.1 1.3 %collective-permute-start.15 = (bf16[96,512]{1,0:T(8,128)(2,1)S(1)}, bf16[96,512]{1,0:T(8,128)(2,1)S(1)}, u32[]{:S(2)}, u32[]{:S(2)}) collective-permute-start(bf16[96,512]{1,0:T(8,128)(2,1)S(1)} %collective-permute-done.14.a2), channel_id=1, source_target_pairs={{0,1},{1,0},{2,3},{3,2},{4,5},{5,4},{6,7},{7,6},{8,9},{9,8},{10,11... | collective-permute-start | bytes 294920 | tf_op jit(solution)/shard_map/ppermute | solution.py:43
  90.5 1.7 %collective-permute-start.16 = (bf16[96,1024]{1,0:T(8,128)(2,1)}, bf16[96,1024]{1,0:T(8,128)(2,1)S(1)}, u32[]{:S(2)}, u32[]{:S(2)}) collective-permute-start(bf16[96,1024]{1,0:T(8,128)(2,1)} %get-tuple-element.48), channel_id=1, source_target_pairs={{0,1},{1,0},{2,3},{3,2},{4,5},{5,4},{6,7},{7,6},{8,9},{9,8},{10,11... | collective-permute-start | bytes 589832 | tf_op jit(solution)/shard_map/ppermute | solution.py:43
  93.9 5.1 %collective-permute-start.17 = (bf16[96,512]{1,0:T(8,128)(2,1)}, bf16[96,512]{1,0:T(8,128)(2,1)S(1)}, u32[]{:S(2)}, u32[]{:S(2)}) collective-permute-start(bf16[96,512]{1,0:T(8,128)(2,1)} %shard_map.258), channel_id=1, source_target_pairs={{0,2},{1,3},{2,0},{3,1},{4,6},{5,7},{6,4},{7,5},{8,10},{9,11},{10,... | collective-permute-start | bytes 294920 | tf_op jit(solution)/shard_map/ppermute | solution.py:43
  (15 other events, 92.6 us)

commit v8 on v7

--- a/solution.py
+++ b/solution.py
@@ -41,11 +41,6 @@
 
 def exchanged(value, mask):
     return lax.ppermute(value, "tp", [(i, i ^ mask) for i in range(4)])
-
-
-def gathered(value):
-    across = exchanged(value, 2)
-    return [value, exchanged(value, 1), across, exchanged(across, 1)]
 
 
 def spread_blocks(out, small, channels):
@@ -79,7 +74,7 @@
     ]
     for load in loads:
         load.start()
-    log_step, decay, skip, b_re, b_im, c_re, c_im, tokens_v, gain, in_v, re_v, im_v, out_v = held
+    log_step, decay, skip, tokens_v, gain, b_re, b_im, in_v, re_v, im_v, c_re, c_im, out_v = held
     groups, entries = decay.shape
     channels = skip.shape[1]
     width = groups * entries
@@ -100,21 +95,23 @@
     denom = eigen * eigen + freq * freq
     fac_re = ((lam_re - 1.0) * eigen + lam_im * freq) / denom
     fac_im = (lam_im * eigen - (lam_re - 1.0) * freq) / denom
-    for load in loads[3:7]:
+    for load in loads[3:5]:
         load.wait()
-    for k, small in enumerate((b_re, b_im, c_re, c_im)):
-        spread_blocks(blocks_v.at[k], small[...], channels)
-    loads[7].wait()
-    loads[8].wait()
     x = tokens_v[...].astype(F32)
     scale = lax.rsqrt(jnp.mean(x * x, axis=-1, keepdims=True) + EPS)
     normed = (x * scale * gain[...].astype(F32).reshape(1, -1)).astype(BF16)
-    loads[9].wait()
+    for load in loads[5:7]:
+        load.wait()
+    spread_blocks(blocks_v.at[0], b_re[...], channels)
+    spread_blocks(blocks_v.at[1], b_im[...], channels)
+    loads[7].wait()
     drive = dot(normed, in_v[...]).astype(BF16)
     in_re = dot(drive, blocks_v[0])
     in_im = dot(drive, blocks_v[1])
-    loads[10].wait()
-    loads[11].wait()
+    for load in loads[8:12]:
+        load.wait()
+    spread_blocks(blocks_v.at[2], c_re[...], channels)
+    spread_blocks(blocks_v.at[3], c_im[...], channels)
     was_re, was_im = re_v[...], im_v[...]
     fresh_re = lam_re * was_re - lam_im * was_im + (fac_re * in_re - fac_im * in_im)
     fresh_im = lam_re * was_im + lam_im * was_re + (fac_re * in_im + fac_im * in_re)
@@ -401,15 +398,15 @@
         log_step,
         eigen_decay_real,
         channel_skip_scale,
+        tokens,
+        norm_gain,
         by_channel(input_matrix_real),
         by_channel(input_matrix_imaginary),
-        output_matrix_real.reshape(groups * channels, entries),
-        output_matrix_imaginary.reshape(groups * channels, entries),
-        tokens,
-        norm_gain,
         in_weight,
         sequence_state_real,
         sequence_state_imaginary,
+        output_matrix_real.reshape(groups * channels, entries),
+        output_matrix_imaginary.reshape(groups * channels, entries),
         out_weight,
     )
     own, beside, new_re, new_im = call(
@@ -424,6 +421,12 @@
         [VMEM] * 4,
     )(*state_inputs)
     came_mix = exchanged(beside, 1)
+    z, w, share0, share1 = call(
+        functools.partial(route_kernel, ep),
+        [((slots, lanes), BF16), ((2 * rows, slots), BF16)] + [((rows, lanes), F32)] * 2,
+        [pltpu.VMEM((8, lanes), jnp.int32)],
+    )(routes.T, group_weight.reshape(1, rows), expert_logit.T)
+    wide = pltpu.VMEM((slots * blocks, lanes), F32)
     (onward,) = call(half_kernel, [piece])(own, came_mix)
     last_mix = exchanged(onward, 2)
     reshard = call(reshard_kernel, [((quarter, 2 * hid), BF16)] * 4 + [((hid, quarter), BF16)] * 4)
@@ -433,12 +436,6 @@
     wide1 = exchanged(pieces[1], 1)
     moved = [pieces[0], wide1, wide2, wide3]
     downs = [pieces[4]] + [exchanged(pieces[4 + m], m) for m in (1, 2, 3)]
-    z, w, share0, share1 = call(
-        functools.partial(route_kernel, ep),
-        [((slots, lanes), BF16), ((2 * rows, slots), BF16)] + [((rows, lanes), F32)] * 2,
-        [pltpu.VMEM((8, lanes), jnp.int32)],
-    )(routes.T, group_weight.reshape(1, rows), expert_logit.T)
-    wide = pltpu.VMEM((slots * blocks, lanes), F32)
     resid16, packed = call(
         functools.partial(pack_kernel, capacity),
         [piece, ((slots * blocks, lanes), BF16)],
@@ -473,12 +470,13 @@
         [OUT] * 3,
     )(gains, *near, blend_weight.reshape(1, width), dense_gate, dense_up, dense_down)
     dense_came = exchanged(dense_beside, 1)
-    (dense_onward,) = call(half_kernel, [piece], out_specs=[OUT])(dense_own, dense_came)
+    (dense_onward,) = call(half_kernel, [piece])(dense_own, dense_came)
     dense_last = exchanged(dense_onward, 2)
     (hidden,) = call(
         functools.partial(hidden_kernel, float(width)), [((slots, hid), BF16)]
     )(keep, came, last)
-    hidden = gathered(hidden)
+    unit_across, unit_beside = exchanged(hidden, 2), exchanged(hidden, 1)
+    hidden = [hidden, unit_beside, unit_across, exchanged(unit_across, 1)]
     (sent,) = call(
         functools.partial(leave_kernel, capacity),
         [((slots * blocks, lanes), BF16)],

time: 102 us -> 101 us (level)
  transfers between devices with their start and end apart: 20 -> 20, of which waited for: 14 -> 14; matrix products, arithmetic and copies ran while one was open for 2% -> 2% of each run, Pallas kernels for 6% -> 5%
where the time goes in v8:
time: 101 us; the launch traced here: 99.2 us
  waiting for transfers between devices  47.9 us (47%)
  starting transfers between devices  32.1 us (32%)
  Pallas kernels  13.2 us (13%)
  local copies, waits for them, and re-layouts  5.14 us (5%)
    ppermute x18, waiting for transfers between devices, exchanged(): return lax.ppermute(value, 'tp', [(i, i ^ mask) for i in range(4)])  44.8 us
    all_to_all x1, starting transfers between devices, per_device(): lax.all_to_all(packed.reshape(ep, capacity * blocks, lanes), 'ep', 0, 0,...  14.2 us
    pallas_call x13, Pallas kernels, run(): pl.pallas_call(kernel, out_shape=tuple(out_shape), in_specs=specs, out_sp...  13.2 us
    all_to_all x1, starting transfers between devices, per_device(): lax.all_to_all(sent.reshape(ep, capacity * blocks, lanes), 'ep', 0, 0, ti...  9.66 us
    ppermute x18, starting transfers between devices, exchanged(): return lax.ppermute(value, 'tp', [(i, i ^ mask) for i in range(4)])  8.23 us
    unnamed x40, local copies, waits for them, and re-layouts  5.13 us
    all_to_all x1, waiting for transfers between devices, per_device(): lax.all_to_all(packed.reshape(ep, capacity * blocks, lanes), 'ep', 0, 0,...  3.11 us
  transfers between devices with their start and end apart: 20, of which 14 were waited for; matrix products, arithmetic and copies ran while one was open for 2% of the time, Pallas kernels for 5%

profile of v8, /device:TPU:32, one launch (start us, length us, event | category | flops | bytes accessed | tf_op | source)
XLA Modules:
  0.0 99.2 jit_solution(17325128819364252134)
XLA Ops:
  0.7 3.4 %shard_map.247 = (bf16[96,1024]{1,0:T(8,128)(2,1)S(1)}, bf16[96,1024]{1,0:T(8,128)(2,1)S(1)}, f32[96,1024]{1,0:T(8,128)S(1)}, f32[96,1024]{1,0:T(8,128)S(1)}) custom-call(f32[16]{0:T(128)} %refs_0_.1, f32[16,64]{1,0:T(8,128)} %refs_1_.1, f32[16,16]{1,0:T(8,128)} %refs_2_.1, bf16[96,2048]{1,0:T(8,128)(2,1)} %tokens.1, bf16[2048]{0:T(1024)(128)(2,1)} %refs_4_.1, ...), custom_call_target="tpu_custom_call" | custom-call | tf_op jit(solution)/shard_map/pallas_call | solution.py:340
  4.2 1.4 %collective-permute-done.came = bf16[96,1024]{1,0:T(8,128)(2,1)S(1)} collective-permute-done((bf16[96,1024]{1,0:T(8,128)(2,1)S(1)}, bf16[96,1024]{1,0:T(8,128)(2,1)S(1)}, u32[]{:S(2)}, u32[]{:S(2)}) %collective-permute-start) | collective-permute-done | bytes 196640 | tf_op jit(solution)/shard_map/ppermute | solution.py:43
  5.7 1.6 %collective-permute-start.1 = (bf16[96,512]{1,0:T(8,128)(2,1)S(1)}, bf16[96,512]{1,0:T(8,128)(2,1)S(1)}, u32[]{:S(2)}, u32[]{:S(2)}) collective-permute-start(bf16[96,512]{1,0:T(8,128)(2,1)S(1)} %shard_map.248), channel_id=1, source_target_pairs={{0,2},{1,3},{2,0},{3,1},{4,6},{5,7},{6,4},{7,5},{8,10},{9,11},{10,... | collective-permute-start | bytes 294920 | tf_op jit(solution)/shard_map/ppermute | solution.py:43
  7.6 3.0 %collective-permute-done.1.last = bf16[96,512]{1,0:T(8,128)(2,1)S(1)} collective-permute-done((bf16[96,512]{1,0:T(8,128)(2,1)S(1)}, bf16[96,512]{1,0:T(8,128)(2,1)S(1)}, u32[]{:S(2)}, u32[]{:S(2)}) %collective-permute-start.1) | collective-permute-done | bytes 98336 | tf_op jit(solution)/shard_map/ppermute | solution.py:43
  10.6 1.1 %shard_map.250 = (bf16[96,512]{1,0:T(8,128)(2,1)S(1)}, bf16[1536,128]{1,0:T(8,128)(2,1)}) custom-call(bf16[96,2048]{1,0:T(8,128)(2,1)S(1)} %copy-done, bf16[96,1024]{1,0:T(8,128)(2,1)S(1)} %get-tuple-element.27.own, bf16[96,1024]{1,0:T(8,128)(2,1)S(1)} %collective-permute-done.came, bf16[96,512]{1,0:T(8,128)(2,1)S(1)} %collective-permute-done.1.last, ...), custom_call_target="tpu_custom_call" | custom-call | tf_op jit(solution)/shard_map/pallas_call | solution.py:340
  11.7 14.2 %all-to-all-start = ((bf16[64,24,128]{2,1,0:T(8,128)(2,1)}), bf16[64,24,128]{2,1,0:T(8,128)(2,1)S(1)}, u32[]{:S(2)}, u32[]{:S(2)}) async-start(bf16[64,24,128]{2,1,0:T(8,128)(2,1)} %bitcast.9), calls=%async_computation | async-start | bytes 786432 | tf_op jit(solution)/shard_map/all_to_all | solution.py:447
  29.6 0.8 collective-permute-done.2.w1
  30.4 8.4 %collective-permute-done.3.w3 = bf16[512,256]{1,0:T(8,128)(2,1)S(1)} collective-permute-done((bf16[512,256]{1,0:T(8,128)(2,1)S(1)}, bf16[512,256]{1,0:T(8,128)(2,1)S(1)}, u32[]{:S(2)}, u32[]{:S(2)}) %collective-permute-start.3) | collective-permute-done | bytes 262176 | tf_op jit(solution)/shard_map/ppermute | solution.py:43
  38.8 3.1 %all-to-all-done = bf16[64,24,128]{2,1,0:T(8,128)(2,1)S(1)} async-done(((bf16[64,24,128]{2,1,0:T(8,128)(2,1)}), bf16[64,24,128]{2,1,0:T(8,128)(2,1)S(1)}, u32[]{:S(2)}, u32[]{:S(2)}) %all-to-all-start) | async-done | bytes 393248 | tf_op jit(solution)/shard_map/all_to_all | solution.py:447
  43.5 8.2 %collective-permute-done.4.w2 = bf16[512,256]{1,0:T(8,128)(2,1)S(1)} collective-permute-done((bf16[512,256]{1,0:T(8,128)(2,1)}, bf16[512,256]{1,0:T(8,128)(2,1)S(1)}, u32[]{:S(2)}, u32[]{:S(2)}) %collective-permute-start.4) | collective-permute-done | bytes 262176 | tf_op jit(solution)/shard_map/ppermute | solution.py:43
  52.9 5.9 %collective-permute-done.6.last = bf16[400,256]{1,0:T(8,128)(2,1)S(1)} collective-permute-done((bf16[400,256]{1,0:T(8,128)(2,1)S(1)}, bf16[400,256]{1,0:T(8,128)(2,1)S(1)}, u32[]{:S(2)}, u32[]{:S(2)}) %collective-permute-start.6) | collective-permute-done | bytes 204832 | tf_op jit(solution)/shard_map/ppermute | solution.py:43
  59.8 1.5 %collective-permute-start.11 = (bf16[128,512]{1,0:T(8,128)(2,1)S(1)}, bf16[128,512]{1,0:T(8,128)(2,1)S(1)}, u32[]{:S(2)}, u32[]{:S(2)}) collective-permute-start(bf16[128,512]{1,0:T(8,128)(2,1)S(1)} %copy-done.14), channel_id=1, source_target_pairs={{0,2},{1,3},{2,0},{3,1},{4,6},{5,7},{6,4},{7,5},{8,10},{9,11},{10,... | collective-permute-start | bytes 393224 | tf_op jit(solution)/shard_map/ppermute | solution.py:43
  62.0 2.7 %collective-permute-done.8.h2 = bf16[384,128]{1,0:T(8,128)(2,1)S(1)} collective-permute-done((bf16[384,128]{1,0:T(8,128)(2,1)S(1)}, bf16[384,128]{1,0:T(8,128)(2,1)S(1)}, u32[]{:S(2)}, u32[]{:S(2)}) %collective-permute-start.8) | collective-permute-done | bytes 98336 | tf_op jit(solution)/shard_map/ppermute | solution.py:43
  64.7 2.8 %collective-permute-done.11.w2 = bf16[128,512]{1,0:T(8,128)(2,1)S(1)} collective-permute-done((bf16[128,512]{1,0:T(8,128)(2,1)S(1)}, bf16[128,512]{1,0:T(8,128)(2,1)S(1)}, u32[]{:S(2)}, u32[]{:S(2)}) %collective-permute-start.11) | collective-permute-done | bytes 131104 | tf_op jit(solution)/shard_map/ppermute | solution.py:43
  67.5 1.0 collective-permute-done.12.w3
  68.5 1.4 %shard_map.256 = bf16[1536,128]{1,0:T(8,128)(2,1)} custom-call(bf16[384,128]{1,0:T(8,128)(2,1)S(1)} %shard_map.255.h0, bf16[384,128]{1,0:T(8,128)(2,1)S(1)} %collective-permute-done.7.h1, bf16[384,128]{1,0:T(8,128)(2,1)S(1)} %collective-permute-done.8.h2, bf16[384,128]{1,0:T(8,128)(2,1)S(1)} %collective-permute-done.9.h3, ...), custom_call_target="tpu_custom_call" | custom-call | tf_op jit(solution)/shard_map/pallas_call | solution.py:340
  69.9 9.7 %all-to-all-start.1 = ((bf16[64,24,128]{2,1,0:T(8,128)(2,1)}), bf16[64,24,128]{2,1,0:T(8,128)(2,1)S(1)}, u32[]{:S(2)}, u32[]{:S(2)}) async-start(bf16[64,24,128]{2,1,0:T(8,128)(2,1)} %bitcast.14), calls=%async_computation.1 | async-start | bytes 786432 | tf_op jit(solution)/shard_map/all_to_all | solution.py:487
  80.0 5.0 %collective-permute-done.14.a2 = bf16[96,512]{1,0:T(8,128)(2,1)S(1)} collective-permute-done((bf16[96,512]{1,0:T(8,128)(2,1)S(1)}, bf16[96,512]{1,0:T(8,128)(2,1)S(1)}, u32[]{:S(2)}, u32[]{:S(2)}) %collective-permute-start.14) | collective-permute-done | bytes 98336 | tf_op jit(solution)/shard_map/ppermute | solution.py:43
  85.0 1.3 %collective-permute-done.15.a3 = bf16[96,512]{1,0:T(8,128)(2,1)S(1)} collective-permute-done((bf16[96,512]{1,0:T(8,128)(2,1)S(1)}, bf16[96,512]{1,0:T(8,128)(2,1)S(1)}, u32[]{:S(2)}, u32[]{:S(2)}) %collective-permute-start.15) | collective-permute-done | bytes 98336 | tf_op jit(solution)/shard_map/ppermute | solution.py:43
  86.3 4.2 %shard_map.257 = (bf16[96,1024]{1,0:T(8,128)(2,1)}, bf16[96,1024]{1,0:T(8,128)(2,1)}, f32[96,128]{1,0:T(8,128)}) custom-call(bf16[1,2048]{1,0:T(2,128)(2,1)S(1)} %reshape.55.gains, bf16[96,512]{1,0:T(8,128)(2,1)S(1)} %get-tuple-element.45.a0.resid, bf16[96,512]{1,0:T(8,128)(2,1)S(1)} %collective-permute-done.13.a1, ...), custom_call_target="tpu_custom_call" | custom-call | tf_op jit(solution)/shard_map/pallas_call | solution.py:340
  90.7 1.5 %collective-permute-done.16.came = bf16[96,1024]{1,0:T(8,128)(2,1)S(1)} collective-permute-done((bf16[96,1024]{1,0:T(8,128)(2,1)}, bf16[96,1024]{1,0:T(8,128)(2,1)S(1)}, u32[]{:S(2)}, u32[]{:S(2)}) %collective-permute-start.16) | collective-permute-done | bytes 196640 | tf_op jit(solution)/shard_map/ppermute | solution.py:43
  92.2 0.9 copy-done.1
  95.4 2.7 %collective-permute-done.17.last = bf16[96,512]{1,0:T(8,128)(2,1)S(1)} collective-permute-done((bf16[96,512]{1,0:T(8,128)(2,1)S(1)}, bf16[96,512]{1,0:T(8,128)(2,1)S(1)}, u32[]{:S(2)}, u32[]{:S(2)}) %collective-permute-start.17) | collective-permute-done | bytes 98336 | tf_op jit(solution)/shard_map/ppermute | solution.py:43
  98.1 1.1 %shard_map.259 = bf16[96,512]{1,0:T(8,128)(2,1)} custom-call(bf16[1536,128]{1,0:T(8,128)(2,1)S(1)} %bitcast.19, bf16[192,384]{1,0:T(8,128)(2,1)S(1)} %get-tuple-element.42.w, f32[96,128]{1,0:T(8,128)S(1)} %get-tuple-element.43.share0, f32[96,128]{1,0:T(8,128)S(1)} %get-tuple-element.44.share1, bf16[96,512]{1,0:T(8,128)(2,1)S(1)} %get-tuple-element.45.a0.resid, ...), custom_call_target="tpu_custom_call" | custom-call | tf_op jit(solution)/shard_map/pallas_call | solution.py:340
  (71 shorter events, 11.5 us)
Async XLA Ops:
  4.1 21.8 %copy-start.3 = (bf16[1,2048,128]{2,1,0:T(8,128)(2,1)S(1)}, bf16[1,2048,128]{2,1,0:T(8,128)(2,1)}, u32[]{:S(2)}) copy-start(bf16[1,2048,128]{2,1,0:T(8,128)(2,1)} %param.41) | copy-start | bytes 1572868
  4.1 21.8 %copy-start.4 = (bf16[1,2048,128]{2,1,0:T(8,128)(2,1)S(1)}, bf16[1,2048,128]{2,1,0:T(8,128)(2,1)}, u32[]{:S(2)}) copy-start(bf16[1,2048,128]{2,1,0:T(8,128)(2,1)} %param.42) | copy-start | bytes 1572868
  4.1 25.4 %copy-start.17 = (bf16[2048]{0:T(1024)(128)(2,1)S(1)}, bf16[2048]{0:T(1024)(128)(2,1)}, u32[]{:S(2)}) copy-start(bf16[2048]{0:T(1024)(128)(2,1)} %param.37) | copy-start | bytes 12292
  4.1 1.5 %collective-permute-start = (bf16[96,1024]{1,0:T(8,128)(2,1)S(1)}, bf16[96,1024]{1,0:T(8,128)(2,1)S(1)}, u32[]{:S(2)}, u32[]{:S(2)}) collective-permute-start(bf16[96,1024]{1,0:T(8,128)(2,1)S(1)} %get-tuple-element.28), channel_id=1, source_target_pairs={{0,1},{1,0},{2,3},{3,2},{4,5},{5,4},{6,7},{7,6},{8,9},{9,8},{10,11... | collective-permute-start | bytes 589832 | tf_op jit(solution)/shard_map/ppermute | solution.py:43
  5.7 4.9 %collective-permute-start.1 = (bf16[96,512]{1,0:T(8,128)(2,1)S(1)}, bf16[96,512]{1,0:T(8,128)(2,1)S(1)}, u32[]{:S(2)}, u32[]{:S(2)}) collective-permute-start(bf16[96,512]{1,0:T(8,128)(2,1)S(1)} %shard_map.248), channel_id=1, source_target_pairs={{0,2},{1,3},{2,0},{3,1},{4,6},{5,7},{6,4},{7,5},{8,10},{9,11},{10,... | collective-permute-start | bytes 294920 | tf_op jit(solution)/shard_map/ppermute | solution.py:43
  11.7 30.2 %all-to-all-start = ((bf16[64,24,128]{2,1,0:T(8,128)(2,1)}), bf16[64,24,128]{2,1,0:T(8,128)(2,1)S(1)}, u32[]{:S(2)}, u32[]{:S(2)}) async-start(bf16[64,24,128]{2,1,0:T(8,128)(2,1)} %bitcast.9), calls=%async_computation | async-start | bytes 786432 | tf_op jit(solution)/shard_map/all_to_all | solution.py:447
  28.8 1.5 %collective-permute-start.2 = (bf16[512,256]{1,0:T(8,128)(2,1)S(1)}, bf16[512,256]{1,0:T(8,128)(2,1)S(1)}, u32[]{:S(2)}, u32[]{:S(2)}) collective-permute-start(bf16[512,256]{1,0:T(8,128)(2,1)S(1)} %get-tuple-element.31), channel_id=1, source_target_pairs={{0,1},{1,0},{2,3},{3,2},{4,5},{5,4},{6,7},{7,6},{8,9},{9,8},{10,11... | collective-permute-start | bytes 786440 | tf_op jit(solution)/shard_map/ppermute | solution.py:43
  28.8 10.0 %collective-permute-start.3 = (bf16[512,256]{1,0:T(8,128)(2,1)S(1)}, bf16[512,256]{1,0:T(8,128)(2,1)S(1)}, u32[]{:S(2)}, u32[]{:S(2)}) collective-permute-start(bf16[512,256]{1,0:T(8,128)(2,1)S(1)} %get-tuple-element.32), channel_id=1, source_target_pairs={{0,3},{1,2},{2,1},{3,0},{4,7},{5,6},{6,5},{7,4},{8,11},{9,10},{10,... | collective-permute-start | bytes 786440 | tf_op jit(solution)/shard_map/ppermute | solution.py:43
  42.7 9.4 %collective-permute-start.5 = (bf16[392,512]{1,0:T(8,128)(2,1)S(1)}, bf16[392,512]{1,0:T(8,128)(2,1)S(1)}, u32[]{:S(2)}, u32[]{:S(2)}) collective-permute-start(bf16[392,512]{1,0:T(8,128)(2,1)S(1)} %get-tuple-element.37), channel_id=1, source_target_pairs={{0,1},{1,0},{2,3},{3,2},{4,5},{5,4},{6,7},{7,6},{8,9},{9,8},{10,11... | collective-permute-start | bytes 1204232 | tf_op jit(solution)/shard_map/ppermute | solution.py:43
  42.8 8.9 %collective-permute-start.4 = (bf16[512,256]{1,0:T(8,128)(2,1)}, bf16[512,256]{1,0:T(8,128)(2,1)S(1)}, u32[]{:S(2)}, u32[]{:S(2)}) collective-permute-start(bf16[512,256]{1,0:T(8,128)(2,1)} %copy-done.10), channel_id=1, source_target_pairs={{0,2},{1,3},{2,0},{3,1},{4,6},{5,7},{6,4},{7,5},{8,10},{9,11},{10,... | collective-permute-start | bytes 786440 | tf_op jit(solution)/shard_map/ppermute | solution.py:43
  52.2 32.8 %copy-start.18 = (bf16[2048]{0:T(1024)(128)(2,1)S(1)}, bf16[2048]{0:T(1024)(128)(2,1)}, u32[]{:S(2)}) copy-start(bf16[2048]{0:T(1024)(128)(2,1)} %param.47) | copy-start | bytes 12292
  52.2 6.6 %collective-permute-start.6 = (bf16[400,256]{1,0:T(8,128)(2,1)S(1)}, bf16[400,256]{1,0:T(8,128)(2,1)S(1)}, u32[]{:S(2)}, u32[]{:S(2)}) collective-permute-start(bf16[400,256]{1,0:T(8,128)(2,1)S(1)} %shard_map.254), channel_id=1, source_target_pairs={{0,2},{1,3},{2,0},{3,1},{4,6},{5,7},{6,4},{7,5},{8,10},{9,11},{10,... | collective-permute-start | bytes 614408 | tf_op jit(solution)/shard_map/ppermute | solution.py:43
  59.1 5.6 %collective-permute-start.8 = (bf16[384,128]{1,0:T(8,128)(2,1)S(1)}, bf16[384,128]{1,0:T(8,128)(2,1)S(1)}, u32[]{:S(2)}, u32[]{:S(2)}) collective-permute-start(bf16[384,128]{1,0:T(8,128)(2,1)S(1)} %shard_map.255.h0), channel_id=1, source_target_pairs={{0,2},{1,3},{2,0},{3,1},{4,6},{5,7},{6,4},{7,5},{8,10},{9,11},{10,... | collective-permute-start | bytes 294920 | tf_op jit(solution)/shard_map/ppermute | solution.py:43
  59.8 4.9 %collective-permute-start.10 = (bf16[128,512]{1,0:T(8,128)(2,1)S(1)}, bf16[128,512]{1,0:T(8,128)(2,1)S(1)}, u32[]{:S(2)}, u32[]{:S(2)}) collective-permute-start(bf16[128,512]{1,0:T(8,128)(2,1)S(1)} %copy-done.16), channel_id=1, source_target_pairs={{0,1},{1,0},{2,3},{3,2},{4,5},{5,4},{6,7},{7,6},{8,9},{9,8},{10,11... | collective-permute-start | bytes 393224 | tf_op jit(solution)/shard_map/ppermute | solution.py:43
  59.8 7.7 %collective-permute-start.11 = (bf16[128,512]{1,0:T(8,128)(2,1)S(1)}, bf16[128,512]{1,0:T(8,128)(2,1)S(1)}, u32[]{:S(2)}, u32[]{:S(2)}) collective-permute-start(bf16[128,512]{1,0:T(8,128)(2,1)S(1)} %copy-done.14), channel_id=1, source_target_pairs={{0,2},{1,3},{2,0},{3,1},{4,6},{5,7},{6,4},{7,5},{8,10},{9,11},{10,... | collective-permute-start | bytes 393224 | tf_op jit(solution)/shard_map/ppermute | solution.py:43
  61.3 7.2 %collective-permute-start.12 = (bf16[128,512]{1,0:T(8,128)(2,1)S(1)}, bf16[128,512]{1,0:T(8,128)(2,1)S(1)}, u32[]{:S(2)}, u32[]{:S(2)}) collective-permute-start(bf16[128,512]{1,0:T(8,128)(2,1)S(1)} %copy-done.12), channel_id=1, source_target_pairs={{0,3},{1,2},{2,1},{3,0},{4,7},{5,6},{6,5},{7,4},{8,11},{9,10},{10,... | collective-permute-start | bytes 393224 | tf_op jit(solution)/shard_map/ppermute | solution.py:43
  61.7 6.9 %collective-permute-start.7 = (bf16[384,128]{1,0:T(8,128)(2,1)S(1)}, bf16[384,128]{1,0:T(8,128)(2,1)S(1)}, u32[]{:S(2)}, u32[]{:S(2)}) collective-permute-start(bf16[384,128]{1,0:T(8,128)(2,1)S(1)} %shard_map.255.h0), channel_id=1, source_target_pairs={{0,1},{1,0},{2,3},{3,2},{4,5},{5,4},{6,7},{7,6},{8,9},{9,8},{10,11... | collective-permute-start | bytes 294920 | tf_op jit(solution)/shard_map/ppermute | solution.py:43
  64.7 3.8 %collective-permute-start.9 = (bf16[384,128]{1,0:T(8,128)(2,1)S(1)}, bf16[384,128]{1,0:T(8,128)(2,1)S(1)}, u32[]{:S(2)}, u32[]{:S(2)}) collective-permute-start(bf16[384,128]{1,0:T(8,128)(2,1)S(1)} %collective-permute-done.8.h2), channel_id=1, source_target_pairs={{0,1},{1,0},{2,3},{3,2},{4,5},{5,4},{6,7},{7,6},{8,9},{9,8},{10,11... | collective-permute-start | bytes 294920 | tf_op jit(solution)/shard_map/ppermute | solution.py:43
  69.9 28.2 %all-to-all-start.1 = ((bf16[64,24,128]{2,1,0:T(8,128)(2,1)}), bf16[64,24,128]{2,1,0:T(8,128)(2,1)S(1)}, u32[]{:S(2)}, u32[]{:S(2)}) async-start(bf16[64,24,128]{2,1,0:T(8,128)(2,1)} %bitcast.14), calls=%async_computation.1 | async-start | bytes 786432 | tf_op jit(solution)/shard_map/all_to_all | solution.py:487
  79.6 5.4 %collective-permute-start.14 = (bf16[96,512]{1,0:T(8,128)(2,1)S(1)}, bf16[96,512]{1,0:T(8,128)(2,1)S(1)}, u32[]{:S(2)}, u32[]{:S(2)}) collective-permute-start(bf16[96,512]{1,0:T(8,128)(2,1)S(1)} %get-tuple-element.45.a0.resid), channel_id=1, source_target_pairs={{0,2},{1,3},{2,0},{3,1},{4,6},{5,7},{6,4},{7,5},{8,10},{9,11},{10,... | collective-permute-start | bytes 294920 | tf_op jit(solution)/shard_map/ppermute | solution.py:43
  80.0 5.0 %collective-permute-start.13 = (bf16[96,512]{1,0:T(8,128)(2,1)S(1)}, bf16[96,512]{1,0:T(8,128)(2,1)S(1)}, u32[]{:S(2)}, u32[]{:S(2)}) collective-permute-start(bf16[96,512]{1,0:T(8,128)(2,1)S(1)} %get-tuple-element.45.a0.resid), channel_id=1, source_target_pairs={{0,1},{1,0},{2,3},{3,2},{4,5},{5,4},{6,7},{7,6},{8,9},{9,8},{10,11... | collective-permute-start | bytes 294920 | tf_op jit(solution)/shard_map/ppermute | solution.py:43
  85.0 1.3 %collective-permute-start.15 = (bf16[96,512]{1,0:T(8,128)(2,1)S(1)}, bf16[96,512]{1,0:T(8,128)(2,1)S(1)}, u32[]{:S(2)}, u32[]{:S(2)}) collective-permute-start(bf16[96,512]{1,0:T(8,128)(2,1)S(1)} %collective-permute-done.14.a2), channel_id=1, source_target_pairs={{0,1},{1,0},{2,3},{3,2},{4,5},{5,4},{6,7},{7,6},{8,9},{9,8},{10,11... | collective-permute-start | bytes 294920 | tf_op jit(solution)/shard_map/ppermute | solution.py:43
  90.5 1.7 %collective-permute-start.16 = (bf16[96,1024]{1,0:T(8,128)(2,1)}, bf16[96,1024]{1,0:T(8,128)(2,1)S(1)}, u32[]{:S(2)}, u32[]{:S(2)}) collective-permute-start(bf16[96,1024]{1,0:T(8,128)(2,1)} %get-tuple-element.48), channel_id=1, source_target_pairs={{0,1},{1,0},{2,3},{3,2},{4,5},{5,4},{6,7},{7,6},{8,9},{9,8},{10,11... | collective-permute-start | bytes 589832 | tf_op jit(solution)/shard_map/ppermute | solution.py:43
  93.2 4.9 %collective-permute-start.17 = (bf16[96,512]{1,0:T(8,128)(2,1)S(1)}, bf16[96,512]{1,0:T(8,128)(2,1)S(1)}, u32[]{:S(2)}, u32[]{:S(2)}) collective-permute-start(bf16[96,512]{1,0:T(8,128)(2,1)S(1)} %shard_map.258), channel_id=1, source_target_pairs={{0,2},{1,3},{2,0},{3,1},{4,6},{5,7},{6,4},{7,5},{8,10},{9,11},{10,... | collective-permute-start | bytes 294920 | tf_op jit(solution)/shard_map/ppermute | solution.py:43
  (15 other events, 91.0 us)

commit v9 on v8

--- a/solution.py
+++ b/solution.py
@@ -41,6 +41,11 @@
 
 def exchanged(value, mask):
     return lax.ppermute(value, "tp", [(i, i ^ mask) for i in range(4)])
+
+
+def gathered(value):
+    across = exchanged(value, 2)
+    return [value, exchanged(value, 1), across, exchanged(across, 1)]
 
 
 def spread_blocks(out, small, channels):
@@ -475,8 +480,7 @@
     (hidden,) = call(
         functools.partial(hidden_kernel, float(width)), [((slots, hid), BF16)]
     )(keep, came, last)
-    unit_across, unit_beside = exchanged(hidden, 2), exchanged(hidden, 1)
-    hidden = [hidden, unit_beside, unit_across, exchanged(unit_across, 1)]
+    hidden = gathered(hidden)
     (sent,) = call(
         functools.partial(leave_kernel, capacity),
         [((slots * blocks, lanes), BF16)],

time: 101 us -> 101 us (level)
  no operation moved by 1% of the time
where the time goes in v9:
time: 101 us; the launch traced here: 99.2 us
  waiting for transfers between devices  47.9 us (47%)
  starting transfers between devices  32.1 us (32%)
  Pallas kernels  13.2 us (13%)
  local copies, waits for them, and re-layouts  5.14 us (5%)
    ppermute x18, waiting for transfers between devices, exchanged(): return lax.ppermute(value, 'tp', [(i, i ^ mask) for i in range(4)])  44.8 us
    all_to_all x1, starting transfers between devices, per_device(): lax.all_to_all(packed.reshape(ep, capacity * blocks, lanes), 'ep', 0, 0,...  14.2 us
    pallas_call x13, Pallas kernels, run(): pl.pallas_call(kernel, out_shape=tuple(out_shape), in_specs=specs, out_sp...  13.2 us
    all_to_all x1, starting transfers between devices, per_device(): lax.all_to_all(sent.reshape(ep, capacity * blocks, lanes), 'ep', 0, 0, ti...  9.66 us
    ppermute x18, starting transfers between devices, exchanged(): return lax.ppermute(value, 'tp', [(i, i ^ mask) for i in range(4)])  8.23 us
    unnamed x40, local copies, waits for them, and re-layouts  5.13 us
    all_to_all x1, waiting for transfers between devices, per_device(): lax.all_to_all(packed.reshape(ep, capacity * blocks, lanes), 'ep', 0, 0,...  3.11 us
  transfers between devices with their start and end apart: 20, of which 14 were waited for; matrix products, arithmetic and copies ran while one was open for 2% of the time, Pallas kernels for 5%

profile of v9, /device:TPU:32, one launch (start us, length us, event | category | flops | bytes accessed | tf_op | source)
XLA Modules:
  0.0 99.2 jit_solution(17325128819364252134)
XLA Ops:
  0.7 3.4 %shard_map.247 = (bf16[96,1024]{1,0:T(8,128)(2,1)S(1)}, bf16[96,1024]{1,0:T(8,128)(2,1)S(1)}, f32[96,1024]{1,0:T(8,128)S(1)}, f32[96,1024]{1,0:T(8,128)S(1)}) custom-call(f32[16]{0:T(128)} %refs_0_.1, f32[16,64]{1,0:T(8,128)} %refs_1_.1, f32[16,16]{1,0:T(8,128)} %refs_2_.1, bf16[96,2048]{1,0:T(8,128)(2,1)} %tokens.1, bf16[2048]{0:T(1024)(128)(2,1)} %refs_4_.1, ...), custom_call_target="tpu_custom_call" | custom-call | tf_op jit(solution)/shard_map/pallas_call | solution.py:345
  4.2 1.4 %collective-permute-done.came = bf16[96,1024]{1,0:T(8,128)(2,1)S(1)} collective-permute-done((bf16[96,1024]{1,0:T(8,128)(2,1)S(1)}, bf16[96,1024]{1,0:T(8,128)(2,1)S(1)}, u32[]{:S(2)}, u32[]{:S(2)}) %collective-permute-start) | collective-permute-done | bytes 196640 | tf_op jit(solution)/shard_map/ppermute | solution.py:43
  5.7 1.6 %collective-permute-start.1 = (bf16[96,512]{1,0:T(8,128)(2,1)S(1)}, bf16[96,512]{1,0:T(8,128)(2,1)S(1)}, u32[]{:S(2)}, u32[]{:S(2)}) collective-permute-start(bf16[96,512]{1,0:T(8,128)(2,1)S(1)} %shard_map.248), channel_id=1, source_target_pairs={{0,2},{1,3},{2,0},{3,1},{4,6},{5,7},{6,4},{7,5},{8,10},{9,11},{10,... | collective-permute-start | bytes 294920 | tf_op jit(solution)/shard_map/ppermute | solution.py:43
  7.6 3.0 %collective-permute-done.1.last = bf16[96,512]{1,0:T(8,128)(2,1)S(1)} collective-permute-done((bf16[96,512]{1,0:T(8,128)(2,1)S(1)}, bf16[96,512]{1,0:T(8,128)(2,1)S(1)}, u32[]{:S(2)}, u32[]{:S(2)}) %collective-permute-start.1) | collective-permute-done | bytes 98336 | tf_op jit(solution)/shard_map/ppermute | solution.py:43
  10.6 1.1 %shard_map.250 = (bf16[96,512]{1,0:T(8,128)(2,1)S(1)}, bf16[1536,128]{1,0:T(8,128)(2,1)}) custom-call(bf16[96,2048]{1,0:T(8,128)(2,1)S(1)} %copy-done, bf16[96,1024]{1,0:T(8,128)(2,1)S(1)} %get-tuple-element.27.own, bf16[96,1024]{1,0:T(8,128)(2,1)S(1)} %collective-permute-done.came, bf16[96,512]{1,0:T(8,128)(2,1)S(1)} %collective-permute-done.1.last, ...), custom_call_target="tpu_custom_call" | custom-call | tf_op jit(solution)/shard_map/pallas_call | solution.py:345
  11.7 14.2 %all-to-all-start = ((bf16[64,24,128]{2,1,0:T(8,128)(2,1)}), bf16[64,24,128]{2,1,0:T(8,128)(2,1)S(1)}, u32[]{:S(2)}, u32[]{:S(2)}) async-start(bf16[64,24,128]{2,1,0:T(8,128)(2,1)} %bitcast.9), calls=%async_computation | async-start | bytes 786432 | tf_op jit(solution)/shard_map/all_to_all | solution.py:452
  29.6 0.8 collective-permute-done.2.w1
  30.4 8.4 %collective-permute-done.3.w3 = bf16[512,256]{1,0:T(8,128)(2,1)S(1)} collective-permute-done((bf16[512,256]{1,0:T(8,128)(2,1)S(1)}, bf16[512,256]{1,0:T(8,128)(2,1)S(1)}, u32[]{:S(2)}, u32[]{:S(2)}) %collective-permute-start.3) | collective-permute-done | bytes 262176 | tf_op jit(solution)/shard_map/ppermute | solution.py:43
  38.8 3.1 %all-to-all-done = bf16[64,24,128]{2,1,0:T(8,128)(2,1)S(1)} async-done(((bf16[64,24,128]{2,1,0:T(8,128)(2,1)}), bf16[64,24,128]{2,1,0:T(8,128)(2,1)S(1)}, u32[]{:S(2)}, u32[]{:S(2)}) %all-to-all-start) | async-done | bytes 393248 | tf_op jit(solution)/shard_map/all_to_all | solution.py:452
  43.5 8.2 %collective-permute-done.4.w2 = bf16[512,256]{1,0:T(8,128)(2,1)S(1)} collective-permute-done((bf16[512,256]{1,0:T(8,128)(2,1)}, bf16[512,256]{1,0:T(8,128)(2,1)S(1)}, u32[]{:S(2)}, u32[]{:S(2)}) %collective-permute-start.4) | collective-permute-done | bytes 262176 | tf_op jit(solution)/shard_map/ppermute | solution.py:43
  52.9 5.9 %collective-permute-done.6.last = bf16[400,256]{1,0:T(8,128)(2,1)S(1)} collective-permute-done((bf16[400,256]{1,0:T(8,128)(2,1)S(1)}, bf16[400,256]{1,0:T(8,128)(2,1)S(1)}, u32[]{:S(2)}, u32[]{:S(2)}) %collective-permute-start.6) | collective-permute-done | bytes 204832 | tf_op jit(solution)/shard_map/ppermute | solution.py:43
  59.8 1.5 %collective-permute-start.11 = (bf16[128,512]{1,0:T(8,128)(2,1)S(1)}, bf16[128,512]{1,0:T(8,128)(2,1)S(1)}, u32[]{:S(2)}, u32[]{:S(2)}) collective-permute-start(bf16[128,512]{1,0:T(8,128)(2,1)S(1)} %copy-done.14), channel_id=1, source_target_pairs={{0,2},{1,3},{2,0},{3,1},{4,6},{5,7},{6,4},{7,5},{8,10},{9,11},{10,... | collective-permute-start | bytes 393224 | tf_op jit(solution)/shard_map/ppermute | solution.py:43
  62.0 2.7 %collective-permute-done.8.h2 = bf16[384,128]{1,0:T(8,128)(2,1)S(1)} collective-permute-done((bf16[384,128]{1,0:T(8,128)(2,1)S(1)}, bf16[384,128]{1,0:T(8,128)(2,1)S(1)}, u32[]{:S(2)}, u32[]{:S(2)}) %collective-permute-start.8) | collective-permute-done | bytes 98336 | tf_op jit(solution)/shard_map/ppermute | solution.py:43
  64.7 2.8 %collective-permute-done.11.w2 = bf16[128,512]{1,0:T(8,128)(2,1)S(1)} collective-permute-done((bf16[128,512]{1,0:T(8,128)(2,1)S(1)}, bf16[128,512]{1,0:T(8,128)(2,1)S(1)}, u32[]{:S(2)}, u32[]{:S(2)}) %collective-permute-start.11) | collective-permute-done | bytes 131104 | tf_op jit(solution)/shard_map/ppermute | solution.py:43
  67.5 1.0 collective-permute-done.12.w3
  68.5 1.4 %shard_map.256 = bf16[1536,128]{1,0:T(8,128)(2,1)} custom-call(bf16[384,128]{1,0:T(8,128)(2,1)S(1)} %shard_map.255.h0, bf16[384,128]{1,0:T(8,128)(2,1)S(1)} %collective-permute-done.7.h1, bf16[384,128]{1,0:T(8,128)(2,1)S(1)} %collective-permute-done.8.h2, bf16[384,128]{1,0:T(8,128)(2,1)S(1)} %collective-permute-done.9.h3, ...), custom_call_target="tpu_custom_call" | custom-call | tf_op jit(solution)/shard_map/pallas_call | solution.py:345
  69.9 9.7 %all-to-all-start.1 = ((bf16[64,24,128]{2,1,0:T(8,128)(2,1)}), bf16[64,24,128]{2,1,0:T(8,128)(2,1)S(1)}, u32[]{:S(2)}, u32[]{:S(2)}) async-start(bf16[64,24,128]{2,1,0:T(8,128)(2,1)} %bitcast.14), calls=%async_computation.1 | async-start | bytes 786432 | tf_op jit(solution)/shard_map/all_to_all | solution.py:491
  80.0 5.0 %collective-permute-done.14.a2 = bf16[96,512]{1,0:T(8,128)(2,1)S(1)} collective-permute-done((bf16[96,512]{1,0:T(8,128)(2,1)S(1)}, bf16[96,512]{1,0:T(8,128)(2,1)S(1)}, u32[]{:S(2)}, u32[]{:S(2)}) %collective-permute-start.14) | collective-permute-done | bytes 98336 | tf_op jit(solution)/shard_map/ppermute | solution.py:43
  85.0 1.3 %collective-permute-done.15.a3 = bf16[96,512]{1,0:T(8,128)(2,1)S(1)} collective-permute-done((bf16[96,512]{1,0:T(8,128)(2,1)S(1)}, bf16[96,512]{1,0:T(8,128)(2,1)S(1)}, u32[]{:S(2)}, u32[]{:S(2)}) %collective-permute-start.15) | collective-permute-done | bytes 98336 | tf_op jit(solution)/shard_map/ppermute | solution.py:43
  86.3 4.2 %shard_map.257 = (bf16[96,1024]{1,0:T(8,128)(2,1)}, bf16[96,1024]{1,0:T(8,128)(2,1)}, f32[96,128]{1,0:T(8,128)}) custom-call(bf16[1,2048]{1,0:T(2,128)(2,1)S(1)} %reshape.55.gains, bf16[96,512]{1,0:T(8,128)(2,1)S(1)} %get-tuple-element.45.a0.resid, bf16[96,512]{1,0:T(8,128)(2,1)S(1)} %collective-permute-done.13.a1, ...), custom_call_target="tpu_custom_call" | custom-call | tf_op jit(solution)/shard_map/pallas_call | solution.py:345
  90.7 1.5 %collective-permute-done.16.came = bf16[96,1024]{1,0:T(8,128)(2,1)S(1)} collective-permute-done((bf16[96,1024]{1,0:T(8,128)(2,1)}, bf16[96,1024]{1,0:T(8,128)(2,1)S(1)}, u32[]{:S(2)}, u32[]{:S(2)}) %collective-permute-start.16) | collective-permute-done | bytes 196640 | tf_op jit(solution)/shard_map/ppermute | solution.py:43
  92.2 0.9 copy-done.1
  95.4 2.7 %collective-permute-done.17.last = bf16[96,512]{1,0:T(8,128)(2,1)S(1)} collective-permute-done((bf16[96,512]{1,0:T(8,128)(2,1)S(1)}, bf16[96,512]{1,0:T(8,128)(2,1)S(1)}, u32[]{:S(2)}, u32[]{:S(2)}) %collective-permute-start.17) | collective-permute-done | bytes 98336 | tf_op jit(solution)/shard_map/ppermute | solution.py:43
  98.1 1.1 %shard_map.259 = bf16[96,512]{1,0:T(8,128)(2,1)} custom-call(bf16[1536,128]{1,0:T(8,128)(2,1)S(1)} %bitcast.19, bf16[192,384]{1,0:T(8,128)(2,1)S(1)} %get-tuple-element.42.w, f32[96,128]{1,0:T(8,128)S(1)} %get-tuple-element.43.share0, f32[96,128]{1,0:T(8,128)S(1)} %get-tuple-element.44.share1, bf16[96,512]{1,0:T(8,128)(2,1)S(1)} %get-tuple-element.45.a0.resid, ...), custom_call_target="tpu_custom_call" | custom-call | tf_op jit(solution)/shard_map/pallas_call | solution.py:345
  (71 shorter events, 11.5 us)
Async XLA Ops:
  4.1 21.8 %copy-start.3 = (bf16[1,2048,128]{2,1,0:T(8,128)(2,1)S(1)}, bf16[1,2048,128]{2,1,0:T(8,128)(2,1)}, u32[]{:S(2)}) copy-start(bf16[1,2048,128]{2,1,0:T(8,128)(2,1)} %param.41) | copy-start | bytes 1572868
  4.1 21.8 %copy-start.4 = (bf16[1,2048,128]{2,1,0:T(8,128)(2,1)S(1)}, bf16[1,2048,128]{2,1,0:T(8,128)(2,1)}, u32[]{:S(2)}) copy-start(bf16[1,2048,128]{2,1,0:T(8,128)(2,1)} %param.42) | copy-start | bytes 1572868
  4.1 25.4 %copy-start.17 = (bf16[2048]{0:T(1024)(128)(2,1)S(1)}, bf16[2048]{0:T(1024)(128)(2,1)}, u32[]{:S(2)}) copy-start(bf16[2048]{0:T(1024)(128)(2,1)} %param.37) | copy-start | bytes 12292
  4.1 1.5 %collective-permute-start = (bf16[96,1024]{1,0:T(8,128)(2,1)S(1)}, bf16[96,1024]{1,0:T(8,128)(2,1)S(1)}, u32[]{:S(2)}, u32[]{:S(2)}) collective-permute-start(bf16[96,1024]{1,0:T(8,128)(2,1)S(1)} %get-tuple-element.28), channel_id=1, source_target_pairs={{0,1},{1,0},{2,3},{3,2},{4,5},{5,4},{6,7},{7,6},{8,9},{9,8},{10,11... | collective-permute-start | bytes 589832 | tf_op jit(solution)/shard_map/ppermute | solution.py:43
  5.7 4.9 %collective-permute-start.1 = (bf16[96,512]{1,0:T(8,128)(2,1)S(1)}, bf16[96,512]{1,0:T(8,128)(2,1)S(1)}, u32[]{:S(2)}, u32[]{:S(2)}) collective-permute-start(bf16[96,512]{1,0:T(8,128)(2,1)S(1)} %shard_map.248), channel_id=1, source_target_pairs={{0,2},{1,3},{2,0},{3,1},{4,6},{5,7},{6,4},{7,5},{8,10},{9,11},{10,... | collective-permute-start | bytes 294920 | tf_op jit(solution)/shard_map/ppermute | solution.py:43
  11.7 30.2 %all-to-all-start = ((bf16[64,24,128]{2,1,0:T(8,128)(2,1)}), bf16[64,24,128]{2,1,0:T(8,128)(2,1)S(1)}, u32[]{:S(2)}, u32[]{:S(2)}) async-start(bf16[64,24,128]{2,1,0:T(8,128)(2,1)} %bitcast.9), calls=%async_computation | async-start | bytes 786432 | tf_op jit(solution)/shard_map/all_to_all | solution.py:452
  28.8 1.5 %collective-permute-start.2 = (bf16[512,256]{1,0:T(8,128)(2,1)S(1)}, bf16[512,256]{1,0:T(8,128)(2,1)S(1)}, u32[]{:S(2)}, u32[]{:S(2)}) collective-permute-start(bf16[512,256]{1,0:T(8,128)(2,1)S(1)} %get-tuple-element.31), channel_id=1, source_target_pairs={{0,1},{1,0},{2,3},{3,2},{4,5},{5,4},{6,7},{7,6},{8,9},{9,8},{10,11... | collective-permute-start | bytes 786440 | tf_op jit(solution)/shard_map/ppermute | solution.py:43
  28.8 10.0 %collective-permute-start.3 = (bf16[512,256]{1,0:T(8,128)(2,1)S(1)}, bf16[512,256]{1,0:T(8,128)(2,1)S(1)}, u32[]{:S(2)}, u32[]{:S(2)}) collective-permute-start(bf16[512,256]{1,0:T(8,128)(2,1)S(1)} %get-tuple-element.32), channel_id=1, source_target_pairs={{0,3},{1,2},{2,1},{3,0},{4,7},{5,6},{6,5},{7,4},{8,11},{9,10},{10,... | collective-permute-start | bytes 786440 | tf_op jit(solution)/shard_map/ppermute | solution.py:43
  42.7 9.4 %collective-permute-start.5 = (bf16[392,512]{1,0:T(8,128)(2,1)S(1)}, bf16[392,512]{1,0:T(8,128)(2,1)S(1)}, u32[]{:S(2)}, u32[]{:S(2)}) collective-permute-start(bf16[392,512]{1,0:T(8,128)(2,1)S(1)} %get-tuple-element.37), channel_id=1, source_target_pairs={{0,1},{1,0},{2,3},{3,2},{4,5},{5,4},{6,7},{7,6},{8,9},{9,8},{10,11... | collective-permute-start | bytes 1204232 | tf_op jit(solution)/shard_map/ppermute | solution.py:43
  42.8 8.9 %collective-permute-start.4 = (bf16[512,256]{1,0:T(8,128)(2,1)}, bf16[512,256]{1,0:T(8,128)(2,1)S(1)}, u32[]{:S(2)}, u32[]{:S(2)}) collective-permute-start(bf16[512,256]{1,0:T(8,128)(2,1)} %copy-done.10), channel_id=1, source_target_pairs={{0,2},{1,3},{2,0},{3,1},{4,6},{5,7},{6,4},{7,5},{8,10},{9,11},{10,... | collective-permute-start | bytes 786440 | tf_op jit(solution)/shard_map/ppermute | solution.py:43
  52.2 32.8 %copy-start.18 = (bf16[2048]{0:T(1024)(128)(2,1)S(1)}, bf16[2048]{0:T(1024)(128)(2,1)}, u32[]{:S(2)}) copy-start(bf16[2048]{0:T(1024)(128)(2,1)} %param.47) | copy-start | bytes 12292
  52.2 6.6 %collective-permute-start.6 = (bf16[400,256]{1,0:T(8,128)(2,1)S(1)}, bf16[400,256]{1,0:T(8,128)(2,1)S(1)}, u32[]{:S(2)}, u32[]{:S(2)}) collective-permute-start(bf16[400,256]{1,0:T(8,128)(2,1)S(1)} %shard_map.254), channel_id=1, source_target_pairs={{0,2},{1,3},{2,0},{3,1},{4,6},{5,7},{6,4},{7,5},{8,10},{9,11},{10,... | collective-permute-start | bytes 614408 | tf_op jit(solution)/shard_map/ppermute | solution.py:43
  59.1 5.6 %collective-permute-start.8 = (bf16[384,128]{1,0:T(8,128)(2,1)S(1)}, bf16[384,128]{1,0:T(8,128)(2,1)S(1)}, u32[]{:S(2)}, u32[]{:S(2)}) collective-permute-start(bf16[384,128]{1,0:T(8,128)(2,1)S(1)} %shard_map.255.h0), channel_id=1, source_target_pairs={{0,2},{1,3},{2,0},{3,1},{4,6},{5,7},{6,4},{7,5},{8,10},{9,11},{10,... | collective-permute-start | bytes 294920 | tf_op jit(solution)/shard_map/ppermute | solution.py:43
  59.8 4.9 %collective-permute-start.10 = (bf16[128,512]{1,0:T(8,128)(2,1)S(1)}, bf16[128,512]{1,0:T(8,128)(2,1)S(1)}, u32[]{:S(2)}, u32[]{:S(2)}) collective-permute-start(bf16[128,512]{1,0:T(8,128)(2,1)S(1)} %copy-done.16), channel_id=1, source_target_pairs={{0,1},{1,0},{2,3},{3,2},{4,5},{5,4},{6,7},{7,6},{8,9},{9,8},{10,11... | collective-permute-start | bytes 393224 | tf_op jit(solution)/shard_map/ppermute | solution.py:43
  59.8 7.7 %collective-permute-start.11 = (bf16[128,512]{1,0:T(8,128)(2,1)S(1)}, bf16[128,512]{1,0:T(8,128)(2,1)S(1)}, u32[]{:S(2)}, u32[]{:S(2)}) collective-permute-start(bf16[128,512]{1,0:T(8,128)(2,1)S(1)} %copy-done.14), channel_id=1, source_target_pairs={{0,2},{1,3},{2,0},{3,1},{4,6},{5,7},{6,4},{7,5},{8,10},{9,11},{10,... | collective-permute-start | bytes 393224 | tf_op jit(solution)/shard_map/ppermute | solution.py:43
  61.3 7.2 %collective-permute-start.12 = (bf16[128,512]{1,0:T(8,128)(2,1)S(1)}, bf16[128,512]{1,0:T(8,128)(2,1)S(1)}, u32[]{:S(2)}, u32[]{:S(2)}) collective-permute-start(bf16[128,512]{1,0:T(8,128)(2,1)S(1)} %copy-done.12), channel_id=1, source_target_pairs={{0,3},{1,2},{2,1},{3,0},{4,7},{5,6},{6,5},{7,4},{8,11},{9,10},{10,... | collective-permute-start | bytes 393224 | tf_op jit(solution)/shard_map/ppermute | solution.py:43
  61.7 6.9 %collective-permute-start.7 = (bf16[384,128]{1,0:T(8,128)(2,1)S(1)}, bf16[384,128]{1,0:T(8,128)(2,1)S(1)}, u32[]{:S(2)}, u32[]{:S(2)}) collective-permute-start(bf16[384,128]{1,0:T(8,128)(2,1)S(1)} %shard_map.255.h0), channel_id=1, source_target_pairs={{0,1},{1,0},{2,3},{3,2},{4,5},{5,4},{6,7},{7,6},{8,9},{9,8},{10,11... | collective-permute-start | bytes 294920 | tf_op jit(solution)/shard_map/ppermute | solution.py:43
  64.7 3.8 %collective-permute-start.9 = (bf16[384,128]{1,0:T(8,128)(2,1)S(1)}, bf16[384,128]{1,0:T(8,128)(2,1)S(1)}, u32[]{:S(2)}, u32[]{:S(2)}) collective-permute-start(bf16[384,128]{1,0:T(8,128)(2,1)S(1)} %collective-permute-done.8.h2), channel_id=1, source_target_pairs={{0,1},{1,0},{2,3},{3,2},{4,5},{5,4},{6,7},{7,6},{8,9},{9,8},{10,11... | collective-permute-start | bytes 294920 | tf_op jit(solution)/shard_map/ppermute | solution.py:43
  69.9 28.2 %all-to-all-start.1 = ((bf16[64,24,128]{2,1,0:T(8,128)(2,1)}), bf16[64,24,128]{2,1,0:T(8,128)(2,1)S(1)}, u32[]{:S(2)}, u32[]{:S(2)}) async-start(bf16[64,24,128]{2,1,0:T(8,128)(2,1)} %bitcast.14), calls=%async_computation.1 | async-start | bytes 786432 | tf_op jit(solution)/shard_map/all_to_all | solution.py:491
  79.6 5.4 %collective-permute-start.14 = (bf16[96,512]{1,0:T(8,128)(2,1)S(1)}, bf16[96,512]{1,0:T(8,128)(2,1)S(1)}, u32[]{:S(2)}, u32[]{:S(2)}) collective-permute-start(bf16[96,512]{1,0:T(8,128)(2,1)S(1)} %get-tuple-element.45.a0.resid), channel_id=1, source_target_pairs={{0,2},{1,3},{2,0},{3,1},{4,6},{5,7},{6,4},{7,5},{8,10},{9,11},{10,... | collective-permute-start | bytes 294920 | tf_op jit(solution)/shard_map/ppermute | solution.py:43
  80.0 5.0 %collective-permute-start.13 = (bf16[96,512]{1,0:T(8,128)(2,1)S(1)}, bf16[96,512]{1,0:T(8,128)(2,1)S(1)}, u32[]{:S(2)}, u32[]{:S(2)}) collective-permute-start(bf16[96,512]{1,0:T(8,128)(2,1)S(1)} %get-tuple-element.45.a0.resid), channel_id=1, source_target_pairs={{0,1},{1,0},{2,3},{3,2},{4,5},{5,4},{6,7},{7,6},{8,9},{9,8},{10,11... | collective-permute-start | bytes 294920 | tf_op jit(solution)/shard_map/ppermute | solution.py:43
  85.0 1.3 %collective-permute-start.15 = (bf16[96,512]{1,0:T(8,128)(2,1)S(1)}, bf16[96,512]{1,0:T(8,128)(2,1)S(1)}, u32[]{:S(2)}, u32[]{:S(2)}) collective-permute-start(bf16[96,512]{1,0:T(8,128)(2,1)S(1)} %collective-permute-done.14.a2), channel_id=1, source_target_pairs={{0,1},{1,0},{2,3},{3,2},{4,5},{5,4},{6,7},{7,6},{8,9},{9,8},{10,11... | collective-permute-start | bytes 294920 | tf_op jit(solution)/shard_map/ppermute | solution.py:43
  90.5 1.7 %collective-permute-start.16 = (bf16[96,1024]{1,0:T(8,128)(2,1)}, bf16[96,1024]{1,0:T(8,128)(2,1)S(1)}, u32[]{:S(2)}, u32[]{:S(2)}) collective-permute-start(bf16[96,1024]{1,0:T(8,128)(2,1)} %get-tuple-element.48), channel_id=1, source_target_pairs={{0,1},{1,0},{2,3},{3,2},{4,5},{5,4},{6,7},{7,6},{8,9},{9,8},{10,11... | collective-permute-start | bytes 589832 | tf_op jit(solution)/shard_map/ppermute | solution.py:43
  93.2 4.9 %collective-permute-start.17 = (bf16[96,512]{1,0:T(8,128)(2,1)S(1)}, bf16[96,512]{1,0:T(8,128)(2,1)S(1)}, u32[]{:S(2)}, u32[]{:S(2)}) collective-permute-start(bf16[96,512]{1,0:T(8,128)(2,1)S(1)} %shard_map.258), channel_id=1, source_target_pairs={{0,2},{1,3},{2,0},{3,1},{4,6},{5,7},{6,4},{7,5},{8,10},{9,11},{10,... | collective-permute-start | bytes 294920 | tf_op jit(solution)/shard_map/ppermute | solution.py:43
  (15 other events, 91.0 us)
